TPU v7x, 512 devices: a whole 4x8x8 slice. The times are simulated.
512 devices in a mesh: ep: 128 (over z, y, core), tp: 4 (over x).
Axes of the slice: x: 4, y: 8, z: 8, core: 2. Of those that a mesh axis runs over, the one named last changes fastest.
Arguments:
- tokens: bfloat16 [2048, 2048], P('ep'), may hold values from -6 to 6
- head_state: float32 [2048, 16, 4096], P('ep', 'tp'), may hold values from -6 to 6
- mixer_gain: float32 [2048], replicated, may hold values from 0.1 to 1.9
- w_query: bfloat16 [2048, 1024], P('ep', 'tp'), may hold values from -0.125 to 0.125
- w_key: bfloat16 [2048, 1024], P('ep', 'tp'), may hold values from -0.125 to 0.125
- w_value: bfloat16 [2048, 1024], P('ep', 'tp'), may hold values from -0.125 to 0.125
- decay_down: bfloat16 [2048, 64], replicated, may hold values from -0.125 to 0.125
- decay_up: bfloat16 [64, 1024], replicated, may hold values from -3 to 3
- decay_base: float32 [1024], P('tp'), may hold values from -4 to 0
- rate_down: bfloat16 [2048, 64], replicated, may hold values from -0.125 to 0.125
- rate_up: bfloat16 [64, 1024], replicated, may hold values from -0.75 to 0.75
- head_gain: float32 [1024], P('tp'), may hold values from 0.1 to 1.9
- w_out: bfloat16 [1024, 2048], P('tp', 'ep'), may hold values from -0.1875 to 0.1875
- expert_gain: float32 [2048], replicated, may hold values from 0.1 to 1.9
- expert_ids: int32 [2048, 2], P('ep'), may hold values from 0 to 127, all different within a row; in each aligned block of 16 rows (0 to 15, 16 to 31, ...) at most 1 rows name the same one
- route_weight: float32 [2048, 2], P('ep'), may hold values from 0.2 to 1
- w_gate: bfloat16 [128, 2048, 512], P('ep', None, 'tp'), may hold values from -0.125 to 0.125
- w_up: bfloat16 [128, 2048, 512], P('ep', None, 'tp'), may hold values from -0.125 to 0.125
- w_down: bfloat16 [128, 512, 2048], P('ep', 'tp'), may hold values from -0.25 to 0.25
Outputs:
- layer_out: bfloat16 [2048, 2048], P('ep', 'tp')
- next_state: float32 [2048, 16, 4096], P('ep', 'tp')
Inputs may be any that keep to these rules, and one draw needn't show every extreme that they name: `expert_ids`: each row names 2 different experts; among the 16 rows of one index of ep no expert is named more than 1 times, and in the rows of some indices one expert is named exactly 1 times.
All inputs are finite; a program needn't handle non-finite values.
Results may differ from a plain program's by a relative error of at most 0.015.
Values may be sent and summed in bfloat16 or wider, within the bound.
No kernel may reach another device: no remote copies, remote signals or barrier semaphores. Data moves between devices by JAX's collectives and lax.ppermute only.
A program may use at most 64 MiB of HBM per device.

v0:
```python
import jax
import jax.numpy as jnp
from jax import lax
from jax.sharding import PartitionSpec as P

norm_eps = 1e-06
group_eps = 0.00064


def sent_together(arrays, axis, dim, along):
    widths = [a.shape[along] for a in arrays]
    both = jnp.concatenate(arrays, axis=along)
    out = lax.all_gather(both, axis, axis=dim, tiled=True)
    return tuple(jnp.split(out, [sum(widths[:k]) for k in range(1, len(widths))], axis=along))


def from_everyone(array, axis):
    copies = jnp.broadcast_to(array, (lax.axis_size(axis), *array.shape))
    return lax.all_to_all(copies, axis, split_axis=0, concat_axis=0, tiled=True)


def taken_together(array, axis):
    everything = from_everyone(array, axis)
    return jnp.sum(everything.astype(jnp.float32), axis=0)


def split_up(array, dim, peers):
    before, after = (array.shape[:dim], array.shape[dim + 1 :])
    return jnp.moveaxis(array.reshape(*before, peers, -1, *after), dim, 0)


def sum_at_owner(array, axis, dim):
    peers = lax.axis_size(axis)
    parts = lax.all_to_all(split_up(array, dim, peers), axis, 0, 0, tiled=True)
    return jnp.sum(parts.astype(jnp.float32), axis=0)


def rms_scale(activity, gain):
    widened = activity.astype(jnp.float32)
    scaled = widened * lax.rsqrt(jnp.mean(widened * widened, axis=-1, keepdims=True) + norm_eps)
    return (scaled * gain).astype(jnp.bfloat16)


def low_rank(normed, decay_down, decay_up, decay_base, rate_down, rate_up):
    decay_low = jnp.tanh(jnp.dot(normed, decay_down, preferred_element_type=jnp.float32)).astype(
        jnp.bfloat16
    )
    decay_pre = decay_base + jnp.dot(decay_low, decay_up, preferred_element_type=jnp.float32)
    decays = jnp.exp(-jnp.exp(-jax.nn.softplus(-decay_pre) - 0.5))
    rate_low = jnp.dot(normed, rate_down, preferred_element_type=jnp.float32).astype(jnp.bfloat16)
    rates = jax.nn.sigmoid(jnp.dot(rate_low, rate_up, preferred_element_type=jnp.float32))
    return (decays, rates)


def recurrence(queries, key_rows, value_rows, decays, rates, old_state, head_gain):
    row_count, head_count, _ = old_state.shape
    head_size = queries.shape[1] // head_count
    head_shape = (row_count, head_count, head_size)
    query_heads = queries.astype(jnp.float32).reshape(head_shape)
    key_heads = key_rows.astype(jnp.float32).reshape(head_shape)
    value_heads = value_rows.astype(jnp.float32).reshape(head_shape)
    decay_heads = decays.reshape(head_shape)
    rate_heads = rates.reshape(head_shape)
    unit_keys = key_heads * lax.rsqrt(jnp.sum(key_heads * key_heads, axis=-1, keepdims=True) + 1.0)
    state_grid = old_state.reshape(row_count, head_count, head_size, head_size)
    removed = jnp.sum(state_grid * unit_keys[:, :, None, :], axis=-1)
    updated = (
        state_grid * decay_heads[:, :, None, :]
        - removed[:, :, :, None] * (unit_keys * rate_heads)[:, :, None, :]
        + value_heads[:, :, :, None] * key_heads[:, :, None, :]
    )
    readout = jnp.sum(updated * query_heads[:, :, None, :], axis=-1)
    centred = readout - jnp.mean(readout, axis=-1, keepdims=True)
    spread = jnp.mean(centred * centred, axis=-1, keepdims=True)
    scaled = centred * lax.rsqrt(spread + group_eps) * head_gain.reshape(head_count, head_size)
    return (
        updated.reshape(row_count, head_count, head_size * head_size),
        scaled.reshape(row_count, head_count * head_size).astype(jnp.bfloat16),
    )


def body(
    tokens,
    head_state,
    mixer_gain,
    w_query,
    w_key,
    w_value,
    decay_down,
    decay_up,
    decay_base,
    rate_down,
    rate_up,
    head_gain,
    w_out,
    expert_gain,
    expert_ids,
    route_weight,
    w_gate,
    w_up,
    w_down,
):
    seq_rows, width = tokens.shape
    local_cols = w_query.shape[1]
    head_lane = lax.axis_index("tp")
    normed = rms_scale(tokens, mixer_gain)
    pieces = sent_together((w_query, w_key, w_value), "ep", 0, 1)
    projected = tuple(
        (
            jnp.dot(normed, weight_piece, preferred_element_type=jnp.float32)
            for weight_piece in pieces
        )
    )
    queries, key_rows, value_rows = (member.astype(jnp.bfloat16) for member in projected)
    col_offset = head_lane * local_cols
    decays, rates = low_rank(
        normed,
        decay_down,
        lax.dynamic_slice_in_dim(decay_up, col_offset, local_cols, 1),
        decay_base,
        rate_down,
        lax.dynamic_slice_in_dim(rate_up, col_offset, local_cols, 1),
    )
    next_state, head_out = recurrence(
        queries, key_rows, value_rows, decays, rates, head_state, head_gain
    )
    partial_out = jnp.dot(
        head_out,
        lax.all_gather(w_out, "ep", axis=1, tiled=True),
        preferred_element_type=jnp.float32,
    )
    mixed_out = taken_together(partial_out.astype(jnp.bfloat16), "tp").astype(jnp.float32)
    residual = (tokens.astype(jnp.float32) + mixed_out).astype(jnp.bfloat16)
    expert_in = rms_scale(residual, expert_gain)
    experts = lax.axis_size("ep")
    top_count = expert_ids.shape[1]
    slot_count = max(1, 2 * seq_rows * top_count // experts)
    slot_total = experts * slot_count
    flat_ids = expert_ids.reshape(-1)
    matches = (flat_ids[:, None] == jnp.arange(experts, dtype=jnp.int32)[None, :]).astype(jnp.int32)
    slot_rank = jnp.sum((jnp.cumsum(matches, axis=0) - 1) * matches, axis=1)
    slot_ids = (flat_ids * slot_count + slot_rank).reshape(seq_rows, top_count)
    slot_match = (
        slot_ids[:, :, None] == jnp.arange(slot_total, dtype=jnp.int32)[None, None, :]
    ).astype(jnp.float32)
    picker = jnp.sum(slot_match, axis=1).astype(jnp.bfloat16)
    outbound = jnp.einsum("ts,td->sd", picker, expert_in, preferred_element_type=jnp.float32)
    outbound = outbound.astype(jnp.bfloat16).reshape(experts, slot_count, expert_in.shape[1])
    gate_local, up_local, down_local = (w_gate[0], w_up[0], w_down[0])
    arrived = lax.all_to_all(outbound, "ep", split_axis=0, concat_axis=0, tiled=True)
    sources, held, _ = arrived.shape
    flat_rows = arrived.reshape(sources * held, width)
    gate_act = jnp.dot(flat_rows, gate_local, preferred_element_type=jnp.float32)
    up_act = jnp.dot(flat_rows, up_local, preferred_element_type=jnp.float32)
    hidden = (jax.nn.silu(gate_act) * up_act).astype(jnp.bfloat16)
    partial_rows = jnp.dot(hidden, down_local, preferred_element_type=jnp.float32).reshape(
        sources, held, width
    )
    reduced = sum_at_owner(partial_rows.astype(jnp.bfloat16), "tp", 2)
    returned = lax.all_to_all(
        reduced.astype(jnp.bfloat16), "ep", split_axis=0, concat_axis=0, tiled=True
    )
    shares = route_weight / jnp.sum(route_weight, axis=1, keepdims=True)
    combine = jnp.sum(slot_match * shares[:, :, None], axis=1)
    routed = jnp.dot(combine, returned.reshape(slot_total, -1).astype(jnp.float32))
    own_cols = routed.shape[1]
    kept = lax.dynamic_slice_in_dim(residual, head_lane * own_cols, own_cols, 1)
    layer_out = (kept.astype(jnp.float32) + routed).astype(jnp.bfloat16)
    return (layer_out, next_state)


def solution(mesh):
    return jax.shard_map(
        body,
        mesh=mesh,
        in_specs=(
            P("ep", None),
            P("ep", "tp", None),
            P(),
            P("ep", "tp"),
            P("ep", "tp"),
            P("ep", "tp"),
            P(),
            P(),
            P("tp"),
            P(),
            P(),
            P("tp"),
            P("tp", "ep"),
            P(),
            P("ep", None),
            P("ep", None),
            P("ep", None, "tp"),
            P("ep", None, "tp"),
            P("ep", "tp", None),
        ),
        out_specs=(P("ep", "tp"), P("ep", "tp", None)),
        check_vma=False,
    )
```

profile of v0, /device:TPU:1, one launch (start us, length us, event | category | flops | bytes accessed | tf_op | source)
XLA Modules:
  0.0 267.5 jit_solution(1612568220506573948)
XLA Ops:
  7.2 1.4 pad_maximum_fusion
  10.4 1.4 fusion.10
  11.8 1.4 fusion.55
  13.4 2.1 reshape.119
  15.5 1.5 mul.201
  17.0 3.1 %mul.221 = f32[16,4,4096]{2,1,0:T(4,128)} reshape(f32[16,4,64,64]{3,2,1,0:T(8,128)} %mul.201) | data formatting | bytes 2097152 | tf_op jit(solution)/shard_map/mul | solution.py:68
  20.4 80.8 %all-gather.3.cloned.1.call-done = bf16[2048,768]{1,0:T(8,128)(2,1)} async-done(((bf16[16,768]{1,0:T(8,128)(2,1)}), bf16[2048,768]{1,0:T(8,128)(2,1)}) %all-gather.3.cloned.1.call-update) | async-done | bytes 3145744 | tf_op jit(solution)/shard_map/all_gather | solution.py:13
  101.2 1.5 fusion.14
  102.8 1.5 fusion.12
  104.4 1.5 fusion.13
  106.2 8.8 %broadcast_multiply_fusion = (f32[16,4,64,64]{3,2,1,0:T(8,128)}, f32[16,4,64]{2,1,0:T(4,128)S(1)}, f32[16,4,64,64]{3,2,1,0:T(8,128)}) fusion(f32[16,4,64]{2,1,0:T(4,128)S(1)} %reshape.128, f32[16,4,64]{2,1,0:T(4,128)S(1)} %reshape.129, f32[16,4,64]{2,1,0:T(4,128)S(1)} %reshape.130, f32[16,4,64,64]{3,2,1,0:T(8,128)S(1)} %reshape.119, ...), kind=kOutput, calls=%fused_computation.33 | output fusion | flops 2097215 | bytes 3260416 | tf_op jit(solution)/shard_map/mul | solution.py:69
  115.1 3.2 %mul.223 = f32[16,4,4096]{2,1,0:T(4,128)} reshape(f32[16,4,64,64]{3,2,1,0:T(8,128)} %get-tuple-element.12) | data formatting | bytes 2097152 | tf_op jit(solution)/shard_map/mul | solution.py:69
  118.2 1.8 mul.224
  120.2 1.8 mul.225
  122.0 4.1 %multiply_reduce_fusion.2 = (f32[16,4]{1,0:T(8,128)S(1)}, f32[16,4,4096]{2,1,0:T(4,128)}) fusion(f32[16,4,4096]{2,1,0:T(4,128)} %mul.225, f32[16,4,4096]{2,1,0:T(4,128)} %mul.224, f32[16,4,4096]{2,1,0:T(4,128)} %mul.223, f32[16,4,4096]{2,1,0:T(4,128)} %param.20, f32[16,4,4096]{2,1,0:T(4,128)} %mul.221), kind=kLoop, calls=%fused_computation.31 | loop fusion | flops 1310656 | bytes 6291712 | tf_op jit(solution)/shard_map/reduce_sum | solution.py:73
  126.5 54.1 %all-gather.5.cloned.1.call-done = bf16[256,2048]{0,1:T(8,128)(2,1)} async-done(((bf16[256,16]{0,1:T(8,128)(2,1)}), bf16[256,2048]{0,1:T(8,128)(2,1)}) %all-gather.5.cloned.1.call-update) | async-done | bytes 1048592 | tf_op jit(solution)/shard_map/all_gather | solution.py:129
  180.6 1.6 convolution_convert_fusion.2
  182.9 4.0 %all-to-all-start = ((bf16[4,16,2048]{2,1,0:T(8,128)(2,1)}), bf16[4,16,2048]{2,1,0:T(8,128)(2,1)S(1)}, u32[]{:S(2)}, u32[]{:S(2)}) async-start(bf16[4,16,2048]{2,1,0:T(8,128)(2,1)} %broadcast_in_dim.2), calls=%async_computation | async-start | bytes 524288 | tf_op jit(solution)/shard_map/all_to_all | solution.py:19
  187.3 5.5 %all-to-all-done = bf16[4,16,2048]{2,1,0:T(8,128)(2,1)S(1)} async-done(((bf16[4,16,2048]{2,1,0:T(8,128)(2,1)}), bf16[4,16,2048]{2,1,0:T(8,128)(2,1)S(1)}, u32[]{:S(2)}, u32[]{:S(2)}) %all-to-all-start) | async-done | bytes 262176 | tf_op jit(solution)/shard_map/all_to_all | solution.py:19
  193.8 1.0 reduce.4
  195.2 30.2 %all_to_all.20 = bf16[128,2,1024]{2,1,0:T(2,128)(2,1)S(1)} all-to-all(bf16[128,2,1024]{2,1,0:T(2,128)(2,1)S(1)} %reshape.132), channel_id=1, replica_groups=mesh['ep'=128,'tp'=4] {'ep'}, dimensions={0} | all-to-all | bytes 1048576 | tf_op jit(solution)/shard_map/all_to_all | solution.py:150
  227.5 12.2 %all_to_all.21 = bf16[4,128,1,512]{3,1,2,0:T(8,128)(2,1)S(1)} all-to-all(bf16[4,128,1,512]{3,1,2,0:T(8,128)(2,1)S(1)} %bitcast.38), channel_id=1, replica_groups=mesh['ep'=128,'tp'=4] {'tp'}, dimensions={0} | all-to-all | bytes 1048576 | tf_op jit(solution)/shard_map/all_to_all | solution.py:34
  241.2 5.8 %all-to-all-start.3 = ((bf16[128,2,256]{2,1,0:T(2,128)(2,1)}), bf16[128,2,256]{2,1,0:T(2,128)(2,1)S(1)}, u32[]{:S(2)}, u32[]{:S(2)}) async-start(bf16[128,2,256]{2,1,0:T(2,128)(2,1)} %reshape.134), calls=%async_computation.3 | async-start | bytes 262144 | tf_op jit(solution)/shard_map/all_to_all | solution.py:160
  247.0 12.8 %all-to-all-done.3 = bf16[128,2,256]{2,1,0:T(2,128)(2,1)S(1)} async-done(((bf16[128,2,256]{2,1,0:T(2,128)(2,1)}), bf16[128,2,256]{2,1,0:T(2,128)(2,1)S(1)}, u32[]{:S(2)}, u32[]{:S(2)}) %all-to-all-start.3) | async-done | bytes 131104 | tf_op jit(solution)/shard_map/all_to_all | solution.py:160
  (68 shorter events, 10.1 us)
Async XLA Ops:
  7.2 219.2 %copy-start = (bf16[1,128,2048]{2,1,0:T(8,128)(2,1)S(1)}, bf16[1,128,2048]{2,1,0:T(8,128)(2,1)}, u32[]{:S(2)}) copy-start(bf16[1,128,2048]{2,1,0:T(8,128)(2,1)} %param.37) | copy-start | bytes 1572868
  7.2 94.0 %all-gather.3.cloned.1.call-start = ((), (), s32[]{:S(2)}) async-start(), calls=%async_computation.4 | async-start | bytes 3170304 | tf_op jit(solution)/shard_map/all_gather | solution.py:13
  8.6 172.0 %all-gather.5.cloned.1.call-start = ((), (), s32[]{:S(2)}) async-start(), calls=%async_computation.5 | async-start | bytes 1056768 | tf_op jit(solution)/shard_map/all_gather | solution.py:129
  17.0 3.1 %copy-start.7 = (s32[16,2]{0,1:T(2,128)S(1)}, s32[16,2]{0,1:T(2,128)}, u32[]{:S(2)}) copy-start(s32[16,2]{0,1:T(2,128)} %param.33) | copy-start | bytes 388
  17.0 3.4 %copy-start.8 = (f32[16,2]{0,1:T(2,128)S(1)}, f32[16,2]{0,1:T(2,128)}, u32[]{:S(2)}) copy-start(f32[16,2]{0,1:T(2,128)} %param.34) | copy-start | bytes 388
  17.0 84.2 %copy-start.2 = (bf16[16,2048]{1,0:T(8,128)(2,1)S(1)}, bf16[16,2048]{1,0:T(8,128)(2,1)}, u32[]{:S(2)}) copy-start(bf16[16,2048]{1,0:T(8,128)(2,1)} %param.19) | copy-start | bytes 196612
  17.0 84.2 %copy-start.5 = (f32[2048]{0:T(1024)S(1)}, f32[2048]{0:T(1024)}, u32[]{:S(2)}) copy-start(f32[2048]{0:T(1024)} %param.21) | copy-start | bytes 24580
  115.1 3.2 %copy-start.1 = (f32[16,4,64,64]{3,2,1,0:T(8,128)S(1)}, f32[16,4,64,64]{3,2,1,0:T(8,128)}, u32[]{:S(2)}) copy-start(f32[16,4,64,64]{3,2,1,0:T(8,128)} %get-tuple-element.10) | copy-start | bytes 3145732
  122.0 58.6 %copy-start.9 = (f32[256]{0:T(256)S(1)}, f32[256]{0:T(256)}, u32[]{:S(2)}) copy-start(f32[256]{0:T(256)} %param.30) | copy-start | bytes 3076
  126.1 66.8 %copy-start.6 = (f32[2048]{0:T(1024)S(1)}, f32[2048]{0:T(1024)}, u32[]{:S(2)}) copy-start(f32[2048]{0:T(1024)} %param.32) | copy-start | bytes 24580
  182.9 9.9 %all-to-all-start = ((bf16[4,16,2048]{2,1,0:T(8,128)(2,1)}), bf16[4,16,2048]{2,1,0:T(8,128)(2,1)S(1)}, u32[]{:S(2)}, u32[]{:S(2)}) async-start(bf16[4,16,2048]{2,1,0:T(8,128)(2,1)} %broadcast_in_dim.2), calls=%async_computation | async-start | bytes 524288 | tf_op jit(solution)/shard_map/all_to_all | solution.py:19
  194.8 31.1 %copy-start.3 = (bf16[1,2048,128]{2,1,0:T(8,128)(2,1)S(1)}, bf16[1,2048,128]{2,1,0:T(8,128)(2,1)}, u32[]{:S(2)}) copy-start(bf16[1,2048,128]{2,1,0:T(8,128)(2,1)} %param.35) | copy-start | bytes 1572868
  195.2 31.1 %copy-start.4 = (bf16[1,2048,128]{2,1,0:T(8,128)(2,1)S(1)}, bf16[1,2048,128]{2,1,0:T(8,128)(2,1)}, u32[]{:S(2)}) copy-start(bf16[1,2048,128]{2,1,0:T(8,128)(2,1)} %param.36) | copy-start | bytes 1572868
  241.2 18.6 %all-to-all-start.3 = ((bf16[128,2,256]{2,1,0:T(2,128)(2,1)}), bf16[128,2,256]{2,1,0:T(2,128)(2,1)S(1)}, u32[]{:S(2)}, u32[]{:S(2)}) async-start(bf16[128,2,256]{2,1,0:T(2,128)(2,1)} %reshape.134), calls=%async_computation.3 | async-start | bytes 262144 | tf_op jit(solution)/shard_map/all_to_all | solution.py:160
Sparse Core Ops, SparseCore 0:
  11.7 89.4 all-gather.2
  104.2 76.3 all-gather.4
where the time goes:
time: 268 us; the launch traced here: 267 us
  waiting for transfers between devices  154 us (57%)
  blocking collectives  42.4 us (16%)
  other arithmetic  18.1 us (7%)
  local copies, waits for them, and re-layouts  17.9 us (7%)
  between operations  14.3 us (5%)
  matrix products  11.1 us (4%)
  starting transfers between devices  9.82 us (4%)
    all_gather x1, waiting for transfers between devices, sent_together(): out = lax.all_gather(both, axis, axis=dim, tiled=True)  80.8 us
    all_gather x1, waiting for transfers between devices, body(): lax.all_gather(w_out, 'ep', axis=1, tiled=True)  54.1 us
    all_to_all x1, blocking collectives, body(): lax.all_to_all(outbound, 'ep', split_axis=0, concat_axis=0, tiled=True)  30.2 us
    all_to_all x1, waiting for transfers between devices, body(): lax.all_to_all(reduced.astype(jnp.bfloat16), 'ep', split_axis=0, concat_a...  12.8 us
    all_to_all x1, blocking collectives, sum_at_owner(): parts = lax.all_to_all(split_up(array, dim, peers), axis, 0, 0, tiled=True)  12.2 us
    mul x1, other arithmetic, recurrence(): removed[:, :, :, None] * (unit_keys * rate_heads)[:, :, None, :]  8.83 us
    all_to_all x1, starting transfers between devices, body(): lax.all_to_all(reduced.astype(jnp.bfloat16), 'ep', split_axis=0, concat_a...  5.77 us
    all_to_all x1, waiting for transfers between devices, from_everyone(): return lax.all_to_all(copies, axis, split_axis=0, concat_axis=0, tiled=True)  5.47 us
  transfers between devices with their start and end apart: 4, of which 4 were waited for; matrix products, arithmetic and copies ran while one was open for 14% of the time, Pallas kernels for 0%

commit v1 on v0

v1 whole, which is shorter than its diff:
```python
import math

import jax
import jax.numpy as jnp
from jax import lax
from jax.sharding import Mesh, PartitionSpec as P

norm_eps = 1e-06
group_eps = 0.00064
EP = ("z", "y", "c")
PLANE = ("y", "c")


def swap(array, axis):
    return lax.all_to_all(array, axis, split_axis=0, concat_axis=0, tiled=True)


def to_all(array, axis):
    return swap(jnp.broadcast_to(array, (lax.axis_size(axis), *array.shape)), axis)


def rms_scale(activity, gain):
    widened = activity.astype(jnp.float32)
    scaled = widened * lax.rsqrt(jnp.mean(widened * widened, axis=-1, keepdims=True) + norm_eps)
    return (scaled * gain).astype(jnp.bfloat16)


def low_rank(normed, decay_down, decay_up, decay_base, rate_down, rate_up):
    decay_low = jnp.tanh(jnp.dot(normed, decay_down, preferred_element_type=jnp.float32)).astype(
        jnp.bfloat16
    )
    decay_pre = decay_base + jnp.dot(decay_low, decay_up, preferred_element_type=jnp.float32)
    decays = jnp.exp(-jnp.exp(-jax.nn.softplus(-decay_pre) - 0.5))
    rate_low = jnp.dot(normed, rate_down, preferred_element_type=jnp.float32).astype(jnp.bfloat16)
    rates = jax.nn.sigmoid(jnp.dot(rate_low, rate_up, preferred_element_type=jnp.float32))
    return (decays, rates)


def recurrence(queries, key_rows, value_rows, decays, rates, old_state, head_gain):
    row_count, head_count, _ = old_state.shape
    head_size = queries.shape[1] // head_count
    head_shape = (row_count, head_count, head_size)
    query_heads = queries.astype(jnp.float32).reshape(head_shape)
    key_heads = key_rows.astype(jnp.float32).reshape(head_shape)
    value_heads = value_rows.astype(jnp.float32).reshape(head_shape)
    decay_heads = decays.reshape(head_shape)
    rate_heads = rates.reshape(head_shape)
    unit_keys = key_heads * lax.rsqrt(jnp.sum(key_heads * key_heads, axis=-1, keepdims=True) + 1.0)
    state_grid = old_state.reshape(row_count, head_count, head_size, head_size)
    removed = jnp.sum(state_grid * unit_keys[:, :, None, :], axis=-1)
    updated = (
        state_grid * decay_heads[:, :, None, :]
        - removed[:, :, :, None] * (unit_keys * rate_heads)[:, :, None, :]
        + value_heads[:, :, :, None] * key_heads[:, :, None, :]
    )
    readout = jnp.sum(updated * query_heads[:, :, None, :], axis=-1)
    centred = readout - jnp.mean(readout, axis=-1, keepdims=True)
    spread = jnp.mean(centred * centred, axis=-1, keepdims=True)
    scaled = centred * lax.rsqrt(spread + group_eps) * head_gain.reshape(head_count, head_size)
    return (
        updated.reshape(row_count, head_count, head_size * head_size),
        scaled.reshape(row_count, head_count * head_size).astype(jnp.bfloat16),
    )


def body(
    tokens,
    head_state,
    mixer_gain,
    w_query,
    w_key,
    w_value,
    decay_down,
    decay_up,
    decay_base,
    rate_down,
    rate_up,
    head_gain,
    w_out,
    expert_gain,
    expert_ids,
    route_weight,
    w_gate,
    w_up,
    w_down,
):
    rows, width = tokens.shape
    cols = w_query.shape[1]
    layers = lax.axis_size("z")
    lanes = lax.axis_size("tp")
    experts = lax.axis_size(EP)
    lane = lax.axis_index("tp")
    block = width // layers
    quarter = width // lanes

    weights = lax.all_gather(
        jnp.concatenate([w_query, w_key, w_value, w_out.T], axis=1), PLANE, axis=0, tiled=True
    )
    normed = rms_scale(tokens, mixer_gain)
    spread_rows = swap(normed.reshape(rows, layers, block).transpose(1, 0, 2), "z")
    partial_rows = jnp.dot(
        spread_rows.reshape(layers * rows, block),
        weights[:, : 3 * cols],
        preferred_element_type=jnp.float32,
    ).astype(jnp.bfloat16)
    summed = swap(partial_rows.reshape(layers, rows, 3 * cols), "z")
    projected = jnp.sum(summed.astype(jnp.float32), axis=0).astype(jnp.bfloat16)
    queries, key_rows, value_rows = jnp.split(projected, 3, axis=1)
    decays, rates = low_rank(
        normed,
        decay_down,
        lax.dynamic_slice_in_dim(decay_up, lane * cols, cols, 1),
        decay_base,
        rate_down,
        lax.dynamic_slice_in_dim(rate_up, lane * cols, cols, 1),
    )
    next_state, head_out = recurrence(
        queries, key_rows, value_rows, decays, rates, head_state, head_gain
    )
    heads_here = to_all(head_out, "z").reshape(layers * rows, cols)
    partial_out = lax.dot_general(
        heads_here,
        weights[:, 3 * cols :],
        (((1,), (1,)), ((), ())),
        preferred_element_type=jnp.float32,
    ).astype(jnp.bfloat16)
    home_out = swap(partial_out.reshape(layers, rows, block), "z")
    quarters = home_out.reshape(lanes, layers // lanes, rows, block).transpose(0, 2, 1, 3)
    mixed_parts = swap(quarters.reshape(lanes, rows, quarter), "tp")
    mixed_out = jnp.sum(mixed_parts.astype(jnp.float32), axis=0)
    own_tokens = lax.dynamic_slice_in_dim(tokens, lane * quarter, quarter, 1)
    residual = (own_tokens.astype(jnp.float32) + mixed_out).astype(jnp.bfloat16)

    match = expert_ids[:, :, None] == jnp.arange(experts, dtype=jnp.int32)[None, None, :]
    picker = jnp.any(match, axis=1).astype(jnp.bfloat16)
    outbound = jnp.einsum("ts,td->sd", picker, residual, preferred_element_type=jnp.float32)
    arrived = swap(outbound.astype(jnp.bfloat16).reshape(experts, 1, quarter), EP)
    whole = to_all(arrived.reshape(experts, quarter), "tp")
    widened = whole.astype(jnp.float32)
    mean_square = jnp.sum(widened * widened, axis=(0, 2), keepdims=True) / width
    gains = expert_gain.reshape(lanes, 1, quarter)
    flat_rows = (widened * lax.rsqrt(mean_square + norm_eps) * gains).astype(jnp.bfloat16)
    flat_rows = flat_rows.transpose(1, 0, 2).reshape(experts, width)
    gate_act = jnp.dot(flat_rows, w_gate[0], preferred_element_type=jnp.float32)
    up_act = jnp.dot(flat_rows, w_up[0], preferred_element_type=jnp.float32)
    hidden = (jax.nn.silu(gate_act) * up_act).astype(jnp.bfloat16)
    expert_parts = jnp.dot(hidden, w_down[0], preferred_element_type=jnp.float32)
    expert_parts = expert_parts.astype(jnp.bfloat16).reshape(experts, lanes, quarter)
    gathered = swap(expert_parts.transpose(1, 0, 2), "tp")
    reduced = jnp.sum(gathered.astype(jnp.float32), axis=0).astype(jnp.bfloat16)
    returned = swap(reduced.reshape(experts, 1, quarter), EP).reshape(experts, quarter)
    shares = route_weight / jnp.sum(route_weight, axis=1, keepdims=True)
    combine = jnp.sum(match.astype(jnp.float32) * shares[:, :, None], axis=1)
    routed = jnp.dot(combine, returned.astype(jnp.float32))
    layer_out = (residual.astype(jnp.float32) + routed).astype(jnp.bfloat16)
    return (layer_out, next_state)


def solution(mesh):
    side = math.isqrt(mesh.shape["ep"] // 2)
    grid = Mesh(
        mesh.devices.reshape(side, side, 2, mesh.shape["tp"]), ("z", "y", "c", "tp")
    )
    return jax.shard_map(
        body,
        mesh=grid,
        in_specs=(
            P(EP, None),
            P(EP, "tp", None),
            P(),
            P(EP, "tp"),
            P(EP, "tp"),
            P(EP, "tp"),
            P(),
            P(),
            P("tp"),
            P(),
            P(),
            P("tp"),
            P("tp", EP),
            P(),
            P(EP, None),
            P(EP, None),
            P(EP, None, "tp"),
            P(EP, None, "tp"),
            P(EP, "tp", None),
        ),
        out_specs=(P(EP, "tp"), P(EP, "tp", None)),
        check_vma=False,
    )
```

time: 268 us -> 182 us (0.68)
  waiting for transfers between devices: 154 us -> 34.8 us
  starting transfers between devices: 9.82 us -> 36.5 us
  blocking collectives: 42.4 us -> 65.2 us
  between operations: 14.3 us -> 0.97 us
  matrix products: 11.1 us -> 5.15 us
    all_gather x2 -> x0, waiting for transfers between devices: 135 us -> none  [the longest x1 80.8 us: sent_together(): out = lax.all_gather(both, axis, axis=dim, tiled=True)]
    all_to_all x2 -> x6, starting transfers between devices: 9.74 us -> 36.5 us  [swap(): return lax.all_to_all(array, axis, split_axis=0, concat_axis=0, tiled=True)]
    all_gather x0 -> x1, blocking collectives: none -> 19.8 us  [body(): lax.all_gather(jnp.concatenate([w_query, w_key, w_value, w_out.T], axis=1...]
    all_to_all x2 -> x6, waiting for transfers between devices: 18.3 us -> 34.8 us  [swap(): return lax.all_to_all(array, axis, split_axis=0, concat_axis=0, tiled=True)]
    dot_general x8 -> x6, matrix products: 8.31 us -> 2.98 us  [the longest x1 0.9 us: body(): jnp.dot(spread_rows.reshape(layers * rows, block), weights[:, :3 * cols],...]
    all_to_all x2 -> x3, blocking collectives: 42.4 us -> 45.4 us  [swap(): return lax.all_to_all(array, axis, split_axis=0, concat_axis=0, tiled=True)]
  transfers between devices with their start and end apart: 4 -> 6, of which waited for: 4 -> 5; matrix products, arithmetic and copies ran while one was open for 14% -> 5% of each run, Pallas kernels for 0% -> 0%
where the time goes in v1:
time: 182 us; the launch traced here: 180 us
  blocking collectives  65.2 us (36%)
  starting transfers between devices  36.5 us (20%)
  waiting for transfers between devices  34.8 us (19%)
  other arithmetic  19.2 us (11%)
  local copies, waits for them, and re-layouts  18.7 us (10%)
  matrix products  5.15 us (3%)
    all_to_all x3, blocking collectives, swap(): return lax.all_to_all(array, axis, split_axis=0, concat_axis=0, tiled=True)  45.4 us
    all_to_all x6, starting transfers between devices, swap(): return lax.all_to_all(array, axis, split_axis=0, concat_axis=0, tiled=True)  36.5 us
    all_to_all x6, waiting for transfers between devices, swap(): return lax.all_to_all(array, axis, split_axis=0, concat_axis=0, tiled=True)  34.8 us
    all_gather x1, blocking collectives, body(): lax.all_gather(jnp.concatenate([w_query, w_key, w_value, w_out.T], axis=1...  19.8 us
    mul x1, other arithmetic, recurrence(): removed[:, :, :, None] * (unit_keys * rate_heads)[:, :, None, :]  8.83 us
    mul x3, local copies, waits for them, and re-layouts, recurrence(): state_grid * decay_heads[:, :, None, :]  4.58 us
    reduce_sum x1, other arithmetic, recurrence(): centred = readout - jnp.mean(readout, axis=-1, keepdims=True)  4.11 us
  transfers between devices with their start and end apart: 6, of which 5 were waited for; matrix products, arithmetic and copies ran while one was open for 5% of the time, Pallas kernels for 0%

profile of v1, /device:TPU:1, one launch (start us, length us, event | category | flops | bytes accessed | tf_op | source)
XLA Modules:
  0.0 180.5 jit_solution(7479068303643784111)
XLA Ops:
  3.3 10.9 %all-to-all-start = ((bf16[8,16,256]{2,1,0:T(8,128)(2,1)}), bf16[8,16,256]{2,1,0:T(8,128)(2,1)S(1)}, u32[]{:S(2)}, u32[]{:S(2)}) async-start(bf16[8,16,256]{2,1,0:T(8,128)(2,1)} %copy.61), calls=%async_computation | async-start | bytes 131072 | tf_op jit(solution)/shard_map/all_to_all | solution.py:15
  14.9 19.8 %all_gather.3 = bf16[256,1024]{1,0:T(8,128)(2,1)S(1)} all-gather(bf16[16,1024]{1,0:T(8,128)(2,1)S(1)} %pad_maximum_fusion), channel_id=1, replica_groups=mesh['z'=8,'y'=8,'c'=2,'tp'=4] {'y','c'}, dimensions={0}, use_global_device_ids=true | all-gather | bytes 557056 | tf_op jit(solution)/shard_map/all_gather | solution.py:96
  35.6 6.9 %all-to-all-start.1 = ((bf16[8,16,768]{2,1,0:T(8,128)(2,1)}), bf16[8,16,768]{2,1,0:T(8,128)(2,1)S(1)}, u32[]{:S(2)}, u32[]{:S(2)}) async-start(bf16[8,16,768]{2,1,0:T(8,128)(2,1)} %bitcast.3), calls=%async_computation.1 | async-start | bytes 393216 | tf_op jit(solution)/shard_map/all_to_all | solution.py:15
  42.6 1.1 fusion.10
  43.8 1.1 fusion.41
  45.0 2.1 %reshape.137 = f32[16,4,64,64]{3,2,1,0:T(8,128)S(1)} reshape(f32[16,4,4096]{2,1,0:T(4,128)} %param.20) | data formatting | bytes 2097152 | tf_op jit(solution)/shard_map/reshape | solution.py:49
  47.1 1.5 mul.202
  48.6 3.0 %mul.222 = f32[16,4,4096]{2,1,0:T(4,128)} reshape(f32[16,4,64,64]{3,2,1,0:T(8,128)} %mul.202) | data formatting | bytes 2097152 | tf_op jit(solution)/shard_map/mul | solution.py:52
  52.8 8.8 %broadcast_multiply_fusion = (f32[16,4,64,64]{3,2,1,0:T(8,128)}, f32[16,4,64]{2,1,0:T(4,128)S(1)}, f32[16,4,64,64]{3,2,1,0:T(8,128)}) fusion(f32[16,4,64]{2,1,0:T(4,128)S(1)} %reshape.155, f32[16,4,64]{2,1,0:T(4,128)S(1)} %reshape.156, f32[16,4,64]{2,1,0:T(4,128)S(1)} %reshape.157, f32[16,4,64,64]{3,2,1,0:T(8,128)S(1)} %reshape.137, ...), kind=kOutput, calls=%fused_computation.30 | output fusion | flops 2097215 | bytes 3260416 | tf_op jit(solution)/shard_map/mul | solution.py:53
  61.7 3.2 %mul.224 = f32[16,4,4096]{2,1,0:T(4,128)} reshape(f32[16,4,64,64]{3,2,1,0:T(8,128)} %get-tuple-element.11) | data formatting | bytes 2097152 | tf_op jit(solution)/shard_map/mul | solution.py:53
  64.8 1.8 %mul.225 = f32[16,4,4096]{2,1,0:T(4,128)} reshape(f32[16,4,64,64]{3,2,1,0:T(8,128)S(1)} %copy-done.1) | data formatting | bytes 2097152 | tf_op jit(solution)/shard_map/mul | solution.py:54
  66.8 1.8 %mul.226 = f32[16,4,4096]{2,1,0:T(4,128)} reshape(f32[16,4,64,64]{3,2,1,0:T(8,128)S(1)} %mul.220) | data formatting | bytes 2097152 | tf_op jit(solution)/shard_map/mul | solution.py:56
  68.6 4.1 %multiply_reduce_fusion.2 = (f32[16,4]{1,0:T(8,128)S(1)}, f32[16,4,4096]{2,1,0:T(4,128)}) fusion(f32[16,4,4096]{2,1,0:T(4,128)} %mul.226, f32[16,4,4096]{2,1,0:T(4,128)} %mul.225, f32[16,4,4096]{2,1,0:T(4,128)} %mul.224, f32[16,4,4096]{2,1,0:T(4,128)} %param.20, f32[16,4,4096]{2,1,0:T(4,128)} %mul.222), kind=kLoop, calls=%fused_computation.28 | loop fusion | flops 1310656 | bytes 6291712 | tf_op jit(solution)/shard_map/reduce_sum | solution.py:57
  73.1 12.9 %all_to_all.45 = bf16[8,16,256]{2,1,0:T(8,128)(2,1)S(1)} all-to-all(bf16[8,16,256]{2,1,0:T(8,128)(2,1)S(1)} %broadcast_in_dim.4), channel_id=1, replica_groups=mesh['z'=8,'y'=8,'c'=2,'tp'=4] {'z'}, dimensions={0} | all-to-all | bytes 131072 | tf_op jit(solution)/shard_map/all_to_all | solution.py:15
  86.3 9.6 %all_to_all.46 = bf16[8,16,256]{2,1,0:T(8,128)(2,1)S(1)} all-to-all(bf16[8,16,256]{2,1,0:T(8,128)(2,1)S(1)} %bitcast.70), channel_id=1, replica_groups=mesh['z'=8,'y'=8,'c'=2,'tp'=4] {'z'}, dimensions={0} | all-to-all | bytes 131072 | tf_op jit(solution)/shard_map/all_to_all | solution.py:15
  96.5 4.0 %all-to-all-start.4 = ((bf16[4,16,512]{2,1,0:T(8,128)(2,1)}), bf16[4,16,512]{2,1,0:T(8,128)(2,1)S(1)}, u32[]{:S(2)}, u32[]{:S(2)}) async-start(bf16[4,16,512]{2,1,0:T(8,128)(2,1)} %bitcast.23), calls=%async_computation.4 | async-start | bytes 131072 | tf_op jit(solution)/shard_map/all_to_all | solution.py:15
  100.6 4.4 %all-to-all-done.4 = bf16[4,16,512]{2,1,0:T(8,128)(2,1)S(1)} async-done(((bf16[4,16,512]{2,1,0:T(8,128)(2,1)}), bf16[4,16,512]{2,1,0:T(8,128)(2,1)S(1)}, u32[]{:S(2)}, u32[]{:S(2)}) %all-to-all-start.4) | async-done | bytes 65568 | tf_op jit(solution)/shard_map/all_to_all | solution.py:15
  107.2 22.9 %all_to_all.47 = bf16[128,2,256]{2,1,0:T(2,128)(2,1)S(1)} all-to-all(bf16[128,2,256]{2,1,0:T(2,128)(2,1)S(1)} %reshape.159), channel_id=1, replica_groups=mesh['z'=8,'y'=8,'c'=2,'tp'=4] {'z','y','c'}, dimensions={0} | all-to-all | bytes 262144 | tf_op jit(solution)/shard_map/all_to_all | solution.py:15
  131.2 3.6 %all-to-all-start.6 = ((bf16[4,128,512]{1,2,0:T(8,128)(2,1)}), bf16[4,128,512]{1,2,0:T(8,128)(2,1)S(1)}, u32[]{:S(2)}, u32[]{:S(2)}) async-start(bf16[4,128,512]{1,2,0:T(8,128)(2,1)} %broadcast_in_dim.5), calls=%async_computation.6 | async-start | bytes 1048576 | tf_op jit(solution)/shard_map/all_to_all | solution.py:15
  134.9 8.9 %all-to-all-done.6 = bf16[4,128,512]{1,2,0:T(8,128)(2,1)S(1)} async-done(((bf16[4,128,512]{1,2,0:T(8,128)(2,1)}), bf16[4,128,512]{1,2,0:T(8,128)(2,1)S(1)}, u32[]{:S(2)}, u32[]{:S(2)}) %all-to-all-start.6) | async-done | bytes 524320 | tf_op jit(solution)/shard_map/all_to_all | solution.py:15
  146.3 3.5 %all-to-all-start.7 = ((bf16[4,128,512]{2,1,0:T(8,128)(2,1)}), bf16[4,128,512]{2,1,0:T(8,128)(2,1)S(1)}, u32[]{:S(2)}, u32[]{:S(2)}) async-start(bf16[4,128,512]{2,1,0:T(8,128)(2,1)} %bitcast.59), calls=%async_computation.7 | async-start | bytes 1048576 | tf_op jit(solution)/shard_map/all_to_all | solution.py:15
  149.8 8.0 %all-to-all-done.7 = bf16[4,128,512]{2,1,0:T(8,128)(2,1)S(1)} async-done(((bf16[4,128,512]{2,1,0:T(8,128)(2,1)}), bf16[4,128,512]{2,1,0:T(8,128)(2,1)S(1)}, u32[]{:S(2)}, u32[]{:S(2)}) %all-to-all-start.7) | async-done | bytes 524320 | tf_op jit(solution)/shard_map/all_to_all | solution.py:15
  159.2 7.6 %all-to-all-start.8 = ((bf16[128,2,256]{2,1,0:T(2,128)(2,1)}), bf16[128,2,256]{2,1,0:T(2,128)(2,1)S(1)}, u32[]{:S(2)}, u32[]{:S(2)}) async-start(bf16[128,2,256]{2,1,0:T(2,128)(2,1)} %reshape.161), calls=%async_computation.8 | async-start | bytes 262144 | tf_op jit(solution)/shard_map/all_to_all | solution.py:15
  166.9 12.7 %all-to-all-done.8 = bf16[128,2,256]{2,1,0:T(2,128)(2,1)S(1)} async-done(((bf16[128,2,256]{2,1,0:T(2,128)(2,1)}), bf16[128,2,256]{2,1,0:T(2,128)(2,1)S(1)}, u32[]{:S(2)}, u32[]{:S(2)}) %all-to-all-start.8) | async-done | bytes 131104 | tf_op jit(solution)/shard_map/all_to_all | solution.py:15
  (76 shorter events, 15.2 us)
Async XLA Ops:
  0.6 144.2 %copy-start = (bf16[1,128,2048]{2,1,0:T(8,128)(2,1)S(1)}, bf16[1,128,2048]{2,1,0:T(8,128)(2,1)}, u32[]{:S(2)}) copy-start(bf16[1,128,2048]{2,1,0:T(8,128)(2,1)} %param.37) | copy-start | bytes 1572868
  0.6 41.9 %copy-start.4 = (bf16[2048,64]{0,1:T(8,128)(2,1)S(1)}, bf16[2048,64]{0,1:T(8,128)(2,1)}, u32[]{:S(2)}) copy-start(bf16[2048,64]{0,1:T(8,128)(2,1)} %param.28) | copy-start | bytes 786436
  0.7 43.1 %copy-start.5 = (bf16[2048,64]{0,1:T(8,128)(2,1)S(1)}, bf16[2048,64]{0,1:T(8,128)(2,1)}, u32[]{:S(2)}) copy-start(bf16[2048,64]{0,1:T(8,128)(2,1)} %param.25) | copy-start | bytes 786436
  0.7 43.1 %copy-start.9 = (f32[256]{0:T(256)S(1)}, f32[256]{0:T(256)}, u32[]{:S(2)}) copy-start(f32[256]{0:T(256)} %param.27) | copy-start | bytes 3076
  3.3 31.4 %all-to-all-start = ((bf16[8,16,256]{2,1,0:T(8,128)(2,1)}), bf16[8,16,256]{2,1,0:T(8,128)(2,1)S(1)}, u32[]{:S(2)}, u32[]{:S(2)}) async-start(bf16[8,16,256]{2,1,0:T(8,128)(2,1)} %copy.61), calls=%async_computation | async-start | bytes 131072 | tf_op jit(solution)/shard_map/all_to_all | solution.py:15
  35.6 16.7 %all-to-all-start.1 = ((bf16[8,16,768]{2,1,0:T(8,128)(2,1)}), bf16[8,16,768]{2,1,0:T(8,128)(2,1)S(1)}, u32[]{:S(2)}, u32[]{:S(2)}) async-start(bf16[8,16,768]{2,1,0:T(8,128)(2,1)} %bitcast.3), calls=%async_computation.1 | async-start | bytes 393216 | tf_op jit(solution)/shard_map/all_to_all | solution.py:15
  61.7 3.2 %copy-start.1 = (f32[16,4,64,64]{3,2,1,0:T(8,128)S(1)}, f32[16,4,64,64]{3,2,1,0:T(8,128)}, u32[]{:S(2)}) copy-start(f32[16,4,64,64]{3,2,1,0:T(8,128)} %get-tuple-element.6) | copy-start | bytes 3145732
  68.6 4.5 %copy-start.10 = (f32[256]{0:T(256)S(1)}, f32[256]{0:T(256)}, u32[]{:S(2)}) copy-start(f32[256]{0:T(256)} %param.30) | copy-start | bytes 3076
  68.6 31.9 %copy-start.8 = (s32[16,2]{0,1:T(2,128)S(1)}, s32[16,2]{0,1:T(2,128)}, u32[]{:S(2)}) copy-start(s32[16,2]{0,1:T(2,128)} %param.33) | copy-start | bytes 388
  86.1 48.8 %copy-start.6 = (f32[2048]{0:T(1024)S(1)}, f32[2048]{0:T(1024)}, u32[]{:S(2)}) copy-start(f32[2048]{0:T(1024)} %param.32) | copy-start | bytes 24580
  96.5 8.5 %all-to-all-start.4 = ((bf16[4,16,512]{2,1,0:T(8,128)(2,1)}), bf16[4,16,512]{2,1,0:T(8,128)(2,1)S(1)}, u32[]{:S(2)}, u32[]{:S(2)}) async-start(bf16[4,16,512]{2,1,0:T(8,128)(2,1)} %bitcast.23), calls=%async_computation.4 | async-start | bytes 131072 | tf_op jit(solution)/shard_map/all_to_all | solution.py:15
  130.1 14.4 %copy-start.2 = (bf16[1,2048,128]{2,1,0:T(8,128)(2,1)S(1)}, bf16[1,2048,128]{2,1,0:T(8,128)(2,1)}, u32[]{:S(2)}) copy-start(bf16[1,2048,128]{2,1,0:T(8,128)(2,1)} %param.35) | copy-start | bytes 1572868
  130.4 14.5 %copy-start.3 = (bf16[1,2048,128]{2,1,0:T(8,128)(2,1)S(1)}, bf16[1,2048,128]{2,1,0:T(8,128)(2,1)}, u32[]{:S(2)}) copy-start(bf16[1,2048,128]{2,1,0:T(8,128)(2,1)} %param.36) | copy-start | bytes 1572868
  131.2 12.6 %all-to-all-start.6 = ((bf16[4,128,512]{1,2,0:T(8,128)(2,1)}), bf16[4,128,512]{1,2,0:T(8,128)(2,1)S(1)}, u32[]{:S(2)}, u32[]{:S(2)}) async-start(bf16[4,128,512]{1,2,0:T(8,128)(2,1)} %broadcast_in_dim.5), calls=%async_computation.6 | async-start | bytes 1048576 | tf_op jit(solution)/shard_map/all_to_all | solution.py:15
  144.9 4.9 %copy-start.7 = (f32[16,2]{0,1:T(2,128)S(1)}, f32[16,2]{0,1:T(2,128)}, u32[]{:S(2)}) copy-start(f32[16,2]{0,1:T(2,128)} %param.34) | copy-start | bytes 388
  146.3 11.5 %all-to-all-start.7 = ((bf16[4,128,512]{2,1,0:T(8,128)(2,1)}), bf16[4,128,512]{2,1,0:T(8,128)(2,1)S(1)}, u32[]{:S(2)}, u32[]{:S(2)}) async-start(bf16[4,128,512]{2,1,0:T(8,128)(2,1)} %bitcast.59), calls=%async_computation.7 | async-start | bytes 1048576 | tf_op jit(solution)/shard_map/all_to_all | solution.py:15
  159.2 20.4 %all-to-all-start.8 = ((bf16[128,2,256]{2,1,0:T(2,128)(2,1)}), bf16[128,2,256]{2,1,0:T(2,128)(2,1)S(1)}, u32[]{:S(2)}, u32[]{:S(2)}) async-start(bf16[128,2,256]{2,1,0:T(2,128)(2,1)} %reshape.161), calls=%async_computation.8 | async-start | bytes 262144 | tf_op jit(solution)/shard_map/all_to_all | solution.py:15

commit v2 on v1

--- a/solution.py
+++ b/solution.py
@@ -1,8 +1,11 @@
+import functools
 import math
 
 import jax
 import jax.numpy as jnp
 from jax import lax
+from jax.experimental import pallas as pl
+from jax.experimental.pallas import tpu as pltpu
 from jax.sharding import Mesh, PartitionSpec as P
 
 norm_eps = 1e-06
@@ -36,31 +39,126 @@
     return (decays, rates)
 
 
-def recurrence(queries, key_rows, value_rows, decays, rates, old_state, head_gain):
-    row_count, head_count, _ = old_state.shape
-    head_size = queries.shape[1] // head_count
-    head_shape = (row_count, head_count, head_size)
-    query_heads = queries.astype(jnp.float32).reshape(head_shape)
-    key_heads = key_rows.astype(jnp.float32).reshape(head_shape)
-    value_heads = value_rows.astype(jnp.float32).reshape(head_shape)
-    decay_heads = decays.reshape(head_shape)
-    rate_heads = rates.reshape(head_shape)
-    unit_keys = key_heads * lax.rsqrt(jnp.sum(key_heads * key_heads, axis=-1, keepdims=True) + 1.0)
-    state_grid = old_state.reshape(row_count, head_count, head_size, head_size)
-    removed = jnp.sum(state_grid * unit_keys[:, :, None, :], axis=-1)
-    updated = (
-        state_grid * decay_heads[:, :, None, :]
-        - removed[:, :, :, None] * (unit_keys * rate_heads)[:, :, None, :]
-        + value_heads[:, :, :, None] * key_heads[:, :, None, :]
-    )
-    readout = jnp.sum(updated * query_heads[:, :, None, :], axis=-1)
-    centred = readout - jnp.mean(readout, axis=-1, keepdims=True)
-    spread = jnp.mean(centred * centred, axis=-1, keepdims=True)
-    scaled = centred * lax.rsqrt(spread + group_eps) * head_gain.reshape(head_count, head_size)
-    return (
-        updated.reshape(row_count, head_count, head_size * head_size),
-        scaled.reshape(row_count, head_count * head_size).astype(jnp.bfloat16),
-    )
+def split_terms(value):
+    high = value.astype(jnp.bfloat16)
+    return high, (value - high.astype(jnp.float32)).astype(jnp.bfloat16)
+
+
+def exact_dot(value, chooser):
+    high, low = split_terms(value)
+    return jnp.dot(high, chooser, preferred_element_type=jnp.float32) + jnp.dot(
+        low, chooser, preferred_element_type=jnp.float32
+    )
+
+
+def recurrence_kernel(size, parts, decays, rates, gain, state, new_state, spread_out):
+    count, cols = decays.shape
+    heads = cols // size
+    lines = state.shape[1]
+    wide = state.shape[2]
+    f32, bf16 = jnp.float32, jnp.bfloat16
+    iota = lambda shape, dim: lax.broadcasted_iota(jnp.int32, shape, dim)
+    projected = jnp.sum(parts[...].astype(f32), axis=0).astype(bf16).astype(f32)
+    queries = projected[:, :cols]
+    keys = projected[:, cols : 2 * cols]
+    values = projected[:, 2 * cols :]
+    square = (cols, cols)
+    same_head = iota(square, 0) // size == iota(square, 1) // size
+    head_sum = jnp.where(same_head, 1.0, 0.0).astype(f32)
+    head_mean = head_sum * (1.0 / size)
+    total = lambda x, m: jnp.dot(x, m, precision=lax.Precision.HIGHEST, preferred_element_type=f32)
+    units = keys * lax.rsqrt(total(keys * keys, head_sum) + 1.0)
+    removal = units * rates[...]
+
+    def by_line(x):
+        copies = jnp.broadcast_to(x[:, None, :], (count, 2 * heads, cols))
+        chosen = iota(copies.shape, 2) // size == iota(copies.shape, 1) % heads
+        kept = jnp.where(chosen, copies, 0.0)
+        folded = kept[:, :, :wide]
+        for start in range(wide, cols, wide):
+            folded = folded + kept[:, :, start : start + wide]
+        folded = folded.reshape(count * 2 * heads, wide)
+        both = folded + pltpu.roll(folded, size, 1)
+        return both.reshape(count, 1, 2 * heads, wide)
+
+    grid_shape = (count, lines // (2 * heads), 2 * heads, wide)
+    flat = (count * lines, wide)
+    old = state[...].reshape(grid_shape)
+    halves = (wide, wide)
+    half_sum = jnp.where(iota(halves, 0) // size == iota(halves, 1) // size, 1.0, 0.0).astype(bf16)
+    removed = exact_dot((old * by_line(units)).reshape(flat), half_sum).reshape(grid_shape)
+    pick = (lines, cols)
+    line, col = iota(pick, 0), iota(pick, 1)
+    owner = (col // size == line % heads) & ((col % size) // 2 == line // heads)
+    value_rows = jnp.where(owner[None], jnp.broadcast_to(values[:, None, :], (count, *pick)), 0.0)
+    tall = (cols, wide)
+    to_half = jnp.where(iota(tall, 0) % 2 == iota(tall, 1) // size, 1.0, 0.0).astype(bf16)
+    value_grid = jnp.dot(
+        value_rows.reshape(count * lines, cols).astype(bf16), to_half, preferred_element_type=f32
+    ).reshape(grid_shape)
+    updated = old * by_line(decays[...]) - removed * by_line(removal) + value_grid * by_line(keys)
+    new_state[...] = updated.reshape(new_state.shape)
+    broad = (wide, cols)
+    from_half = jnp.where(iota(broad, 0) // size == iota(broad, 1) % 2, 1.0, 0.0).astype(bf16)
+    reads = exact_dot((updated * by_line(queries)).reshape(flat), from_half)
+    readout = jnp.sum(jnp.where(owner[None], reads.reshape(count, *pick), 0.0), axis=1)
+    centred = readout - total(readout, head_mean)
+    spread = total(centred * centred, head_mean)
+    scaled = (centred * lax.rsqrt(spread + group_eps) * gain[...]).astype(bf16)
+    spread_out[...] = jnp.broadcast_to(scaled[None], spread_out.shape)
+
+
+def recurrence(parts, decays, rates, old_state, head_gain):
+    layers = parts.shape[0]
+    count, cols = decays.shape
+    heads, area = old_state.shape[1:]
+    size = math.isqrt(area)
+    wide = 2 * size
+    lines = area // wide
+    state = old_state.reshape(count, heads, lines, wide).transpose(0, 2, 1, 3)
+    state = state.reshape(count, lines * heads, wide)
+    new_state, spread_out = pl.pallas_call(
+        functools.partial(recurrence_kernel, size),
+        out_shape=(
+            jax.ShapeDtypeStruct(state.shape, jnp.float32),
+            jax.ShapeDtypeStruct((layers, count, cols), jnp.bfloat16),
+        ),
+        compiler_params=pltpu.CompilerParams(vmem_limit_bytes=40 << 20),
+        name="recurrence",
+    )(parts, decays, rates, head_gain.reshape(1, cols), state)
+    new_state = new_state.reshape(count, lines, heads, wide).transpose(0, 2, 1, 3)
+    return new_state.reshape(old_state.shape), spread_out
+
+
+def expert_kernel(rows, gain, gate, up, down, result):
+    lanes, _, quarter = rows.shape
+    f32 = jnp.float32
+    squares = jnp.zeros((rows.shape[1], 1), f32)
+    for part in range(lanes):
+        widened = rows[part].astype(f32)
+        squares = squares + jnp.sum(widened * widened, axis=1, keepdims=True)
+    scale = lax.rsqrt(squares / (lanes * quarter) + norm_eps)
+    gate_act = up_act = 0.0
+    for part in range(lanes):
+        here = slice(part * quarter, (part + 1) * quarter)
+        normed = (rows[part].astype(f32) * scale * gain[part]).astype(jnp.bfloat16)
+        gate_act = gate_act + jnp.dot(normed, gate[here], preferred_element_type=f32)
+        up_act = up_act + jnp.dot(normed, up[here], preferred_element_type=f32)
+    hidden = (gate_act / (1.0 + jnp.exp(-gate_act)) * up_act).astype(jnp.bfloat16)
+    for part in range(lanes):
+        here = slice(part * quarter, (part + 1) * quarter)
+        product = jnp.dot(hidden, down[:, here], preferred_element_type=f32)
+        result[part] = product.astype(jnp.bfloat16)
+
+
+def expert_rows(rows, gain, gate, up, down):
+    lanes, _, quarter = rows.shape
+    return pl.pallas_call(
+        expert_kernel,
+        out_shape=jax.ShapeDtypeStruct(rows.shape, jnp.bfloat16),
+        compiler_params=pltpu.CompilerParams(vmem_limit_bytes=20 << 20),
+        name="expert",
+    )(rows, gain.reshape(lanes, 1, quarter), gate, up, down)
 
 
 def body(
@@ -104,8 +202,6 @@
         preferred_element_type=jnp.float32,
     ).astype(jnp.bfloat16)
     summed = swap(partial_rows.reshape(layers, rows, 3 * cols), "z")
-    projected = jnp.sum(summed.astype(jnp.float32), axis=0).astype(jnp.bfloat16)
-    queries, key_rows, value_rows = jnp.split(projected, 3, axis=1)
     decays, rates = low_rank(
         normed,
         decay_down,
@@ -114,10 +210,8 @@
         rate_down,
         lax.dynamic_slice_in_dim(rate_up, lane * cols, cols, 1),
     )
-    next_state, head_out = recurrence(
-        queries, key_rows, value_rows, decays, rates, head_state, head_gain
-    )
-    heads_here = to_all(head_out, "z").reshape(layers * rows, cols)
+    next_state, spread_out = recurrence(summed, decays, rates, head_state, head_gain)
+    heads_here = swap(spread_out, "z").reshape(layers * rows, cols)
     partial_out = lax.dot_general(
         heads_here,
         weights[:, 3 * cols :],
@@ -136,17 +230,8 @@
     outbound = jnp.einsum("ts,td->sd", picker, residual, preferred_element_type=jnp.float32)
     arrived = swap(outbound.astype(jnp.bfloat16).reshape(experts, 1, quarter), EP)
     whole = to_all(arrived.reshape(experts, quarter), "tp")
-    widened = whole.astype(jnp.float32)
-    mean_square = jnp.sum(widened * widened, axis=(0, 2), keepdims=True) / width
-    gains = expert_gain.reshape(lanes, 1, quarter)
-    flat_rows = (widened * lax.rsqrt(mean_square + norm_eps) * gains).astype(jnp.bfloat16)
-    flat_rows = flat_rows.transpose(1, 0, 2).reshape(experts, width)
-    gate_act = jnp.dot(flat_rows, w_gate[0], preferred_element_type=jnp.float32)
-    up_act = jnp.dot(flat_rows, w_up[0], preferred_element_type=jnp.float32)
-    hidden = (jax.nn.silu(gate_act) * up_act).astype(jnp.bfloat16)
-    expert_parts = jnp.dot(hidden, w_down[0], preferred_element_type=jnp.float32)
-    expert_parts = expert_parts.astype(jnp.bfloat16).reshape(experts, lanes, quarter)
-    gathered = swap(expert_parts.transpose(1, 0, 2), "tp")
+    expert_parts = expert_rows(whole, expert_gain, w_gate[0], w_up[0], w_down[0])
+    gathered = swap(expert_parts, "tp")
     reduced = jnp.sum(gathered.astype(jnp.float32), axis=0).astype(jnp.bfloat16)
     returned = swap(reduced.reshape(experts, 1, quarter), EP).reshape(experts, quarter)
     shares = route_weight / jnp.sum(route_weight, axis=1, keepdims=True)

time: 182 us -> 157 us (0.86)
  other arithmetic: 19.2 us -> 3.46 us
  local copies, waits for them, and re-layouts: 18.7 us -> 3.52 us
  blocking collectives: 65.2 us -> 74.3 us
  Pallas kernels: 0 us -> 4.22 us
  starting transfers between devices: 36.5 us -> 33.2 us
  waiting for transfers between devices: 34.8 us -> 32.6 us
    mul x11 -> x0, local copies, waits for them, and re-layouts: 11.8 us -> none  [the longest x3 4.58 us: recurrence(): state_grid * decay_heads[:, :, None, :]]
    all_to_all x3 -> x4, blocking collectives: 45.4 us -> 54.5 us  [swap(): return lax.all_to_all(array, axis, split_axis=0, concat_axis=0, tiled=True)]
    mul x4 -> x0, other arithmetic: 9.02 us -> none  [the longest x1 8.83 us: recurrence(): removed[:, :, :, None] * (unit_keys * rate_heads)[:, :, None, :]]
    reduce_sum x5 -> x0, other arithmetic: 4.68 us -> none  [the longest x1 4.11 us: recurrence(): centred = readout - jnp.mean(readout, axis=-1, keepdims=True)]
    pallas_call x0 -> x2, Pallas kernels: none -> 4.22 us  [the longest x1 2.6 us: recurrence(): pl.pallas_call(functools.partial(recurrence_kernel, size), out_shape=(jax...]
    reshape x5 -> x0, local copies, waits for them, and re-layouts: 3.31 us -> none  [the longest x1 2.13 us: recurrence(): state_grid = old_state.reshape(row_count, head_count, head_size, head_size)]
    all_to_all x6 -> x5, starting transfers between devices: 36.5 us -> 33.2 us  [swap(): return lax.all_to_all(array, axis, split_axis=0, concat_axis=0, tiled=True)]
    all_to_all x6 -> x5, waiting for transfers between devices: 34.8 us -> 32.6 us  [swap(): return lax.all_to_all(array, axis, split_axis=0, concat_axis=0, tiled=True)]
  transfers between devices with their start and end apart: 6 -> 5, of which waited for: 5 -> 4; matrix products, arithmetic and copies ran while one was open for 5% -> 2% of each run, Pallas kernels for 0% -> 0%
where the time goes in v2:
time: 157 us; the launch traced here: 156 us
  blocking collectives  74.3 us (47%)
  starting transfers between devices  33.2 us (21%)
  waiting for transfers between devices  32.6 us (21%)
  matrix products  4.26 us (3%)
  Pallas kernels  4.22 us (3%)
  local copies, waits for them, and re-layouts  3.52 us (2%)
  other arithmetic  3.46 us (2%)
    all_to_all x4, blocking collectives, swap(): return lax.all_to_all(array, axis, split_axis=0, concat_axis=0, tiled=True)  54.5 us
    all_to_all x5, starting transfers between devices, swap(): return lax.all_to_all(array, axis, split_axis=0, concat_axis=0, tiled=True)  33.2 us
    all_to_all x5, waiting for transfers between devices, swap(): return lax.all_to_all(array, axis, split_axis=0, concat_axis=0, tiled=True)  32.6 us
    all_gather x1, blocking collectives, body(): lax.all_gather(jnp.concatenate([w_query, w_key, w_value, w_out.T], axis=1...  19.8 us
  transfers between devices with their start and end apart: 5, of which 4 were waited for; matrix products, arithmetic and copies ran while one was open for 2% of the time, Pallas kernels for 0%

profile of v2, /device:TPU:1, one launch (start us, length us, event | category | flops | bytes accessed | tf_op | source)
XLA Modules:
  0.0 156.4 jit_solution(8411307792401901056)
XLA Ops:
  0.7 1.0 fusion.8
  1.7 0.8 fusion.10
  3.2 11.0 %all-to-all-start = ((bf16[8,16,256]{2,1,0:T(8,128)(2,1)}), bf16[8,16,256]{2,1,0:T(8,128)(2,1)S(1)}, u32[]{:S(2)}, u32[]{:S(2)}) async-start(bf16[8,16,256]{2,1,0:T(8,128)(2,1)} %copy.50), calls=%async_computation | async-start | bytes 131072 | tf_op jit(solution)/shard_map/all_to_all | solution.py:18
  14.2 19.8 %all_gather.3 = bf16[256,1024]{1,0:T(8,128)(2,1)S(1)} all-gather(bf16[16,1024]{1,0:T(8,128)(2,1)S(1)} %pad_maximum_fusion), channel_id=1, replica_groups=mesh['z'=8,'y'=8,'c'=2,'tp'=4] {'y','c'}, dimensions={0}, use_global_device_ids=true | all-gather | bytes 557056 | tf_op jit(solution)/shard_map/all_gather | solution.py:194
  34.0 0.9 convolution_convert_fusion
  34.9 6.9 %all-to-all-start.1 = ((bf16[8,16,768]{2,1,0:T(8,128)(2,1)}), bf16[8,16,768]{2,1,0:T(8,128)(2,1)S(1)}, u32[]{:S(2)}, u32[]{:S(2)}) async-start(bf16[8,16,768]{2,1,0:T(8,128)(2,1)} %bitcast.3), calls=%async_computation.1 | async-start | bytes 393216 | tf_op jit(solution)/shard_map/all_to_all | solution.py:18
  41.9 1.1 fusion.4.rates
  43.0 1.1 fusion.20.decays
  44.1 7.5 %all-to-all-done.1.parts = bf16[8,16,768]{2,1,0:T(8,128)(2,1)S(1)} async-done(((bf16[8,16,768]{2,1,0:T(8,128)(2,1)}), bf16[8,16,768]{2,1,0:T(8,128)(2,1)S(1)}, u32[]{:S(2)}, u32[]{:S(2)}) %all-to-all-start.1) | async-done | bytes 196640 | tf_op jit(solution)/shard_map/all_to_all | solution.py:18
  52.3 2.6 %recurrence.1 = (f32[16,128,128]{2,1,0:T(8,128)}, bf16[8,16,256]{2,1,0:T(8,128)(2,1)S(1)}) custom-call(bf16[8,16,768]{2,1,0:T(8,128)(2,1)S(1)} %all-to-all-done.1.parts, f32[16,256]{1,0:T(8,128)S(1)} %fusion.20.decays, f32[16,256]{1,0:T(8,128)S(1)} %fusion.4.rates, f32[1,256]{1,0:T(1,128)S(1)} %bitcast.52, f32[16,128,128]{2,1,0:T(8,128)S(1)} %bitcast.47), custom_call_target="tpu_custom_call" | custom-call | tf_op jit(solution)/shard_map/recurrence/pallas_call | solution.py:120
  54.9 9.7 %all_to_all.45 = bf16[8,16,256]{2,1,0:T(8,128)(2,1)S(1)} all-to-all(bf16[8,16,256]{2,1,0:T(8,128)(2,1)S(1)} %get-tuple-element.4), channel_id=1, replica_groups=mesh['z'=8,'y'=8,'c'=2,'tp'=4] {'z'}, dimensions={0} | all-to-all | bytes 131072 | tf_op jit(solution)/shard_map/all_to_all | solution.py:18
  64.8 9.7 %all_to_all.46 = bf16[8,16,256]{2,1,0:T(8,128)(2,1)S(1)} all-to-all(bf16[8,16,256]{2,1,0:T(8,128)(2,1)S(1)} %bitcast.60), channel_id=1, replica_groups=mesh['z'=8,'y'=8,'c'=2,'tp'=4] {'z'}, dimensions={0} | all-to-all | bytes 131072 | tf_op jit(solution)/shard_map/all_to_all | solution.py:18
  75.1 4.1 %all-to-all-start.4 = ((bf16[4,16,512]{2,1,0:T(8,128)(2,1)}), bf16[4,16,512]{2,1,0:T(8,128)(2,1)S(1)}, u32[]{:S(2)}, u32[]{:S(2)}) async-start(bf16[4,16,512]{2,1,0:T(8,128)(2,1)} %bitcast.29), calls=%async_computation.4 | async-start | bytes 131072 | tf_op jit(solution)/shard_map/all_to_all | solution.py:18
  79.3 4.4 %all-to-all-done.4 = bf16[4,16,512]{2,1,0:T(8,128)(2,1)S(1)} async-done(((bf16[4,16,512]{2,1,0:T(8,128)(2,1)}), bf16[4,16,512]{2,1,0:T(8,128)(2,1)S(1)}, u32[]{:S(2)}, u32[]{:S(2)}) %all-to-all-start.4) | async-done | bytes 65568 | tf_op jit(solution)/shard_map/all_to_all | solution.py:18
  85.2 23.4 %all_to_all.47 = bf16[128,2,256]{2,1,0:T(2,128)(2,1)S(1)} all-to-all(bf16[128,2,256]{2,1,0:T(2,128)(2,1)S(1)} %reshape.85), channel_id=1, replica_groups=mesh['z'=8,'y'=8,'c'=2,'tp'=4] {'z','y','c'}, dimensions={0} | all-to-all | bytes 262144 | tf_op jit(solution)/shard_map/all_to_all | solution.py:18
  108.8 11.7 %all_to_all.48.rows = bf16[4,128,512]{2,1,0:T(8,128)(2,1)S(1)} all-to-all(bf16[4,128,512]{2,1,0:T(8,128)(2,1)S(1)} %broadcast_in_dim.2), channel_id=1, replica_groups=mesh['z'=8,'y'=8,'c'=2,'tp'=4] {'tp'}, dimensions={0} | all-to-all | bytes 1048576 | tf_op jit(solution)/shard_map/all_to_all | solution.py:18
  120.6 1.6 %expert.1 = bf16[4,128,512]{2,1,0:T(8,128)(2,1)} custom-call(bf16[4,128,512]{2,1,0:T(8,128)(2,1)S(1)} %all_to_all.48.rows, f32[4,1,512]{2,1,0:T(1,128)S(1)} %bitcast.51, bf16[2048,128]{1,0:T(8,128)(2,1)S(1)} %bitcast.48, bf16[2048,128]{1,0:T(8,128)(2,1)S(1)} %bitcast.49, bf16[128,2048]{1,0:T(8,128)(2,1)S(1)} %bitcast.50), custom_call_target="tpu_custom_call" | custom-call | tf_op jit(solution)/shard_map/expert/pallas_call | solution.py:156
  122.2 3.6 %all-to-all-start.7 = ((bf16[4,128,512]{2,1,0:T(8,128)(2,1)}), bf16[4,128,512]{2,1,0:T(8,128)(2,1)S(1)}, u32[]{:S(2)}, u32[]{:S(2)}) async-start(bf16[4,128,512]{2,1,0:T(8,128)(2,1)} %expert.1), calls=%async_computation.7 | async-start | bytes 1048576 | tf_op jit(solution)/shard_map/all_to_all | solution.py:18
  125.8 8.0 %all-to-all-done.7 = bf16[4,128,512]{2,1,0:T(8,128)(2,1)S(1)} async-done(((bf16[4,128,512]{2,1,0:T(8,128)(2,1)}), bf16[4,128,512]{2,1,0:T(8,128)(2,1)S(1)}, u32[]{:S(2)}, u32[]{:S(2)}) %all-to-all-start.7) | async-done | bytes 524320 | tf_op jit(solution)/shard_map/all_to_all | solution.py:18
  133.9 0.7 reduce.2
  134.6 0.7 reshape.87
  135.2 7.5 %all-to-all-start.8 = ((bf16[128,2,256]{2,1,0:T(2,128)(2,1)}), bf16[128,2,256]{2,1,0:T(2,128)(2,1)S(1)}, u32[]{:S(2)}, u32[]{:S(2)}) async-start(bf16[128,2,256]{2,1,0:T(2,128)(2,1)} %reshape.87), calls=%async_computation.8 | async-start | bytes 262144 | tf_op jit(solution)/shard_map/all_to_all | solution.py:18
  142.9 12.7 %all-to-all-done.8 = bf16[128,2,256]{2,1,0:T(2,128)(2,1)S(1)} async-done(((bf16[128,2,256]{2,1,0:T(2,128)(2,1)}), bf16[128,2,256]{2,1,0:T(2,128)(2,1)S(1)}, u32[]{:S(2)}, u32[]{:S(2)}) %all-to-all-start.8) | async-done | bytes 131104 | tf_op jit(solution)/shard_map/all_to_all | solution.py:18
  155.7 0.7 fusion.1
  (54 shorter events, 4.2 us)
Async XLA Ops:
  0.6 41.2 %copy-start = (bf16[2048,64]{0,1:T(8,128)(2,1)S(1)}, bf16[2048,64]{0,1:T(8,128)(2,1)}, u32[]{:S(2)}) copy-start(bf16[2048,64]{0,1:T(8,128)(2,1)} %param.28) | copy-start | bytes 786436
  0.6 1.1 copy-start.7
  3.2 11.0 %copy-start.9 = (bf16[256,16]{0,1:T(8,128)(2,1)S(1)}, bf16[256,16]{0,1:T(8,128)(2,1)}, u32[]{:S(2)}) copy-start(bf16[256,16]{0,1:T(8,128)(2,1)} %param.31) | copy-start | bytes 24580
  3.2 11.0 %copy-start.10 = (bf16[16,256]{1,0:T(8,128)(2,1)S(1)}, bf16[16,256]{1,0:T(8,128)(2,1)}, u32[]{:S(2)}) copy-start(bf16[16,256]{1,0:T(8,128)(2,1)} %param.24) | copy-start | bytes 24580
  3.2 11.0 %copy-start.11 = (bf16[16,256]{1,0:T(8,128)(2,1)S(1)}, bf16[16,256]{1,0:T(8,128)(2,1)}, u32[]{:S(2)}) copy-start(bf16[16,256]{1,0:T(8,128)(2,1)} %param.23) | copy-start | bytes 24580
  3.2 11.0 %copy-start.12 = (bf16[16,256]{1,0:T(8,128)(2,1)S(1)}, bf16[16,256]{1,0:T(8,128)(2,1)}, u32[]{:S(2)}) copy-start(bf16[16,256]{1,0:T(8,128)(2,1)} %param.22) | copy-start | bytes 24580
  3.2 30.9 %all-to-all-start = ((bf16[8,16,256]{2,1,0:T(8,128)(2,1)}), bf16[8,16,256]{2,1,0:T(8,128)(2,1)S(1)}, u32[]{:S(2)}, u32[]{:S(2)}) async-start(bf16[8,16,256]{2,1,0:T(8,128)(2,1)} %copy.50), calls=%async_computation | async-start | bytes 131072 | tf_op jit(solution)/shard_map/all_to_all | solution.py:18
  34.0 17.6 %copy-start.1 = (f32[16,4,4096]{2,1,0:T(4,128)S(1)}, f32[16,4,4096]{2,1,0:T(4,128)}, u32[]{:S(2)}) copy-start(f32[16,4,4096]{2,1,0:T(4,128)} %param.20) | copy-start | bytes 3145732
  34.9 16.7 %all-to-all-start.1 = ((bf16[8,16,768]{2,1,0:T(8,128)(2,1)}), bf16[8,16,768]{2,1,0:T(8,128)(2,1)S(1)}, u32[]{:S(2)}, u32[]{:S(2)}) async-start(bf16[8,16,768]{2,1,0:T(8,128)(2,1)} %bitcast.3), calls=%async_computation.1 | async-start | bytes 393216 | tf_op jit(solution)/shard_map/all_to_all | solution.py:18
  41.9 1.1 copy-start.8
  41.9 1.1 copy-start.15
  51.6 0.7 copy-start.6
  75.1 4.1 %copy-start.14 = (s32[16,2]{0,1:T(2,128)S(1)}, s32[16,2]{0,1:T(2,128)}, u32[]{:S(2)}) copy-start(s32[16,2]{0,1:T(2,128)} %param.33) | copy-start | bytes 388
  75.1 8.6 %all-to-all-start.4 = ((bf16[4,16,512]{2,1,0:T(8,128)(2,1)}), bf16[4,16,512]{2,1,0:T(8,128)(2,1)S(1)}, u32[]{:S(2)}, u32[]{:S(2)}) async-start(bf16[4,16,512]{2,1,0:T(8,128)(2,1)} %bitcast.29), calls=%async_computation.4 | async-start | bytes 131072 | tf_op jit(solution)/shard_map/all_to_all | solution.py:18
  108.7 11.8 %copy-start.4 = (bf16[1,128,2048]{2,1,0:T(8,128)(2,1)S(1)}, bf16[1,128,2048]{2,1,0:T(8,128)(2,1)}, u32[]{:S(2)}) copy-start(bf16[1,128,2048]{2,1,0:T(8,128)(2,1)} %param.37) | copy-start | bytes 1572868
  108.8 11.8 %copy-start.5 = (f32[2048]{0:T(1024)S(1)}, f32[2048]{0:T(1024)}, u32[]{:S(2)}) copy-start(f32[2048]{0:T(1024)} %param.32) | copy-start | bytes 24580
  108.8 11.7 %copy-start.2 = (bf16[1,2048,128]{2,1,0:T(8,128)(2,1)S(1)}, bf16[1,2048,128]{2,1,0:T(8,128)(2,1)}, u32[]{:S(2)}) copy-start(bf16[1,2048,128]{2,1,0:T(8,128)(2,1)} %param.35) | copy-start | bytes 1572868
  108.8 11.7 %copy-start.3 = (bf16[1,2048,128]{2,1,0:T(8,128)(2,1)S(1)}, bf16[1,2048,128]{2,1,0:T(8,128)(2,1)}, u32[]{:S(2)}) copy-start(bf16[1,2048,128]{2,1,0:T(8,128)(2,1)} %param.36) | copy-start | bytes 1572868
  122.2 3.6 %copy-start.13 = (f32[16,2]{0,1:T(2,128)S(1)}, f32[16,2]{0,1:T(2,128)}, u32[]{:S(2)}) copy-start(f32[16,2]{0,1:T(2,128)} %param.34) | copy-start | bytes 388
  122.2 11.6 %all-to-all-start.7 = ((bf16[4,128,512]{2,1,0:T(8,128)(2,1)}), bf16[4,128,512]{2,1,0:T(8,128)(2,1)S(1)}, u32[]{:S(2)}, u32[]{:S(2)}) async-start(bf16[4,128,512]{2,1,0:T(8,128)(2,1)} %expert.1), calls=%async_computation.7 | async-start | bytes 1048576 | tf_op jit(solution)/shard_map/all_to_all | solution.py:18
  135.2 20.4 %all-to-all-start.8 = ((bf16[128,2,256]{2,1,0:T(2,128)(2,1)}), bf16[128,2,256]{2,1,0:T(2,128)(2,1)S(1)}, u32[]{:S(2)}, u32[]{:S(2)}) async-start(bf16[128,2,256]{2,1,0:T(2,128)(2,1)} %reshape.87), calls=%async_computation.8 | async-start | bytes 262144 | tf_op jit(solution)/shard_map/all_to_all | solution.py:18

commit v3 on v2

--- a/solution.py
+++ b/solution.py
@@ -16,10 +16,6 @@
 
 def swap(array, axis):
     return lax.all_to_all(array, axis, split_axis=0, concat_axis=0, tiled=True)
-
-
-def to_all(array, axis):
-    return swap(jnp.broadcast_to(array, (lax.axis_size(axis), *array.shape)), axis)
 
 
 def rms_scale(activity, gain):
@@ -130,20 +126,73 @@
     return new_state.reshape(old_state.shape), spread_out
 
 
-def expert_kernel(rows, gain, gate, up, down, result):
-    lanes, _, quarter = rows.shape
+def dispatch_kernel(slots, lane, parts, tokens, gain, outbound, kept, residual, lines, rows):
+    layers, lanes, count, block = parts.shape
+    wide = lines.shape[2]
     f32 = jnp.float32
-    squares = jnp.zeros((rows.shape[1], 1), f32)
-    for part in range(lanes):
-        widened = rows[part].astype(f32)
-        squares = squares + jnp.sum(widened * widened, axis=1, keepdims=True)
-    scale = lax.rsqrt(squares / (lanes * quarter) + norm_eps)
+    squares = jnp.zeros((count, 1), f32)
+    for z in range(layers):
+        mixed = parts[z, 0].astype(f32)
+        for part in range(1, lanes):
+            mixed = mixed + parts[z, part].astype(f32)
+        here = tokens[:, z * block : (z + 1) * block].astype(f32)
+        residual[z] = (here + mixed).astype(jnp.bfloat16).astype(f32)
+        squares = squares + jnp.sum(residual[z] * residual[z], axis=1, keepdims=True)
+    scale = lax.rsqrt(squares / (layers * block) + norm_eps)
+    for z in range(layers):
+        normed = residual[z] * scale * gain[:, z * block : (z + 1) * block]
+        for piece in range(block // wide):
+            lines[:count, z * (block // wide) + piece, :] = normed[:, piece * wide : (piece + 1) * wide]
+    lines[count] = jnp.zeros(lines.shape[1:], f32)
+    rows[...] = lines[...].astype(jnp.bfloat16)
+
+    def send(step, carry):
+        outbound[step] = rows[slots[step]]
+        return carry
+
+    lax.fori_loop(0, outbound.shape[0], send, 0, unroll=8)
+    own = layers // lanes
+    for piece in range(own):
+        kept[:, piece * block : (piece + 1) * block] = residual[lane[0] * own + piece]
+
+
+def dispatch(parts, tokens, gain, slots, lane):
+    layers, lanes, count, block = parts.shape
+    width = layers * block
+    wide = 128
+    pieces = width // wide
+    vmem = pl.BlockSpec(memory_space=pltpu.VMEM)
+    smem = pl.BlockSpec(memory_space=pltpu.SMEM)
+    return pl.pallas_call(
+        dispatch_kernel,
+        in_specs=[smem, smem, vmem, vmem, vmem],
+        out_specs=(vmem, vmem),
+        out_shape=(
+            jax.ShapeDtypeStruct((slots.shape[0], pieces, wide), jnp.bfloat16),
+            jax.ShapeDtypeStruct((count, width // lanes), jnp.float32),
+        ),
+        scratch_shapes=[
+            pltpu.VMEM((layers, count, block), jnp.float32),
+            pltpu.VMEM((count + 1, pieces, wide), jnp.float32),
+            pltpu.VMEM((count + 1, pieces, wide), jnp.bfloat16),
+        ],
+        compiler_params=pltpu.CompilerParams(vmem_limit_bytes=20 << 20),
+        name="dispatch",
+    )(slots, lane.reshape(1), parts, tokens, gain.reshape(1, width))
+
+
+def expert_kernel(rows, gate, up, down, result, lines):
+    _, pieces, wide = rows.shape
+    lanes, _, quarter = result.shape
+    f32 = jnp.float32
+    lines[...] = rows[...].astype(f32)
     gate_act = up_act = 0.0
-    for part in range(lanes):
-        here = slice(part * quarter, (part + 1) * quarter)
-        normed = (rows[part].astype(f32) * scale * gain[part]).astype(jnp.bfloat16)
-        gate_act = gate_act + jnp.dot(normed, gate[here], preferred_element_type=f32)
-        up_act = up_act + jnp.dot(normed, up[here], preferred_element_type=f32)
+    for piece in range(0, pieces, 2):
+        here = slice(piece * wide, (piece + 2) * wide)
+        both = jnp.concatenate([lines[:, piece, :], lines[:, piece + 1, :]], axis=1)
+        both = both.astype(jnp.bfloat16)
+        gate_act = gate_act + jnp.dot(both, gate[here], preferred_element_type=f32)
+        up_act = up_act + jnp.dot(both, up[here], preferred_element_type=f32)
     hidden = (gate_act / (1.0 + jnp.exp(-gate_act)) * up_act).astype(jnp.bfloat16)
     for part in range(lanes):
         here = slice(part * quarter, (part + 1) * quarter)
@@ -151,14 +200,16 @@
         result[part] = product.astype(jnp.bfloat16)
 
 
-def expert_rows(rows, gain, gate, up, down):
-    lanes, _, quarter = rows.shape
+def expert_rows(rows, gate, up, down, lanes):
     return pl.pallas_call(
         expert_kernel,
-        out_shape=jax.ShapeDtypeStruct(rows.shape, jnp.bfloat16),
+        out_shape=jax.ShapeDtypeStruct(
+            (lanes, rows.shape[0], down.shape[1] // lanes), jnp.bfloat16
+        ),
+        scratch_shapes=[pltpu.VMEM(rows.shape, jnp.float32)],
         compiler_params=pltpu.CompilerParams(vmem_limit_bytes=20 << 20),
         name="expert",
-    )(rows, gain.reshape(lanes, 1, quarter), gate, up, down)
+    )(rows, gate, up, down)
 
 
 def body(
@@ -218,26 +269,25 @@
         (((1,), (1,)), ((), ())),
         preferred_element_type=jnp.float32,
     ).astype(jnp.bfloat16)
-    home_out = swap(partial_out.reshape(layers, rows, block), "z")
-    quarters = home_out.reshape(lanes, layers // lanes, rows, block).transpose(0, 2, 1, 3)
-    mixed_parts = swap(quarters.reshape(lanes, rows, quarter), "tp")
-    mixed_out = jnp.sum(mixed_parts.astype(jnp.float32), axis=0)
-    own_tokens = lax.dynamic_slice_in_dim(tokens, lane * quarter, quarter, 1)
-    residual = (own_tokens.astype(jnp.float32) + mixed_out).astype(jnp.bfloat16)
-
+    home_out = swap(
+        jnp.broadcast_to(
+            partial_out.reshape(layers, 1, rows, block), (layers, lanes, rows, block)
+        ).reshape(layers * lanes, rows, block),
+        ("z", "tp"),
+    ).reshape(layers, lanes, rows, block)
     match = expert_ids[:, :, None] == jnp.arange(experts, dtype=jnp.int32)[None, None, :]
-    picker = jnp.any(match, axis=1).astype(jnp.bfloat16)
-    outbound = jnp.einsum("ts,td->sd", picker, residual, preferred_element_type=jnp.float32)
-    arrived = swap(outbound.astype(jnp.bfloat16).reshape(experts, 1, quarter), EP)
-    whole = to_all(arrived.reshape(experts, quarter), "tp")
-    expert_parts = expert_rows(whole, expert_gain, w_gate[0], w_up[0], w_down[0])
+    order = jnp.arange(rows, dtype=jnp.int32)[:, None, None]
+    slots = jnp.min(jnp.where(match, order, rows), axis=(0, 1))
+    outbound, residual = dispatch(home_out, tokens, expert_gain, slots, lane)
+    arrived = swap(outbound, EP)
+    expert_parts = expert_rows(arrived, w_gate[0], w_up[0], w_down[0], lanes)
     gathered = swap(expert_parts, "tp")
     reduced = jnp.sum(gathered.astype(jnp.float32), axis=0).astype(jnp.bfloat16)
     returned = swap(reduced.reshape(experts, 1, quarter), EP).reshape(experts, quarter)
     shares = route_weight / jnp.sum(route_weight, axis=1, keepdims=True)
     combine = jnp.sum(match.astype(jnp.float32) * shares[:, :, None], axis=1)
     routed = jnp.dot(combine, returned.astype(jnp.float32))
-    layer_out = (residual.astype(jnp.float32) + routed).astype(jnp.bfloat16)
+    layer_out = (residual + routed).astype(jnp.bfloat16)
     return (layer_out, next_state)
 
 

time: 157 us -> 150 us (0.955)
  blocking collectives: 74.3 us -> 60.3 us
  waiting for transfers between devices: 32.6 us -> 40.4 us
    all_to_all x4 -> x2, blocking collectives: 54.5 us -> 40.4 us  [swap(): return lax.all_to_all(array, axis, split_axis=0, concat_axis=0, tiled=True)]
    all_to_all x5, waiting for transfers between devices: 32.6 us -> 40.4 us  [swap(): return lax.all_to_all(array, axis, split_axis=0, concat_axis=0, tiled=True)]
where the time goes in v3:
time: 150 us; the launch traced here: 149 us
  blocking collectives  60.3 us (40%)
  waiting for transfers between devices  40.4 us (27%)
  starting transfers between devices  32 us (21%)
  Pallas kernels  5.43 us (4%)
  matrix products  4.04 us (3%)
  local copies, waits for them, and re-layouts  3.43 us (2%)
  other arithmetic  2.77 us (2%)
    all_to_all x2, blocking collectives, swap(): return lax.all_to_all(array, axis, split_axis=0, concat_axis=0, tiled=True)  40.4 us
    all_to_all x5, waiting for transfers between devices, swap(): return lax.all_to_all(array, axis, split_axis=0, concat_axis=0, tiled=True)  40.4 us
    all_to_all x5, starting transfers between devices, swap(): return lax.all_to_all(array, axis, split_axis=0, concat_axis=0, tiled=True)  32 us
    all_gather x1, blocking collectives, body(): lax.all_gather(jnp.concatenate([w_query, w_key, w_value, w_out.T], axis=1...  19.8 us
  transfers between devices with their start and end apart: 5, of which 4 were waited for; matrix products, arithmetic and copies ran while one was open for 2% of the time, Pallas kernels for 0%

profile of v3, /device:TPU:1, one launch (start us, length us, event | category | flops | bytes accessed | tf_op | source)
XLA Modules:
  0.0 149.2 jit_solution(8033190099560190335)
XLA Ops:
  0.7 1.0 fusion.7
  1.7 0.8 fusion.9
  3.2 11.0 %all-to-all-start = ((bf16[8,16,256]{2,1,0:T(8,128)(2,1)}), bf16[8,16,256]{2,1,0:T(8,128)(2,1)S(1)}, u32[]{:S(2)}, u32[]{:S(2)}) async-start(bf16[8,16,256]{2,1,0:T(8,128)(2,1)} %copy.45), calls=%async_computation | async-start | bytes 131072 | tf_op jit(solution)/shard_map/all_to_all | solution.py:18
  14.2 19.8 %all_gather.3 = bf16[256,1024]{1,0:T(8,128)(2,1)S(1)} all-gather(bf16[16,1024]{1,0:T(8,128)(2,1)S(1)} %pad_maximum_fusion), channel_id=1, replica_groups=mesh['z'=8,'y'=8,'c'=2,'tp'=4] {'y','c'}, dimensions={0}, use_global_device_ids=true | all-gather | bytes 557056 | tf_op jit(solution)/shard_map/all_gather | solution.py:245
  34.0 0.9 convolution_convert_fusion
  34.9 6.9 %all-to-all-start.1 = ((bf16[8,16,768]{2,1,0:T(8,128)(2,1)}), bf16[8,16,768]{2,1,0:T(8,128)(2,1)S(1)}, u32[]{:S(2)}, u32[]{:S(2)}) async-start(bf16[8,16,768]{2,1,0:T(8,128)(2,1)} %bitcast.4), calls=%async_computation.1 | async-start | bytes 393216 | tf_op jit(solution)/shard_map/all_to_all | solution.py:18
  41.9 1.1 fusion.3.rates
  43.0 1.1 fusion.19.decays
  44.1 7.5 %all-to-all-done.1.parts = bf16[8,16,768]{2,1,0:T(8,128)(2,1)S(1)} async-done(((bf16[8,16,768]{2,1,0:T(8,128)(2,1)}), bf16[8,16,768]{2,1,0:T(8,128)(2,1)S(1)}, u32[]{:S(2)}, u32[]{:S(2)}) %all-to-all-start.1) | async-done | bytes 196640 | tf_op jit(solution)/shard_map/all_to_all | solution.py:18
  51.6 0.7 copy-done.7
  52.3 2.6 %recurrence.1 = (f32[16,128,128]{2,1,0:T(8,128)}, bf16[8,16,256]{2,1,0:T(8,128)(2,1)S(1)}) custom-call(bf16[8,16,768]{2,1,0:T(8,128)(2,1)S(1)} %all-to-all-done.1.parts, f32[16,256]{1,0:T(8,128)S(1)} %fusion.19.decays, f32[16,256]{1,0:T(8,128)S(1)} %fusion.3.rates, f32[1,256]{1,0:T(1,128)S(1)} %bitcast.44, f32[16,128,128]{2,1,0:T(8,128)S(1)} %bitcast.38), custom_call_target="tpu_custom_call" | custom-call | tf_op jit(solution)/shard_map/recurrence/pallas_call | solution.py:116
  54.9 9.7 %all_to_all.35 = bf16[8,16,256]{2,1,0:T(8,128)(2,1)S(1)} all-to-all(bf16[8,16,256]{2,1,0:T(8,128)(2,1)S(1)} %get-tuple-element.6), channel_id=1, replica_groups=mesh['z'=8,'y'=8,'c'=2,'tp'=4] {'z'}, dimensions={0} | all-to-all | bytes 131072 | tf_op jit(solution)/shard_map/all_to_all | solution.py:18
  64.8 0.7 broadcast_in_dim.30
  65.5 4.8 %all-to-all-start.3 = ((bf16[32,16,256]{2,1,0:T(8,128)(2,1)}), bf16[32,16,256]{2,1,0:T(8,128)(2,1)S(1)}, u32[]{:S(2)}, u32[]{:S(2)}) async-start(bf16[32,16,256]{2,1,0:T(8,128)(2,1)} %bitcast.11), calls=%async_computation.3 | async-start | bytes 524288 | tf_op jit(solution)/shard_map/all_to_all | solution.py:18
  70.4 10.4 %all-to-all-done.3 = bf16[32,16,256]{2,1,0:T(8,128)(2,1)S(1)} async-done(((bf16[32,16,256]{2,1,0:T(8,128)(2,1)}), bf16[32,16,256]{2,1,0:T(8,128)(2,1)S(1)}, u32[]{:S(2)}, u32[]{:S(2)}) %all-to-all-start.3) | async-done | bytes 262176 | tf_op jit(solution)/shard_map/all_to_all | solution.py:18
  80.8 1.0 dispatch.1
  81.8 30.8 %all_to_all.36.rows = bf16[128,16,128]{2,1,0:T(8,128)(2,1)S(1)} all-to-all(bf16[128,16,128]{2,1,0:T(8,128)(2,1)S(1)} %get-tuple-element.8), channel_id=1, replica_groups=mesh['z'=8,'y'=8,'c'=2,'tp'=4] {'z','y','c'}, dimensions={0} | all-to-all | bytes 1048576 | tf_op jit(solution)/shard_map/all_to_all | solution.py:18
  112.6 1.8 %expert.1 = bf16[4,128,512]{2,1,0:T(8,128)(2,1)} custom-call(bf16[128,16,128]{2,1,0:T(8,128)(2,1)S(1)} %all_to_all.36.rows, bf16[2048,128]{1,0:T(8,128)(2,1)S(1)} %bitcast.40, bf16[2048,128]{1,0:T(8,128)(2,1)S(1)} %bitcast.41, bf16[128,2048]{1,0:T(8,128)(2,1)S(1)} %bitcast.42), custom_call_target="tpu_custom_call" | custom-call | tf_op jit(solution)/shard_map/expert/pallas_call | solution.py:204
  114.4 3.6 %all-to-all-start.5 = ((bf16[4,128,512]{2,1,0:T(8,128)(2,1)}), bf16[4,128,512]{2,1,0:T(8,128)(2,1)S(1)}, u32[]{:S(2)}, u32[]{:S(2)}) async-start(bf16[4,128,512]{2,1,0:T(8,128)(2,1)} %expert.1), calls=%async_computation.5 | async-start | bytes 1048576 | tf_op jit(solution)/shard_map/all_to_all | solution.py:18
  118.1 9.8 %all-to-all-done.5 = bf16[4,128,512]{2,1,0:T(8,128)(2,1)S(1)} async-done(((bf16[4,128,512]{2,1,0:T(8,128)(2,1)}), bf16[4,128,512]{2,1,0:T(8,128)(2,1)S(1)}, u32[]{:S(2)}, u32[]{:S(2)}) %all-to-all-start.5) | async-done | bytes 524320 | tf_op jit(solution)/shard_map/all_to_all | solution.py:18
  129.1 0.7 reshape.79
  129.8 5.7 %all-to-all-start.6 = ((bf16[128,2,256]{2,1,0:T(2,128)(2,1)}), bf16[128,2,256]{2,1,0:T(2,128)(2,1)S(1)}, u32[]{:S(2)}, u32[]{:S(2)}) async-start(bf16[128,2,256]{2,1,0:T(2,128)(2,1)} %reshape.79), calls=%async_computation.6 | async-start | bytes 262144 | tf_op jit(solution)/shard_map/all_to_all | solution.py:18
  135.6 12.7 %all-to-all-done.6 = bf16[128,2,256]{2,1,0:T(2,128)(2,1)S(1)} async-done(((bf16[128,2,256]{2,1,0:T(2,128)(2,1)}), bf16[128,2,256]{2,1,0:T(2,128)(2,1)S(1)}, u32[]{:S(2)}, u32[]{:S(2)}) %all-to-all-start.6) | async-done | bytes 131104 | tf_op jit(solution)/shard_map/all_to_all | solution.py:18
  148.5 0.7 fusion
  (45 shorter events, 2.5 us)
Async XLA Ops:
  0.6 41.2 %copy-start = (bf16[2048,64]{0,1:T(8,128)(2,1)S(1)}, bf16[2048,64]{0,1:T(8,128)(2,1)}, u32[]{:S(2)}) copy-start(bf16[2048,64]{0,1:T(8,128)(2,1)} %param.28) | copy-start | bytes 786436
  0.6 1.1 copy-start.2
  3.2 11.0 %copy-start.9 = (bf16[256,16]{0,1:T(8,128)(2,1)S(1)}, bf16[256,16]{0,1:T(8,128)(2,1)}, u32[]{:S(2)}) copy-start(bf16[256,16]{0,1:T(8,128)(2,1)} %param.31) | copy-start | bytes 24580
  3.2 11.0 %copy-start.10 = (bf16[16,256]{1,0:T(8,128)(2,1)S(1)}, bf16[16,256]{1,0:T(8,128)(2,1)}, u32[]{:S(2)}) copy-start(bf16[16,256]{1,0:T(8,128)(2,1)} %param.24) | copy-start | bytes 24580
  3.2 11.0 %copy-start.11 = (bf16[16,256]{1,0:T(8,128)(2,1)S(1)}, bf16[16,256]{1,0:T(8,128)(2,1)}, u32[]{:S(2)}) copy-start(bf16[16,256]{1,0:T(8,128)(2,1)} %param.23) | copy-start | bytes 24580
  3.2 11.0 %copy-start.12 = (bf16[16,256]{1,0:T(8,128)(2,1)S(1)}, bf16[16,256]{1,0:T(8,128)(2,1)}, u32[]{:S(2)}) copy-start(bf16[16,256]{1,0:T(8,128)(2,1)} %param.22) | copy-start | bytes 24580
  3.2 30.9 %all-to-all-start = ((bf16[8,16,256]{2,1,0:T(8,128)(2,1)}), bf16[8,16,256]{2,1,0:T(8,128)(2,1)S(1)}, u32[]{:S(2)}, u32[]{:S(2)}) async-start(bf16[8,16,256]{2,1,0:T(8,128)(2,1)} %copy.45), calls=%async_computation | async-start | bytes 131072 | tf_op jit(solution)/shard_map/all_to_all | solution.py:18
  34.0 17.6 %copy-start.1 = (f32[16,4,4096]{2,1,0:T(4,128)S(1)}, f32[16,4,4096]{2,1,0:T(4,128)}, u32[]{:S(2)}) copy-start(f32[16,4,4096]{2,1,0:T(4,128)} %param.20) | copy-start | bytes 3145732
  34.9 16.7 %all-to-all-start.1 = ((bf16[8,16,768]{2,1,0:T(8,128)(2,1)}), bf16[8,16,768]{2,1,0:T(8,128)(2,1)S(1)}, u32[]{:S(2)}, u32[]{:S(2)}) async-start(bf16[8,16,768]{2,1,0:T(8,128)(2,1)} %bitcast.4), calls=%async_computation.1 | async-start | bytes 393216 | tf_op jit(solution)/shard_map/all_to_all | solution.py:18
  41.9 1.1 copy-start.8
  41.9 1.1 copy-start.14
  51.6 0.7 copy-start.7
  64.8 5.5 %copy-start.15 = (s32[16,2]{0,1:T(2,128)S(1)}, s32[16,2]{0,1:T(2,128)}, u32[]{:S(2)}) copy-start(s32[16,2]{0,1:T(2,128)} %param.33) | copy-start | bytes 388
  65.5 15.3 %copy-start.6 = (f32[2048]{0:T(1024)S(1)}, f32[2048]{0:T(1024)}, u32[]{:S(2)}) copy-start(f32[2048]{0:T(1024)} %param.32) | copy-start | bytes 24580
  65.5 47.0 %copy-start.5 = (bf16[1,128,2048]{2,1,0:T(8,128)(2,1)S(1)}, bf16[1,128,2048]{2,1,0:T(8,128)(2,1)}, u32[]{:S(2)}) copy-start(bf16[1,128,2048]{2,1,0:T(8,128)(2,1)} %param.37) | copy-start | bytes 1572868
  65.5 15.3 %all-to-all-start.3 = ((bf16[32,16,256]{2,1,0:T(8,128)(2,1)}), bf16[32,16,256]{2,1,0:T(8,128)(2,1)S(1)}, u32[]{:S(2)}, u32[]{:S(2)}) async-start(bf16[32,16,256]{2,1,0:T(8,128)(2,1)} %bitcast.11), calls=%async_computation.3 | async-start | bytes 524288 | tf_op jit(solution)/shard_map/all_to_all | solution.py:18
  81.8 30.8 %copy-start.3 = (bf16[1,2048,128]{2,1,0:T(8,128)(2,1)S(1)}, bf16[1,2048,128]{2,1,0:T(8,128)(2,1)}, u32[]{:S(2)}) copy-start(bf16[1,2048,128]{2,1,0:T(8,128)(2,1)} %param.35) | copy-start | bytes 1572868
  81.8 30.8 %copy-start.4 = (bf16[1,2048,128]{2,1,0:T(8,128)(2,1)S(1)}, bf16[1,2048,128]{2,1,0:T(8,128)(2,1)}, u32[]{:S(2)}) copy-start(bf16[1,2048,128]{2,1,0:T(8,128)(2,1)} %param.36) | copy-start | bytes 1572868
  114.4 3.6 %copy-start.13 = (f32[16,2]{0,1:T(2,128)S(1)}, f32[16,2]{0,1:T(2,128)}, u32[]{:S(2)}) copy-start(f32[16,2]{0,1:T(2,128)} %param.34) | copy-start | bytes 388
  114.4 13.4 %all-to-all-start.5 = ((bf16[4,128,512]{2,1,0:T(8,128)(2,1)}), bf16[4,128,512]{2,1,0:T(8,128)(2,1)S(1)}, u32[]{:S(2)}, u32[]{:S(2)}) async-start(bf16[4,128,512]{2,1,0:T(8,128)(2,1)} %expert.1), calls=%async_computation.5 | async-start | bytes 1048576 | tf_op jit(solution)/shard_map/all_to_all | solution.py:18
  129.8 18.6 %all-to-all-start.6 = ((bf16[128,2,256]{2,1,0:T(2,128)(2,1)}), bf16[128,2,256]{2,1,0:T(2,128)(2,1)S(1)}, u32[]{:S(2)}, u32[]{:S(2)}) async-start(bf16[128,2,256]{2,1,0:T(2,128)(2,1)} %reshape.79), calls=%async_computation.6 | async-start | bytes 262144 | tf_op jit(solution)/shard_map/all_to_all | solution.py:18

commit v4 on v3

--- a/solution.py
+++ b/solution.py
@@ -11,17 +11,10 @@
 norm_eps = 1e-06
 group_eps = 0.00064
 EP = ("z", "y", "c")
-PLANE = ("y", "c")
 
 
 def swap(array, axis):
     return lax.all_to_all(array, axis, split_axis=0, concat_axis=0, tiled=True)
-
-
-def rms_scale(activity, gain):
-    widened = activity.astype(jnp.float32)
-    scaled = widened * lax.rsqrt(jnp.mean(widened * widened, axis=-1, keepdims=True) + norm_eps)
-    return (scaled * gain).astype(jnp.bfloat16)
 
 
 def low_rank(normed, decay_down, decay_up, decay_base, rate_down, rate_up):
@@ -45,6 +38,91 @@
     return jnp.dot(high, chooser, preferred_element_type=jnp.float32) + jnp.dot(
         low, chooser, preferred_element_type=jnp.float32
     )
+
+
+def prepare_kernel(tokens, gain, query, key, value, out, rows, normed, weights):
+    layers, _, block = rows.shape
+    f32 = jnp.float32
+    widened = tokens[...].astype(f32)
+    scale = lax.rsqrt(jnp.mean(widened * widened, axis=1, keepdims=True) + norm_eps)
+    scaled = (widened * scale * gain[...]).astype(jnp.bfloat16)
+    normed[...] = scaled
+    for z in range(layers):
+        rows[z] = scaled[:, z * block : (z + 1) * block]
+    joined = jnp.concatenate([query[...], key[...], value[...], out[...]], axis=1)
+    for y in range(weights.shape[0]):
+        weights[y] = joined
+
+
+def prepare(tokens, gain, pieces, layers, peers):
+    count, width = tokens.shape
+    bf16 = jnp.bfloat16
+    total = sum(piece.shape[1] for piece in pieces)
+    return pl.pallas_call(
+        prepare_kernel,
+        out_shape=(
+            jax.ShapeDtypeStruct((layers, count, width // layers), bf16),
+            jax.ShapeDtypeStruct((count, width), bf16),
+            jax.ShapeDtypeStruct((peers, pieces[0].shape[0], total), bf16),
+        ),
+        compiler_params=pltpu.CompilerParams(vmem_limit_bytes=20 << 20),
+        name="prepare",
+    )(tokens, gain.reshape(1, width), *pieces)
+
+
+def project_kernel(rows, weights, result, whole):
+    cores, peers, depth, _ = weights.shape
+    layers, count, cols = result.shape
+    for y in range(peers):
+        for c in range(cores):
+            start = (y * cores + c) * depth
+            whole[start : start + depth, :] = weights[c, y, :, :cols]
+    product = jnp.dot(
+        rows[...].reshape(layers * count, rows.shape[2]),
+        whole[...],
+        preferred_element_type=jnp.float32,
+    )
+    result[...] = product.astype(jnp.bfloat16).reshape(result.shape)
+
+
+def project(rows, weights, cols):
+    layers, count, block = rows.shape
+    return pl.pallas_call(
+        project_kernel,
+        out_shape=jax.ShapeDtypeStruct((layers, count, cols), jnp.bfloat16),
+        scratch_shapes=[pltpu.VMEM((block, cols), jnp.bfloat16)],
+        compiler_params=pltpu.CompilerParams(vmem_limit_bytes=20 << 20),
+        name="project",
+    )(rows, weights)
+
+
+def output_kernel(heads, weights, result, whole):
+    cores, peers, depth, total = weights.shape
+    layers, lanes, count, block = result.shape
+    cols = heads.shape[2]
+    for y in range(peers):
+        for c in range(cores):
+            start = (y * cores + c) * depth
+            whole[start : start + depth, :] = weights[c, y, :, total - cols :]
+    product = lax.dot_general(
+        heads[...].reshape(layers * count, cols),
+        whole[...],
+        (((1,), (1,)), ((), ())),
+        preferred_element_type=jnp.float32,
+    )
+    product = product.astype(jnp.bfloat16).reshape(layers, 1, count, block)
+    result[...] = jnp.broadcast_to(product, result.shape)
+
+
+def output(heads, weights, lanes, block):
+    layers, count, cols = heads.shape
+    return pl.pallas_call(
+        output_kernel,
+        out_shape=jax.ShapeDtypeStruct((layers, lanes, count, block), jnp.bfloat16),
+        scratch_shapes=[pltpu.VMEM((block, cols), jnp.bfloat16)],
+        compiler_params=pltpu.CompilerParams(vmem_limit_bytes=20 << 20),
+        name="output",
+    )(heads, weights)
 
 
 def recurrence_kernel(size, parts, decays, rates, gain, state, new_state, spread_out):
@@ -242,17 +320,13 @@
     block = width // layers
     quarter = width // lanes
 
-    weights = lax.all_gather(
-        jnp.concatenate([w_query, w_key, w_value, w_out.T], axis=1), PLANE, axis=0, tiled=True
-    )
-    normed = rms_scale(tokens, mixer_gain)
-    spread_rows = swap(normed.reshape(rows, layers, block).transpose(1, 0, 2), "z")
-    partial_rows = jnp.dot(
-        spread_rows.reshape(layers * rows, block),
-        weights[:, : 3 * cols],
-        preferred_element_type=jnp.float32,
-    ).astype(jnp.bfloat16)
-    summed = swap(partial_rows.reshape(layers, rows, 3 * cols), "z")
+    spread_rows, normed, own_weights = prepare(
+        tokens, mixer_gain, (w_query, w_key, w_value, w_out.T), layers, lax.axis_size("y")
+    )
+    own_weights = swap(own_weights, "y")
+    spread_rows = swap(spread_rows, "z")
+    weights = lax.all_gather(own_weights, "c", axis=0)
+    summed = swap(project(spread_rows, weights, 3 * cols), "z")
     decays, rates = low_rank(
         normed,
         decay_down,
@@ -262,19 +336,9 @@
         lax.dynamic_slice_in_dim(rate_up, lane * cols, cols, 1),
     )
     next_state, spread_out = recurrence(summed, decays, rates, head_state, head_gain)
-    heads_here = swap(spread_out, "z").reshape(layers * rows, cols)
-    partial_out = lax.dot_general(
-        heads_here,
-        weights[:, 3 * cols :],
-        (((1,), (1,)), ((), ())),
-        preferred_element_type=jnp.float32,
-    ).astype(jnp.bfloat16)
-    home_out = swap(
-        jnp.broadcast_to(
-            partial_out.reshape(layers, 1, rows, block), (layers, lanes, rows, block)
-        ).reshape(layers * lanes, rows, block),
-        ("z", "tp"),
-    ).reshape(layers, lanes, rows, block)
+    partial_out = output(swap(spread_out, "z"), weights, lanes, block)
+    home_out = swap(partial_out.reshape(layers * lanes, rows, block), ("z", "tp"))
+    home_out = home_out.reshape(layers, lanes, rows, block)
     match = expert_ids[:, :, None] == jnp.arange(experts, dtype=jnp.int32)[None, None, :]
     order = jnp.arange(rows, dtype=jnp.int32)[:, None, None]
     slots = jnp.min(jnp.where(match, order, rows), axis=(0, 1))

time: 150 us -> 154 us (1.027)
  blocking collectives: 60.3 us -> 45.9 us
  waiting for transfers between devices: 40.4 us -> 51.5 us
  starting transfers between devices: 32 us -> 36.7 us
  local copies, waits for them, and re-layouts: 3.43 us -> 6.41 us
  Pallas kernels: 5.43 us -> 8 us
  other arithmetic: 2.77 us -> 0.94 us
    all_gather x1, blocking collectives: 19.8 us -> 4.41 us  [body(): weights = lax.all_gather(own_weights, 'c', axis=0)]
    all_to_all x5 -> x6, waiting for transfers between devices: 40.4 us -> 51.5 us  [swap(): return lax.all_to_all(array, axis, split_axis=0, concat_axis=0, tiled=True)]
    all_to_all x5 -> x6, starting transfers between devices: 32 us -> 36.7 us  [swap(): return lax.all_to_all(array, axis, split_axis=0, concat_axis=0, tiled=True)]
    unnamed x35 -> x38, local copies, waits for them, and re-layouts: 1.54 us -> 5.89 us
    pallas_call x0 -> x3, Pallas kernels: none -> 2.56 us  [the longest x1 0.91 us: output(): pl.pallas_call(output_kernel, out_shape=jax.ShapeDtypeStruct((layers, lan...]
  transfers between devices with their start and end apart: 5 -> 6, of which waited for: 4 -> 6; matrix products, arithmetic and copies ran while one was open for 2% -> 2% of each run, Pallas kernels for 0% -> 0%
where the time goes in v4:
time: 154 us; the launch traced here: 153 us
  waiting for transfers between devices  51.5 us (33%)
  blocking collectives  45.9 us (30%)
  starting transfers between devices  36.7 us (24%)
  Pallas kernels  8 us (5%)
  local copies, waits for them, and re-layouts  6.41 us (4%)
  matrix products  2.95 us (2%)
    all_to_all x6, waiting for transfers between devices, swap(): return lax.all_to_all(array, axis, split_axis=0, concat_axis=0, tiled=True)  51.5 us
    all_to_all x2, blocking collectives, swap(): return lax.all_to_all(array, axis, split_axis=0, concat_axis=0, tiled=True)  41.5 us
    all_to_all x6, starting transfers between devices, swap(): return lax.all_to_all(array, axis, split_axis=0, concat_axis=0, tiled=True)  36.7 us
    unnamed x38, local copies, waits for them, and re-layouts  5.89 us
    all_gather x1, blocking collectives, body(): weights = lax.all_gather(own_weights, 'c', axis=0)  4.41 us
  transfers between devices with their start and end apart: 6, of which 6 were waited for; matrix products, arithmetic and copies ran while one was open for 2% of the time, Pallas kernels for 0%

profile of v4, /device:TPU:1, one launch (start us, length us, event | category | flops | bytes accessed | tf_op | source)
XLA Modules:
  0.0 153.3 jit_solution(7437340166519720597)
XLA Ops:
  0.7 0.9 copy-done.5
  5.0 0.8 prepare.1
  5.8 7.6 %all-to-all-start.1 = ((bf16[8,16,1024]{2,1,0:T(8,128)(2,1)}), bf16[8,16,1024]{2,1,0:T(8,128)(2,1)S(1)}, u32[]{:S(2)}, u32[]{:S(2)}) async-start(bf16[8,16,1024]{2,1,0:T(8,128)(2,1)} %get-tuple-element.10), calls=%async_computation.1 | async-start | bytes 524288 | tf_op jit(solution)/shard_map/all_to_all | solution.py:17
  13.4 9.4 %all-to-all-done.1 = bf16[8,16,1024]{2,1,0:T(8,128)(2,1)S(1)} async-done(((bf16[8,16,1024]{2,1,0:T(8,128)(2,1)}), bf16[8,16,1024]{2,1,0:T(8,128)(2,1)S(1)}, u32[]{:S(2)}, u32[]{:S(2)}) %all-to-all-start.1) | async-done | bytes 262176 | tf_op jit(solution)/shard_map/all_to_all | solution.py:17
  22.9 11.1 %all-to-all-start = ((bf16[8,16,256]{2,1,0:T(8,128)(2,1)}), bf16[8,16,256]{2,1,0:T(8,128)(2,1)S(1)}, u32[]{:S(2)}, u32[]{:S(2)}) async-start(bf16[8,16,256]{2,1,0:T(8,128)(2,1)} %get-tuple-element.9), calls=%async_computation | async-start | bytes 131072 | tf_op jit(solution)/shard_map/all_to_all | solution.py:17
  33.9 4.4 %all-gather = bf16[16,16,1024]{2,1,0:T(8,128)(2,1)S(1)} all-gather(bf16[8,16,1024]{2,1,0:T(8,128)(2,1)S(1)} %all-to-all-done.1), channel_id=2, replica_groups=mesh['z'=8,'y'=8,'c'=2,'tp'=4] {'c'}, dimensions={0}, use_global_device_ids=true | all-gather | bytes 786432 | tf_op jit(solution)/shard_map/all_gather | solution.py:328
  38.4 2.8 %all-to-all-done.rows = bf16[8,16,256]{2,1,0:T(8,128)(2,1)S(1)} async-done(((bf16[8,16,256]{2,1,0:T(8,128)(2,1)}), bf16[8,16,256]{2,1,0:T(8,128)(2,1)S(1)}, u32[]{:S(2)}, u32[]{:S(2)}) %all-to-all-start) | async-done | bytes 65568 | tf_op jit(solution)/shard_map/all_to_all | solution.py:17
  41.2 0.9 project.1
  42.1 4.1 %all-to-all-start.2 = ((bf16[8,16,768]{2,1,0:T(8,128)(2,1)}), bf16[8,16,768]{2,1,0:T(8,128)(2,1)S(1)}, u32[]{:S(2)}, u32[]{:S(2)}) async-start(bf16[8,16,768]{2,1,0:T(8,128)(2,1)} %project.1), calls=%async_computation.2 | async-start | bytes 393216 | tf_op jit(solution)/shard_map/all_to_all | solution.py:17
  46.2 1.1 fusion.3.rates
  47.3 1.1 fusion.14.decays
  48.5 6.5 %all-to-all-done.2.parts = bf16[8,16,768]{2,1,0:T(8,128)(2,1)S(1)} async-done(((bf16[8,16,768]{2,1,0:T(8,128)(2,1)}), bf16[8,16,768]{2,1,0:T(8,128)(2,1)S(1)}, u32[]{:S(2)}, u32[]{:S(2)}) %all-to-all-start.2) | async-done | bytes 196640 | tf_op jit(solution)/shard_map/all_to_all | solution.py:17
  55.6 2.6 %recurrence.1 = (f32[16,128,128]{2,1,0:T(8,128)}, bf16[8,16,256]{2,1,0:T(8,128)(2,1)S(1)}) custom-call(bf16[8,16,768]{2,1,0:T(8,128)(2,1)S(1)} %all-to-all-done.2.parts, f32[16,256]{1,0:T(8,128)S(1)} %fusion.14.decays, f32[16,256]{1,0:T(8,128)S(1)} %fusion.3.rates, f32[1,256]{1,0:T(1,128)S(1)} %bitcast.40, f32[16,128,128]{2,1,0:T(8,128)S(1)} %bitcast.32), custom_call_target="tpu_custom_call" | custom-call | tf_op jit(solution)/shard_map/recurrence/pallas_call | solution.py:194
  58.2 9.6 %all_to_all.40.heads = bf16[8,16,256]{2,1,0:T(8,128)(2,1)S(1)} all-to-all(bf16[8,16,256]{2,1,0:T(8,128)(2,1)S(1)} %get-tuple-element.12), channel_id=1, replica_groups=mesh['z'=8,'y'=8,'c'=2,'tp'=4] {'z'}, dimensions={0} | all-to-all | bytes 131072 | tf_op jit(solution)/shard_map/all_to_all | solution.py:17
  67.8 0.9 output.1
  68.7 4.5 %all-to-all-start.4 = ((bf16[32,16,256]{2,1,0:T(8,128)(2,1)}), bf16[32,16,256]{2,1,0:T(8,128)(2,1)S(1)}, u32[]{:S(2)}, u32[]{:S(2)}) async-start(bf16[32,16,256]{2,1,0:T(8,128)(2,1)} %bitcast.8), calls=%async_computation.4 | async-start | bytes 524288 | tf_op jit(solution)/shard_map/all_to_all | solution.py:17
  73.4 10.3 %all-to-all-done.4 = bf16[32,16,256]{2,1,0:T(8,128)(2,1)S(1)} async-done(((bf16[32,16,256]{2,1,0:T(8,128)(2,1)}), bf16[32,16,256]{2,1,0:T(8,128)(2,1)S(1)}, u32[]{:S(2)}, u32[]{:S(2)}) %all-to-all-start.4) | async-done | bytes 262176 | tf_op jit(solution)/shard_map/all_to_all | solution.py:17
  83.7 1.0 dispatch.1
  84.7 31.9 %all_to_all.41.rows = bf16[128,16,128]{2,1,0:T(8,128)(2,1)S(1)} all-to-all(bf16[128,16,128]{2,1,0:T(8,128)(2,1)S(1)} %get-tuple-element.14), channel_id=1, replica_groups=mesh['z'=8,'y'=8,'c'=2,'tp'=4] {'z','y','c'}, dimensions={0} | all-to-all | bytes 1048576 | tf_op jit(solution)/shard_map/all_to_all | solution.py:17
  116.6 1.9 %expert.1 = bf16[4,128,512]{2,1,0:T(8,128)(2,1)} custom-call(bf16[128,16,128]{2,1,0:T(8,128)(2,1)S(1)} %all_to_all.41.rows, bf16[2048,128]{1,0:T(8,128)(2,1)S(1)} %bitcast.34, bf16[2048,128]{1,0:T(8,128)(2,1)S(1)} %bitcast.35, bf16[128,2048]{1,0:T(8,128)(2,1)S(1)} %bitcast.36), custom_call_target="tpu_custom_call" | custom-call | tf_op jit(solution)/shard_map/expert/pallas_call | solution.py:282
  118.5 3.6 %all-to-all-start.6 = ((bf16[4,128,512]{2,1,0:T(8,128)(2,1)}), bf16[4,128,512]{2,1,0:T(8,128)(2,1)S(1)}, u32[]{:S(2)}, u32[]{:S(2)}) async-start(bf16[4,128,512]{2,1,0:T(8,128)(2,1)} %expert.1), calls=%async_computation.6 | async-start | bytes 1048576 | tf_op jit(solution)/shard_map/all_to_all | solution.py:17
  122.1 9.8 %all-to-all-done.6 = bf16[4,128,512]{2,1,0:T(8,128)(2,1)S(1)} async-done(((bf16[4,128,512]{2,1,0:T(8,128)(2,1)}), bf16[4,128,512]{2,1,0:T(8,128)(2,1)S(1)}, u32[]{:S(2)}, u32[]{:S(2)}) %all-to-all-start.6) | async-done | bytes 524320 | tf_op jit(solution)/shard_map/all_to_all | solution.py:17
  133.9 5.8 %all-to-all-start.7 = ((bf16[128,2,256]{2,1,0:T(2,128)(2,1)}), bf16[128,2,256]{2,1,0:T(2,128)(2,1)S(1)}, u32[]{:S(2)}, u32[]{:S(2)}) async-start(bf16[128,2,256]{2,1,0:T(2,128)(2,1)} %reshape.57), calls=%async_computation.7 | async-start | bytes 262144 | tf_op jit(solution)/shard_map/all_to_all | solution.py:17
  139.7 12.7 %all-to-all-done.7 = bf16[128,2,256]{2,1,0:T(2,128)(2,1)S(1)} async-done(((bf16[128,2,256]{2,1,0:T(2,128)(2,1)}), bf16[128,2,256]{2,1,0:T(2,128)(2,1)S(1)}, u32[]{:S(2)}, u32[]{:S(2)}) %all-to-all-start.7) | async-done | bytes 131104 | tf_op jit(solution)/shard_map/all_to_all | solution.py:17
  (45 shorter events, 7.2 us)
Async XLA Ops:
  0.6 45.6 %copy-start = (bf16[2048,64]{0,1:T(8,128)(2,1)S(1)}, bf16[2048,64]{0,1:T(8,128)(2,1)}, u32[]{:S(2)}) copy-start(bf16[2048,64]{0,1:T(8,128)(2,1)} %param.28) | copy-start | bytes 786436
  0.6 0.9 copy-start.5
  1.5 0.7 copy-start.7
  2.2 0.7 copy-start.8
  2.9 0.7 copy-start.9
  3.6 0.7 copy-start.10
  4.3 0.7 copy-start.11
  5.8 17.1 %all-to-all-start.1 = ((bf16[8,16,1024]{2,1,0:T(8,128)(2,1)}), bf16[8,16,1024]{2,1,0:T(8,128)(2,1)S(1)}, u32[]{:S(2)}, u32[]{:S(2)}) async-start(bf16[8,16,1024]{2,1,0:T(8,128)(2,1)} %get-tuple-element.10), calls=%async_computation.1 | async-start | bytes 524288 | tf_op jit(solution)/shard_map/all_to_all | solution.py:17
  22.9 18.4 %all-to-all-start = ((bf16[8,16,256]{2,1,0:T(8,128)(2,1)}), bf16[8,16,256]{2,1,0:T(8,128)(2,1)S(1)}, u32[]{:S(2)}, u32[]{:S(2)}) async-start(bf16[8,16,256]{2,1,0:T(8,128)(2,1)} %get-tuple-element.9), calls=%async_computation | async-start | bytes 131072 | tf_op jit(solution)/shard_map/all_to_all | solution.py:17
  38.4 16.6 %copy-start.1 = (f32[16,4,4096]{2,1,0:T(4,128)S(1)}, f32[16,4,4096]{2,1,0:T(4,128)}, u32[]{:S(2)}) copy-start(f32[16,4,4096]{2,1,0:T(4,128)} %param.20) | copy-start | bytes 3145732
  42.1 12.8 %all-to-all-start.2 = ((bf16[8,16,768]{2,1,0:T(8,128)(2,1)}), bf16[8,16,768]{2,1,0:T(8,128)(2,1)S(1)}, u32[]{:S(2)}, u32[]{:S(2)}) async-start(bf16[8,16,768]{2,1,0:T(8,128)(2,1)} %project.1), calls=%async_computation.2 | async-start | bytes 393216 | tf_op jit(solution)/shard_map/all_to_all | solution.py:17
  46.2 1.1 copy-start.14
  46.2 1.1 copy-start.16
  54.9 0.7 copy-start.13
  67.8 5.5 %copy-start.17 = (s32[16,2]{0,1:T(2,128)S(1)}, s32[16,2]{0,1:T(2,128)}, u32[]{:S(2)}) copy-start(s32[16,2]{0,1:T(2,128)} %param.33) | copy-start | bytes 388
  67.8 15.9 %copy-start.6 = (bf16[16,2048]{1,0:T(8,128)(2,1)S(1)}, bf16[16,2048]{1,0:T(8,128)(2,1)}, u32[]{:S(2)}) copy-start(bf16[16,2048]{1,0:T(8,128)(2,1)} %tokens.3) | copy-start | bytes 196612
  68.7 15.0 %copy-start.12 = (f32[2048]{0:T(1024)S(1)}, f32[2048]{0:T(1024)}, u32[]{:S(2)}) copy-start(f32[2048]{0:T(1024)} %param.32) | copy-start | bytes 24580
  68.7 47.9 %copy-start.4 = (bf16[1,128,2048]{2,1,0:T(8,128)(2,1)S(1)}, bf16[1,128,2048]{2,1,0:T(8,128)(2,1)}, u32[]{:S(2)}) copy-start(bf16[1,128,2048]{2,1,0:T(8,128)(2,1)} %param.37) | copy-start | bytes 1572868
  68.7 15.0 %all-to-all-start.4 = ((bf16[32,16,256]{2,1,0:T(8,128)(2,1)}), bf16[32,16,256]{2,1,0:T(8,128)(2,1)S(1)}, u32[]{:S(2)}, u32[]{:S(2)}) async-start(bf16[32,16,256]{2,1,0:T(8,128)(2,1)} %bitcast.8), calls=%async_computation.4 | async-start | bytes 524288 | tf_op jit(solution)/shard_map/all_to_all | solution.py:17
  84.7 31.9 %copy-start.2 = (bf16[1,2048,128]{2,1,0:T(8,128)(2,1)S(1)}, bf16[1,2048,128]{2,1,0:T(8,128)(2,1)}, u32[]{:S(2)}) copy-start(bf16[1,2048,128]{2,1,0:T(8,128)(2,1)} %param.35) | copy-start | bytes 1572868
  84.7 31.9 %copy-start.3 = (bf16[1,2048,128]{2,1,0:T(8,128)(2,1)S(1)}, bf16[1,2048,128]{2,1,0:T(8,128)(2,1)}, u32[]{:S(2)}) copy-start(bf16[1,2048,128]{2,1,0:T(8,128)(2,1)} %param.36) | copy-start | bytes 1572868
  118.5 3.6 %copy-start.15 = (f32[16,2]{0,1:T(2,128)S(1)}, f32[16,2]{0,1:T(2,128)}, u32[]{:S(2)}) copy-start(f32[16,2]{0,1:T(2,128)} %param.34) | copy-start | bytes 388
  118.5 13.4 %all-to-all-start.6 = ((bf16[4,128,512]{2,1,0:T(8,128)(2,1)}), bf16[4,128,512]{2,1,0:T(8,128)(2,1)S(1)}, u32[]{:S(2)}, u32[]{:S(2)}) async-start(bf16[4,128,512]{2,1,0:T(8,128)(2,1)} %expert.1), calls=%async_computation.6 | async-start | bytes 1048576 | tf_op jit(solution)/shard_map/all_to_all | solution.py:17
  133.9 18.6 %all-to-all-start.7 = ((bf16[128,2,256]{2,1,0:T(2,128)(2,1)}), bf16[128,2,256]{2,1,0:T(2,128)(2,1)S(1)}, u32[]{:S(2)}, u32[]{:S(2)}) async-start(bf16[128,2,256]{2,1,0:T(2,128)(2,1)} %reshape.57), calls=%async_computation.7 | async-start | bytes 262144 | tf_op jit(solution)/shard_map/all_to_all | solution.py:17

commit v5 on v3

--- a/solution.py
+++ b/solution.py
@@ -18,21 +18,69 @@
     return lax.all_to_all(array, axis, split_axis=0, concat_axis=0, tiled=True)
 
 
-def rms_scale(activity, gain):
-    widened = activity.astype(jnp.float32)
-    scaled = widened * lax.rsqrt(jnp.mean(widened * widened, axis=-1, keepdims=True) + norm_eps)
-    return (scaled * gain).astype(jnp.bfloat16)
-
-
-def low_rank(normed, decay_down, decay_up, decay_base, rate_down, rate_up):
-    decay_low = jnp.tanh(jnp.dot(normed, decay_down, preferred_element_type=jnp.float32)).astype(
-        jnp.bfloat16
-    )
-    decay_pre = decay_base + jnp.dot(decay_low, decay_up, preferred_element_type=jnp.float32)
-    decays = jnp.exp(-jnp.exp(-jax.nn.softplus(-decay_pre) - 0.5))
-    rate_low = jnp.dot(normed, rate_down, preferred_element_type=jnp.float32).astype(jnp.bfloat16)
-    rates = jax.nn.sigmoid(jnp.dot(rate_low, rate_up, preferred_element_type=jnp.float32))
-    return (decays, rates)
+def norm_kernel(tokens, gain, rows, normed):
+    layers, _, block = rows.shape
+    f32 = jnp.float32
+    widened = tokens[...].astype(f32)
+    scale = lax.rsqrt(jnp.mean(widened * widened, axis=1, keepdims=True) + norm_eps)
+    scaled = (widened * scale * gain[...]).astype(jnp.bfloat16)
+    normed[...] = scaled
+    for z in range(layers):
+        rows[z] = scaled[:, z * block : (z + 1) * block]
+
+
+def norm(tokens, gain, layers):
+    count, width = tokens.shape
+    bf16 = jnp.bfloat16
+    return pl.pallas_call(
+        norm_kernel,
+        out_shape=(
+            jax.ShapeDtypeStruct((layers, count, width // layers), bf16),
+            jax.ShapeDtypeStruct((count, width), bf16),
+        ),
+        compiler_params=pltpu.CompilerParams(vmem_limit_bytes=20 << 20),
+        name="norm",
+    )(tokens, gain.reshape(1, width))
+
+
+def low_rank_kernel(lane, normed, down, up, base, rate_down, rate_up, gain, result):
+    f32, bf16 = jnp.float32, jnp.bfloat16
+    _, count, cols = result.shape
+    own = pl.ds(pl.multiple_of(lane[0] * cols, cols), cols)
+    rows = normed[...]
+    across = lambda w: lax.dot_general(
+        rows, w[...], (((1,), (1,)), ((), ())), preferred_element_type=f32
+    )
+    decay_low = jnp.tanh(across(down)).astype(bf16)
+    decay_pre = base[...] + jnp.dot(decay_low, up[:, own], preferred_element_type=f32)
+    softplus = jnp.maximum(-decay_pre, 0.0) + jnp.log1p(jnp.exp(-jnp.abs(decay_pre)))
+    result[0] = jnp.exp(-jnp.exp(-softplus - 0.5))
+    rate_low = across(rate_down).astype(bf16)
+    rate_pre = jnp.dot(rate_low, rate_up[:, own], preferred_element_type=f32)
+    result[1] = 1.0 / (1.0 + jnp.exp(-rate_pre))
+    result[2] = jnp.broadcast_to(gain[...], (count, cols))
+
+
+def low_rank(normed, decay_down, decay_up, decay_base, rate_down, rate_up, head_gain, lane):
+    cols = decay_base.shape[0]
+    vmem = pl.BlockSpec(memory_space=pltpu.VMEM)
+    return pl.pallas_call(
+        low_rank_kernel,
+        in_specs=[pl.BlockSpec(memory_space=pltpu.SMEM)] + [vmem] * 7,
+        out_specs=vmem,
+        out_shape=jax.ShapeDtypeStruct((3, normed.shape[0], cols), jnp.float32),
+        compiler_params=pltpu.CompilerParams(vmem_limit_bytes=20 << 20),
+        name="low_rank",
+    )(
+        lane.reshape(1),
+        normed,
+        decay_down.T,
+        decay_up,
+        decay_base.reshape(1, cols),
+        rate_down.T,
+        rate_up,
+        head_gain.reshape(1, cols),
+    )
 
 
 def split_terms(value):
@@ -47,7 +95,8 @@
     )
 
 
-def recurrence_kernel(size, parts, decays, rates, gain, state, new_state, spread_out):
+def recurrence_kernel(size, parts, factors, state, new_state, spread_out):
+    decays, rates, gain = factors[0], factors[1], factors[2]
     count, cols = decays.shape
     heads = cols // size
     lines = state.shape[1]
@@ -64,7 +113,7 @@
     head_mean = head_sum * (1.0 / size)
     total = lambda x, m: jnp.dot(x, m, precision=lax.Precision.HIGHEST, preferred_element_type=f32)
     units = keys * lax.rsqrt(total(keys * keys, head_sum) + 1.0)
-    removal = units * rates[...]
+    removal = units * rates
 
     def by_line(x):
         copies = jnp.broadcast_to(x[:, None, :], (count, 2 * heads, cols))
@@ -92,7 +141,7 @@
     value_grid = jnp.dot(
         value_rows.reshape(count * lines, cols).astype(bf16), to_half, preferred_element_type=f32
     ).reshape(grid_shape)
-    updated = old * by_line(decays[...]) - removed * by_line(removal) + value_grid * by_line(keys)
+    updated = old * by_line(decays) - removed * by_line(removal) + value_grid * by_line(keys)
     new_state[...] = updated.reshape(new_state.shape)
     broad = (wide, cols)
     from_half = jnp.where(iota(broad, 0) // size == iota(broad, 1) % 2, 1.0, 0.0).astype(bf16)
@@ -100,13 +149,13 @@
     readout = jnp.sum(jnp.where(owner[None], reads.reshape(count, *pick), 0.0), axis=1)
     centred = readout - total(readout, head_mean)
     spread = total(centred * centred, head_mean)
-    scaled = (centred * lax.rsqrt(spread + group_eps) * gain[...]).astype(bf16)
+    scaled = (centred * lax.rsqrt(spread + group_eps) * gain).astype(bf16)
     spread_out[...] = jnp.broadcast_to(scaled[None], spread_out.shape)
 
 
-def recurrence(parts, decays, rates, old_state, head_gain):
+def recurrence(parts, factors, old_state):
     layers = parts.shape[0]
-    count, cols = decays.shape
+    _, count, cols = factors.shape
     heads, area = old_state.shape[1:]
     size = math.isqrt(area)
     wide = 2 * size
@@ -121,9 +170,33 @@
         ),
         compiler_params=pltpu.CompilerParams(vmem_limit_bytes=40 << 20),
         name="recurrence",
-    )(parts, decays, rates, head_gain.reshape(1, cols), state)
+    )(parts, factors, state)
     new_state = new_state.reshape(count, lines, heads, wide).transpose(0, 2, 1, 3)
     return new_state.reshape(old_state.shape), spread_out
+
+
+def output_kernel(heads, weights, result):
+    layers, lanes, count, block = result.shape
+    cols = heads.shape[2]
+    product = lax.dot_general(
+        heads[...].reshape(layers * count, cols),
+        weights[:, weights.shape[1] - cols :],
+        (((1,), (1,)), ((), ())),
+        preferred_element_type=jnp.float32,
+    )
+    product = product.astype(jnp.bfloat16).reshape(layers, 1, count, block)
+    result[...] = jnp.broadcast_to(product, result.shape)
+
+
+def output(heads, weights, lanes):
+    layers, count, _ = heads.shape
+    shape = (layers, lanes, count, weights.shape[0])
+    return pl.pallas_call(
+        output_kernel,
+        out_shape=jax.ShapeDtypeStruct(shape, jnp.bfloat16),
+        compiler_params=pltpu.CompilerParams(vmem_limit_bytes=20 << 20),
+        name="output",
+    )(heads, weights)
 
 
 def dispatch_kernel(slots, lane, parts, tokens, gain, outbound, kept, residual, lines, rows):
@@ -210,6 +283,58 @@
         compiler_params=pltpu.CompilerParams(vmem_limit_bytes=20 << 20),
         name="expert",
     )(rows, gate, up, down)
+
+
+def settle_kernel(parts, result, lines):
+    lanes, _, quarter = parts.shape
+    pieces, wide = lines.shape[1:]
+    total = parts[0].astype(jnp.float32)
+    for part in range(1, lanes):
+        total = total + parts[part].astype(jnp.float32)
+    for piece in range(pieces):
+        lines[:, piece, :] = total[:, piece * wide : (piece + 1) * wide]
+    result[...] = lines[...].astype(jnp.bfloat16)
+
+
+def settle(parts):
+    _, count, quarter = parts.shape
+    shape = (count, quarter // 128, 128)
+    return pl.pallas_call(
+        settle_kernel,
+        out_shape=jax.ShapeDtypeStruct(shape, jnp.bfloat16),
+        scratch_shapes=[pltpu.VMEM(shape, jnp.float32)],
+        compiler_params=pltpu.CompilerParams(vmem_limit_bytes=20 << 20),
+        name="settle",
+    )(parts)
+
+
+def combine_kernel(chosen, shares, returned, residual, result, lines):
+    count, pieces, wide = lines.shape
+    top = chosen.shape[0] // count
+    for row in range(count):
+        total = 0.0
+        for k in range(top):
+            place = row * top + k
+            total = total + shares[place] * returned[chosen[place]].astype(jnp.float32)
+        lines[row] = total
+    for piece in range(pieces):
+        here = slice(piece * wide, (piece + 1) * wide)
+        result[:, here] = (residual[:, here] + lines[:, piece, :]).astype(jnp.bfloat16)
+
+
+def combine(chosen, shares, returned, residual):
+    count, quarter = residual.shape
+    vmem = pl.BlockSpec(memory_space=pltpu.VMEM)
+    smem = pl.BlockSpec(memory_space=pltpu.SMEM)
+    return pl.pallas_call(
+        combine_kernel,
+        in_specs=[smem, smem, vmem, vmem],
+        out_specs=vmem,
+        out_shape=jax.ShapeDtypeStruct((count, quarter), jnp.bfloat16),
+        scratch_shapes=[pltpu.VMEM((count, *returned.shape[1:]), jnp.float32)],
+        compiler_params=pltpu.CompilerParams(vmem_limit_bytes=20 << 20),
+        name="combine",
+    )(chosen, shares, returned, residual)
 
 
 def body(
@@ -240,54 +365,38 @@
     experts = lax.axis_size(EP)
     lane = lax.axis_index("tp")
     block = width // layers
-    quarter = width // lanes
-
+
+    spread_rows, normed = norm(tokens, mixer_gain, layers)
+    spread_rows = swap(spread_rows, "z")
     weights = lax.all_gather(
         jnp.concatenate([w_query, w_key, w_value, w_out.T], axis=1), PLANE, axis=0, tiled=True
     )
-    normed = rms_scale(tokens, mixer_gain)
-    spread_rows = swap(normed.reshape(rows, layers, block).transpose(1, 0, 2), "z")
     partial_rows = jnp.dot(
         spread_rows.reshape(layers * rows, block),
         weights[:, : 3 * cols],
         preferred_element_type=jnp.float32,
     ).astype(jnp.bfloat16)
     summed = swap(partial_rows.reshape(layers, rows, 3 * cols), "z")
-    decays, rates = low_rank(
-        normed,
-        decay_down,
-        lax.dynamic_slice_in_dim(decay_up, lane * cols, cols, 1),
-        decay_base,
-        rate_down,
-        lax.dynamic_slice_in_dim(rate_up, lane * cols, cols, 1),
-    )
-    next_state, spread_out = recurrence(summed, decays, rates, head_state, head_gain)
-    heads_here = swap(spread_out, "z").reshape(layers * rows, cols)
-    partial_out = lax.dot_general(
-        heads_here,
-        weights[:, 3 * cols :],
-        (((1,), (1,)), ((), ())),
-        preferred_element_type=jnp.float32,
-    ).astype(jnp.bfloat16)
-    home_out = swap(
-        jnp.broadcast_to(
-            partial_out.reshape(layers, 1, rows, block), (layers, lanes, rows, block)
-        ).reshape(layers * lanes, rows, block),
-        ("z", "tp"),
-    ).reshape(layers, lanes, rows, block)
+    factors = low_rank(
+        normed, decay_down, decay_up, decay_base, rate_down, rate_up, head_gain, lane
+    )
     match = expert_ids[:, :, None] == jnp.arange(experts, dtype=jnp.int32)[None, None, :]
     order = jnp.arange(rows, dtype=jnp.int32)[:, None, None]
     slots = jnp.min(jnp.where(match, order, rows), axis=(0, 1))
+    shares = (route_weight / jnp.sum(route_weight, axis=1, keepdims=True)).reshape(-1)
+    chosen = expert_ids.reshape(-1)
+    summed, factors, slots, shares, chosen = lax.optimization_barrier(
+        (summed, factors, slots, shares, chosen)
+    )
+    next_state, spread_out = recurrence(summed, factors, head_state)
+    partial_out = output(swap(spread_out, "z"), weights, lanes)
+    home_out = swap(partial_out.reshape(layers * lanes, rows, block), ("z", "tp"))
+    home_out = home_out.reshape(layers, lanes, rows, block)
     outbound, residual = dispatch(home_out, tokens, expert_gain, slots, lane)
     arrived = swap(outbound, EP)
     expert_parts = expert_rows(arrived, w_gate[0], w_up[0], w_down[0], lanes)
-    gathered = swap(expert_parts, "tp")
-    reduced = jnp.sum(gathered.astype(jnp.float32), axis=0).astype(jnp.bfloat16)
-    returned = swap(reduced.reshape(experts, 1, quarter), EP).reshape(experts, quarter)
-    shares = route_weight / jnp.sum(route_weight, axis=1, keepdims=True)
-    combine = jnp.sum(match.astype(jnp.float32) * shares[:, :, None], axis=1)
-    routed = jnp.dot(combine, returned.astype(jnp.float32))
-    layer_out = (residual + routed).astype(jnp.bfloat16)
+    returned = swap(settle(swap(expert_parts, "tp")), EP)
+    layer_out = combine(chosen, shares, returned, residual)
     return (layer_out, next_state)
 
 

time: 150 us -> 144 us (0.960)
  blocking collectives: 60.3 us -> 106 us
  waiting for transfers between devices: 40.4 us -> 8.58 us
  starting transfers between devices: 32 us -> 17.9 us
  matrix products: 4.04 us -> 0.9 us
  other arithmetic: 2.77 us -> 0.12 us
  Pallas kernels: 5.43 us -> 7.7 us
    all_to_all x2 -> x5, blocking collectives: 40.4 us -> 85.7 us  [swap(): return lax.all_to_all(array, axis, split_axis=0, concat_axis=0, tiled=True)]
    all_to_all x5 -> x2, waiting for transfers between devices: 40.4 us -> 8.58 us  [swap(): return lax.all_to_all(array, axis, split_axis=0, concat_axis=0, tiled=True)]
    all_to_all x5 -> x2, starting transfers between devices: 32 us -> 17.9 us  [swap(): return lax.all_to_all(array, axis, split_axis=0, concat_axis=0, tiled=True)]
    dot_general x4 -> x0, matrix products: 3.14 us -> none  [the longest x1 1.11 us: low_rank(): jnp.dot(rate_low, rate_up, preferred_element_type=jnp.float32)]
    pallas_call x0 -> x5, Pallas kernels: none -> 3.06 us  [the longest x1 1.21 us: combine(): pl.pallas_call(combine_kernel, in_specs=[smem, smem, vmem, vmem], out_spe...]
  transfers between devices with their start and end apart: 5 -> 2, of which waited for: 4 -> 1; matrix products, arithmetic and copies ran while one was open for 2% -> 0% of each run, Pallas kernels for 0% -> 0%
where the time goes in v5:
time: 144 us
  blocking collectives  106 us (74%)
  starting transfers between devices  17.9 us (12%)
  waiting for transfers between devices  8.58 us (6%)
  Pallas kernels  7.7 us (5%)
  local copies, waits for them, and re-layouts  1.97 us (1%)
    all_to_all x5, blocking collectives, swap(): return lax.all_to_all(array, axis, split_axis=0, concat_axis=0, tiled=True)  85.7 us
    all_gather x1, blocking collectives, body(): lax.all_gather(jnp.concatenate([w_query, w_key, w_value, w_out.T], axis=1...  19.9 us
    all_to_all x2, starting transfers between devices, swap(): return lax.all_to_all(array, axis, split_axis=0, concat_axis=0, tiled=True)  17.9 us
    all_to_all x2, waiting for transfers between devices, swap(): return lax.all_to_all(array, axis, split_axis=0, concat_axis=0, tiled=True)  8.58 us
  transfers between devices with their start and end apart: 2, of which 1 were waited for; matrix products, arithmetic and copies ran while one was open for 0% of the time, Pallas kernels for 0%

profile of v5, /device:TPU:1, one launch (start us, length us, event | category | flops | bytes accessed | tf_op | source)
XLA Modules:
  0.0 143.7 jit_solution(14886935467418078031)
XLA Ops:
  0.6 0.8 copy-done.6
  1.5 0.7 copy-done.10
  2.2 0.7 norm.1
  2.9 11.0 %all-to-all-start = ((bf16[8,16,256]{2,1,0:T(8,128)(2,1)}), bf16[8,16,256]{2,1,0:T(8,128)(2,1)S(1)}, u32[]{:S(2)}, u32[]{:S(2)}) async-start(bf16[8,16,256]{2,1,0:T(8,128)(2,1)} %get-tuple-element.13), calls=%async_computation | async-start | bytes 131072 | tf_op jit(solution)/shard_map/all_to_all | solution.py:18
  14.1 19.9 %all_gather.3.weights = bf16[256,1024]{1,0:T(8,128)(2,1)S(1)} all-gather(bf16[16,1024]{1,0:T(8,128)(2,1)S(1)} %pad_maximum_fusion), channel_id=1, replica_groups=mesh['z'=8,'y'=8,'c'=2,'tp'=4] {'y','c'}, dimensions={0}, use_global_device_ids=true | all-gather | bytes 557056 | tf_op jit(solution)/shard_map/all_gather | solution.py:371
  34.0 0.9 convolution_convert_fusion
  34.9 6.9 %all-to-all-start.1 = ((bf16[8,16,768]{2,1,0:T(8,128)(2,1)}), bf16[8,16,768]{2,1,0:T(8,128)(2,1)S(1)}, u32[]{:S(2)}, u32[]{:S(2)}) async-start(bf16[8,16,768]{2,1,0:T(8,128)(2,1)} %bitcast.3), calls=%async_computation.1 | async-start | bytes 393216 | tf_op jit(solution)/shard_map/all_to_all | solution.py:18
  41.9 0.1 copy.31
  42.0 0.1 reshape.58.shares
  42.1 0.1 reshape.59.chosen
  42.3 0.6 low_rank.1.factors
  42.9 0.1 select_reduce_fusion.slots
  43.0 8.6 %all-to-all-done.1.parts = bf16[8,16,768]{2,1,0:T(8,128)(2,1)S(1)} async-done(((bf16[8,16,768]{2,1,0:T(8,128)(2,1)}), bf16[8,16,768]{2,1,0:T(8,128)(2,1)S(1)}, u32[]{:S(2)}, u32[]{:S(2)}) %all-to-all-start.1) | async-done | bytes 196640 | tf_op jit(solution)/shard_map/all_to_all | solution.py:18
  51.6 2.6 %recurrence.1 = (f32[16,128,128]{2,1,0:T(8,128)}, bf16[8,16,256]{2,1,0:T(8,128)(2,1)S(1)}) custom-call(bf16[8,16,768]{2,1,0:T(8,128)(2,1)S(1)} %all-to-all-done.1.parts, f32[3,16,256]{2,1,0:T(8,128)S(1)} %low_rank.1.factors, f32[16,128,128]{2,1,0:T(8,128)S(1)} %bitcast.26), custom_call_target="tpu_custom_call" | custom-call | tf_op jit(solution)/shard_map/recurrence/pallas_call | solution.py:165
  54.2 9.7 %all_to_all.35.heads = bf16[8,16,256]{2,1,0:T(8,128)(2,1)S(1)} all-to-all(bf16[8,16,256]{2,1,0:T(8,128)(2,1)S(1)} %get-tuple-element.20), channel_id=1, replica_groups=mesh['z'=8,'y'=8,'c'=2,'tp'=4] {'z'}, dimensions={0} | all-to-all | bytes 131072 | tf_op jit(solution)/shard_map/all_to_all | solution.py:18
  63.9 0.2 output.1
  64.1 15.1 %all_to_all.36 = bf16[32,16,256]{2,1,0:T(8,128)(2,1)S(1)} all-to-all(bf16[32,16,256]{2,1,0:T(8,128)(2,1)S(1)} %bitcast.28), channel_id=1, replica_groups=mesh['z'=8,'y'=8,'c'=2,'tp'=4] {'z','tp'}, dimensions={0} | all-to-all | bytes 524288 | tf_op jit(solution)/shard_map/all_to_all | solution.py:18
  79.2 1.0 dispatch.1
  80.2 30.8 %all_to_all.37.rows = bf16[128,16,128]{2,1,0:T(8,128)(2,1)S(1)} all-to-all(bf16[128,16,128]{2,1,0:T(8,128)(2,1)S(1)} %get-tuple-element.21), channel_id=1, replica_groups=mesh['z'=8,'y'=8,'c'=2,'tp'=4] {'z','y','c'}, dimensions={0} | all-to-all | bytes 1048576 | tf_op jit(solution)/shard_map/all_to_all | solution.py:18
  111.0 1.1 expert.1
  112.0 12.2 %all_to_all.38.parts = bf16[4,128,512]{2,1,0:T(8,128)(2,1)S(1)} all-to-all(bf16[4,128,512]{2,1,0:T(8,128)(2,1)S(1)} %expert.1), channel_id=1, replica_groups=mesh['z'=8,'y'=8,'c'=2,'tp'=4] {'tp'}, dimensions={0} | all-to-all | bytes 1048576 | tf_op jit(solution)/shard_map/all_to_all | solution.py:18
  124.3 0.3 settle.1
  124.5 17.9 %all_to_all.39.returned = bf16[128,4,128]{2,1,0:T(4,128)(2,1)S(1)} all-to-all(bf16[128,4,128]{2,1,0:T(4,128)(2,1)S(1)} %settle.1), channel_id=1, replica_groups=mesh['z'=8,'y'=8,'c'=2,'tp'=4] {'z','y','c'}, dimensions={0} | all-to-all | bytes 262144 | tf_op jit(solution)/shard_map/all_to_all | solution.py:18
  142.5 1.2 combine.1
  (43 shorter events, 0.2 us)
Async XLA Ops:
  0.6 0.8 copy-start.6
  1.5 0.7 copy-start.10
  2.9 11.0 %copy-start.14 = (bf16[256,16]{0,1:T(8,128)(2,1)S(1)}, bf16[256,16]{0,1:T(8,128)(2,1)}, u32[]{:S(2)}) copy-start(bf16[256,16]{0,1:T(8,128)(2,1)} %param.31) | copy-start | bytes 24580
  2.9 11.0 %copy-start.15 = (bf16[16,256]{1,0:T(8,128)(2,1)S(1)}, bf16[16,256]{1,0:T(8,128)(2,1)}, u32[]{:S(2)}) copy-start(bf16[16,256]{1,0:T(8,128)(2,1)} %param.24) | copy-start | bytes 24580
  2.9 11.0 %copy-start.16 = (bf16[16,256]{1,0:T(8,128)(2,1)S(1)}, bf16[16,256]{1,0:T(8,128)(2,1)}, u32[]{:S(2)}) copy-start(bf16[16,256]{1,0:T(8,128)(2,1)} %param.23) | copy-start | bytes 24580
  2.9 11.0 %copy-start.17 = (bf16[16,256]{1,0:T(8,128)(2,1)S(1)}, bf16[16,256]{1,0:T(8,128)(2,1)}, u32[]{:S(2)}) copy-start(bf16[16,256]{1,0:T(8,128)(2,1)} %param.22) | copy-start | bytes 24580
  2.9 31.1 %all-to-all-start = ((bf16[8,16,256]{2,1,0:T(8,128)(2,1)}), bf16[8,16,256]{2,1,0:T(8,128)(2,1)S(1)}, u32[]{:S(2)}, u32[]{:S(2)}) async-start(bf16[8,16,256]{2,1,0:T(8,128)(2,1)} %get-tuple-element.13), calls=%async_computation | async-start | bytes 131072 | tf_op jit(solution)/shard_map/all_to_all | solution.py:18
  14.0 27.9 %copy-start.18 = (f32[16,2]{0,1:T(2,128)S(1)}, f32[16,2]{0,1:T(2,128)}, u32[]{:S(2)}) copy-start(f32[16,2]{0,1:T(2,128)} %param.34) | copy-start | bytes 388
  14.0 28.1 %copy-start.19 = (s32[16,2]{0,1:T(2,128)S(1)}, s32[16,2]{0,1:T(2,128)}, u32[]{:S(2)}) copy-start(s32[16,2]{0,1:T(2,128)} %param.33) | copy-start | bytes 388
  14.0 28.2 %copy-start.4 = (bf16[2048,64]{0,1:T(8,128)(2,1)S(1)}, bf16[2048,64]{0,1:T(8,128)(2,1)}, u32[]{:S(2)}) copy-start(bf16[2048,64]{0,1:T(8,128)(2,1)} %param.25) | copy-start | bytes 786436
  14.0 28.2 %copy-start.5 = (bf16[2048,64]{0,1:T(8,128)(2,1)S(1)}, bf16[2048,64]{0,1:T(8,128)(2,1)}, u32[]{:S(2)}) copy-start(bf16[2048,64]{0,1:T(8,128)(2,1)} %param.28) | copy-start | bytes 786436
  14.0 28.2 %copy-start.8 = (bf16[64,1024]{1,0:T(8,128)(2,1)S(1)}, bf16[64,1024]{1,0:T(8,128)(2,1)}, u32[]{:S(2)}) copy-start(bf16[64,1024]{1,0:T(8,128)(2,1)} %up.1) | copy-start | bytes 393220
  14.0 28.2 %copy-start.9 = (bf16[64,1024]{1,0:T(8,128)(2,1)S(1)}, bf16[64,1024]{1,0:T(8,128)(2,1)}, u32[]{:S(2)}) copy-start(bf16[64,1024]{1,0:T(8,128)(2,1)} %rate_up.1) | copy-start | bytes 393220
  14.0 28.2 %copy-start.12 = (f32[256]{0:T(256)S(1)}, f32[256]{0:T(256)}, u32[]{:S(2)}) copy-start(f32[256]{0:T(256)} %param.27) | copy-start | bytes 3076
  14.1 28.2 %copy-start.13 = (f32[256]{0:T(256)S(1)}, f32[256]{0:T(256)}, u32[]{:S(2)}) copy-start(f32[256]{0:T(256)} %param.30) | copy-start | bytes 3076
  34.0 17.6 %copy-start = (f32[16,4,4096]{2,1,0:T(4,128)S(1)}, f32[16,4,4096]{2,1,0:T(4,128)}, u32[]{:S(2)}) copy-start(f32[16,4,4096]{2,1,0:T(4,128)} %param.20) | copy-start | bytes 3145732
  34.9 16.7 %all-to-all-start.1 = ((bf16[8,16,768]{2,1,0:T(8,128)(2,1)}), bf16[8,16,768]{2,1,0:T(8,128)(2,1)S(1)}, u32[]{:S(2)}, u32[]{:S(2)}) async-start(bf16[8,16,768]{2,1,0:T(8,128)(2,1)} %bitcast.3), calls=%async_computation.1 | async-start | bytes 393216 | tf_op jit(solution)/shard_map/all_to_all | solution.py:18
  63.9 15.3 %copy-start.7 = (bf16[16,2048]{1,0:T(8,128)(2,1)S(1)}, bf16[16,2048]{1,0:T(8,128)(2,1)}, u32[]{:S(2)}) copy-start(bf16[16,2048]{1,0:T(8,128)(2,1)} %tokens.3) | copy-start | bytes 196612
  63.9 15.3 %copy-start.11 = (f32[2048]{0:T(1024)S(1)}, f32[2048]{0:T(1024)}, u32[]{:S(2)}) copy-start(f32[2048]{0:T(1024)} %param.32) | copy-start | bytes 24580
  64.1 46.9 %copy-start.3 = (bf16[1,128,2048]{2,1,0:T(8,128)(2,1)S(1)}, bf16[1,128,2048]{2,1,0:T(8,128)(2,1)}, u32[]{:S(2)}) copy-start(bf16[1,128,2048]{2,1,0:T(8,128)(2,1)} %param.37) | copy-start | bytes 1572868
  80.2 30.8 %copy-start.1 = (bf16[1,2048,128]{2,1,0:T(8,128)(2,1)S(1)}, bf16[1,2048,128]{2,1,0:T(8,128)(2,1)}, u32[]{:S(2)}) copy-start(bf16[1,2048,128]{2,1,0:T(8,128)(2,1)} %param.35) | copy-start | bytes 1572868
  80.2 30.8 %copy-start.2 = (bf16[1,2048,128]{2,1,0:T(8,128)(2,1)S(1)}, bf16[1,2048,128]{2,1,0:T(8,128)(2,1)}, u32[]{:S(2)}) copy-start(bf16[1,2048,128]{2,1,0:T(8,128)(2,1)} %param.36) | copy-start | bytes 1572868

commit v6 on v5

--- a/solution.py
+++ b/solution.py
@@ -18,29 +18,82 @@
     return lax.all_to_all(array, axis, split_axis=0, concat_axis=0, tiled=True)
 
 
-def norm_kernel(tokens, gain, rows, normed):
-    layers, _, block = rows.shape
-    f32 = jnp.float32
+def norm_kernel(experts, tokens_in, gain_in, ids_in, rows, normed, tokens, gain, ids, done):
+    layers, depth, block = rows.shape
+    count = tokens.shape[0]
+    f32, bf16 = jnp.float32, jnp.bfloat16
+    sources = (tokens_in, gain_in, ids_in)
+    copies = [
+        pltpu.make_async_copy(source, target, done.at[k])
+        for k, (source, target) in enumerate(zip(sources, (tokens, gain, ids)))
+    ]
+    for copy in copies:
+        copy.start()
+    for copy in copies:
+        copy.wait()
     widened = tokens[...].astype(f32)
     scale = lax.rsqrt(jnp.mean(widened * widened, axis=1, keepdims=True) + norm_eps)
-    scaled = (widened * scale * gain[...]).astype(jnp.bfloat16)
+    scaled = (widened * scale * gain[...]).astype(bf16)
     normed[...] = scaled
+    table_shape = (experts, count)
+    row = lax.broadcasted_iota(jnp.int32, table_shape, 0)
+    named = row == ids[0:1, :]
+    for k in range(1, ids.shape[0]):
+        named = named | (row == ids[k : k + 1, :])
+    offsets = lax.broadcasted_iota(jnp.int32, (8, count), 1) - count
+    table = count + lax.dot_general(
+        offsets.astype(f32).astype(bf16),
+        jnp.where(named, 1.0, 0.0).astype(bf16),
+        (((1,), (1,)), ((), ())),
+        preferred_element_type=f32,
+    )
+    table = jnp.concatenate([table, table], axis=0).astype(bf16)
     for z in range(layers):
-        rows[z] = scaled[:, z * block : (z + 1) * block]
-
-
-def norm(tokens, gain, layers):
+        here = slice(z * block, (z + 1) * block)
+        rows[z, :count] = scaled[:, here]
+        rows[z, count : 2 * count] = tokens[:, here]
+        rows[z, 2 * count :, :experts] = table
+
+
+def norm(tokens, gain, expert_ids, layers, experts):
     count, width = tokens.shape
     bf16 = jnp.bfloat16
-    return pl.pallas_call(
-        norm_kernel,
+    top = expert_ids.shape[1]
+    return pl.pallas_call(
+        functools.partial(norm_kernel, experts),
+        in_specs=[pl.BlockSpec(memory_space=pltpu.HBM)] * 3,
         out_shape=(
-            jax.ShapeDtypeStruct((layers, count, width // layers), bf16),
+            jax.ShapeDtypeStruct((layers, 3 * count, width // layers), bf16),
             jax.ShapeDtypeStruct((count, width), bf16),
         ),
+        scratch_shapes=[
+            pltpu.VMEM((count, width), bf16),
+            pltpu.VMEM((1, width), jnp.float32),
+            pltpu.VMEM((top, count), jnp.int32),
+            pltpu.SemaphoreType.DMA((3,)),
+        ],
         compiler_params=pltpu.CompilerParams(vmem_limit_bytes=20 << 20),
         name="norm",
-    )(tokens, gain.reshape(1, width))
+    )(tokens, gain.reshape(1, width), expert_ids.T)
+
+
+def project_kernel(rows, weights, result):
+    layers, count, cols = result.shape
+    product = jnp.dot(
+        rows[:, :count, :].reshape(layers * count, rows.shape[2]),
+        weights[:, :cols],
+        preferred_element_type=jnp.float32,
+    )
+    result[...] = product.astype(jnp.bfloat16).reshape(result.shape)
+
+
+def project(rows, weights, count, cols):
+    return pl.pallas_call(
+        project_kernel,
+        out_shape=jax.ShapeDtypeStruct((rows.shape[0], count, cols), jnp.bfloat16),
+        compiler_params=pltpu.CompilerParams(vmem_limit_bytes=20 << 20),
+        name="project",
+    )(rows, weights)
 
 
 def low_rank_kernel(lane, normed, down, up, base, rate_down, rate_up, gain, result):
@@ -176,21 +229,19 @@
 
 
 def output_kernel(heads, weights, result):
-    layers, lanes, count, block = result.shape
-    cols = heads.shape[2]
+    layers, count, cols = heads.shape
     product = lax.dot_general(
         heads[...].reshape(layers * count, cols),
         weights[:, weights.shape[1] - cols :],
         (((1,), (1,)), ((), ())),
         preferred_element_type=jnp.float32,
     )
-    product = product.astype(jnp.bfloat16).reshape(layers, 1, count, block)
-    result[...] = jnp.broadcast_to(product, result.shape)
+    result[...] = product.astype(jnp.bfloat16).reshape(result.shape)
 
 
 def output(heads, weights, lanes):
     layers, count, _ = heads.shape
-    shape = (layers, lanes, count, weights.shape[0])
+    shape = (lanes, layers * count // lanes, weights.shape[0])
     return pl.pallas_call(
         output_kernel,
         out_shape=jax.ShapeDtypeStruct(shape, jnp.bfloat16),
@@ -199,73 +250,93 @@
     )(heads, weights)
 
 
-def dispatch_kernel(slots, lane, parts, tokens, gain, outbound, kept, residual, lines, rows):
-    layers, lanes, count, block = parts.shape
-    wide = lines.shape[2]
-    f32 = jnp.float32
-    squares = jnp.zeros((count, 1), f32)
-    for z in range(layers):
-        mixed = parts[z, 0].astype(f32)
-        for part in range(1, lanes):
-            mixed = mixed + parts[z, part].astype(f32)
-        here = tokens[:, z * block : (z + 1) * block].astype(f32)
-        residual[z] = (here + mixed).astype(jnp.bfloat16).astype(f32)
-        squares = squares + jnp.sum(residual[z] * residual[z], axis=1, keepdims=True)
-    scale = lax.rsqrt(squares / (layers * block) + norm_eps)
-    for z in range(layers):
-        normed = residual[z] * scale * gain[:, z * block : (z + 1) * block]
-        for piece in range(block // wide):
-            lines[:count, z * (block // wide) + piece, :] = normed[:, piece * wide : (piece + 1) * wide]
-    lines[count] = jnp.zeros(lines.shape[1:], f32)
-    rows[...] = lines[...].astype(jnp.bfloat16)
-
-    def send(step, carry):
-        outbound[step] = rows[slots[step]]
+def dispatch_kernel(slots, lane, parts, rows, outbound, residual, lines):
+    lanes, some, block = parts.shape
+    own = rows.shape[0] // lanes
+    count = some // own
+    experts, _, wide = lines.shape
+    pieces = block // wide
+    f32, bf16 = jnp.float32, jnp.bfloat16
+    mixed = parts[0].astype(f32)
+    for part in range(1, lanes):
+        mixed = mixed + parts[part].astype(f32)
+    for k in range(own):
+        here = rows[lane[0] * own + k, count : 2 * count, :].astype(f32)
+        total = (here + mixed[k * count : (k + 1) * count]).astype(bf16).astype(f32)
+        base = k * (count + 1)
+        for piece in range(pieces):
+            residual[base : base + count, piece, :] = total[:, piece * wide : (piece + 1) * wide]
+        residual[base + count] = jnp.zeros((pieces, wide), f32)
+
+    def send(expert, carry):
+        for k in range(own):
+            slot = slots[k * experts + expert] + k * (count + 1)
+            lines[expert, k * pieces : (k + 1) * pieces, :] = residual[slot]
         return carry
 
-    lax.fori_loop(0, outbound.shape[0], send, 0, unroll=8)
-    own = layers // lanes
-    for piece in range(own):
-        kept[:, piece * block : (piece + 1) * block] = residual[lane[0] * own + piece]
-
-
-def dispatch(parts, tokens, gain, slots, lane):
-    layers, lanes, count, block = parts.shape
-    width = layers * block
+    lax.fori_loop(0, experts, send, 0, unroll=8)
+    outbound[...] = lines[...].astype(bf16)
+
+
+def dispatch(parts, rows, slots, lane, experts):
+    lanes, some, block = parts.shape
+    own = rows.shape[0] // lanes
     wide = 128
-    pieces = width // wide
+    pieces = block // wide
     vmem = pl.BlockSpec(memory_space=pltpu.VMEM)
     smem = pl.BlockSpec(memory_space=pltpu.SMEM)
+    shape = (experts, own * pieces, wide)
     return pl.pallas_call(
         dispatch_kernel,
-        in_specs=[smem, smem, vmem, vmem, vmem],
-        out_specs=(vmem, vmem),
-        out_shape=(
-            jax.ShapeDtypeStruct((slots.shape[0], pieces, wide), jnp.bfloat16),
-            jax.ShapeDtypeStruct((count, width // lanes), jnp.float32),
-        ),
+        in_specs=[smem, smem, vmem, vmem],
+        out_specs=vmem,
+        out_shape=jax.ShapeDtypeStruct(shape, jnp.bfloat16),
         scratch_shapes=[
-            pltpu.VMEM((layers, count, block), jnp.float32),
-            pltpu.VMEM((count + 1, pieces, wide), jnp.float32),
-            pltpu.VMEM((count + 1, pieces, wide), jnp.bfloat16),
+            pltpu.VMEM((own + some, pieces, wide), jnp.float32),
+            pltpu.VMEM(shape, jnp.float32),
         ],
         compiler_params=pltpu.CompilerParams(vmem_limit_bytes=20 << 20),
         name="dispatch",
-    )(slots, lane.reshape(1), parts, tokens, gain.reshape(1, width))
-
-
-def expert_kernel(rows, gate, up, down, result, lines):
-    _, pieces, wide = rows.shape
-    lanes, _, quarter = result.shape
+    )(slots, lane.reshape(1), parts, rows)
+
+
+def assemble_kernel(layers, arrived, result, lines):
+    lanes, some, width = result.shape
+    peers = arrived.shape[0] // layers
+    wide = arrived.shape[2]
+    own = some // peers
+    pieces = arrived.shape[1] // own
+    lines[...] = arrived[...].astype(jnp.float32)
+    for k in range(own):
+        for z in range(layers):
+            for piece in range(pieces):
+                start = (z * pieces + piece) * wide
+                block = lines[z * peers : (z + 1) * peers, k * pieces + piece, :]
+                block = block.astype(jnp.bfloat16)
+                for part in range(lanes):
+                    result[part, k * peers : (k + 1) * peers, start : start + wide] = block
+
+
+def assemble(arrived, layers, lanes, width):
+    some = arrived.shape[0] // lanes
+    return pl.pallas_call(
+        functools.partial(assemble_kernel, layers),
+        out_shape=jax.ShapeDtypeStruct((lanes, some, width), jnp.bfloat16),
+        scratch_shapes=[pltpu.VMEM(arrived.shape, jnp.float32)],
+        compiler_params=pltpu.CompilerParams(vmem_limit_bytes=20 << 20),
+        name="assemble",
+    )(arrived)
+
+
+def expert_kernel(rows, gain, gate, up, down, result):
+    lanes, count, quarter = result.shape
+    width = rows.shape[2]
     f32 = jnp.float32
-    lines[...] = rows[...].astype(f32)
-    gate_act = up_act = 0.0
-    for piece in range(0, pieces, 2):
-        here = slice(piece * wide, (piece + 2) * wide)
-        both = jnp.concatenate([lines[:, piece, :], lines[:, piece + 1, :]], axis=1)
-        both = both.astype(jnp.bfloat16)
-        gate_act = gate_act + jnp.dot(both, gate[here], preferred_element_type=f32)
-        up_act = up_act + jnp.dot(both, up[here], preferred_element_type=f32)
+    widened = rows[...].astype(f32).reshape(count, width)
+    scale = lax.rsqrt(jnp.mean(widened * widened, axis=1, keepdims=True) + norm_eps)
+    normed = (widened * scale * gain[...]).astype(jnp.bfloat16)
+    gate_act = jnp.dot(normed, gate[...], preferred_element_type=f32)
+    up_act = jnp.dot(normed, up[...], preferred_element_type=f32)
     hidden = (gate_act / (1.0 + jnp.exp(-gate_act)) * up_act).astype(jnp.bfloat16)
     for part in range(lanes):
         here = slice(part * quarter, (part + 1) * quarter)
@@ -273,42 +344,44 @@
         result[part] = product.astype(jnp.bfloat16)
 
 
-def expert_rows(rows, gate, up, down, lanes):
+def expert_rows(rows, gain, gate, up, down):
+    lanes, some, width = rows.shape
     return pl.pallas_call(
         expert_kernel,
-        out_shape=jax.ShapeDtypeStruct(
-            (lanes, rows.shape[0], down.shape[1] // lanes), jnp.bfloat16
-        ),
-        scratch_shapes=[pltpu.VMEM(rows.shape, jnp.float32)],
+        out_shape=jax.ShapeDtypeStruct((lanes, lanes * some, width // lanes), jnp.bfloat16),
         compiler_params=pltpu.CompilerParams(vmem_limit_bytes=20 << 20),
         name="expert",
-    )(rows, gate, up, down)
-
-
-def settle_kernel(parts, result, lines):
-    lanes, _, quarter = parts.shape
+    )(rows, gain.reshape(1, width), gate, up, down)
+
+
+def settle_kernel(lane, parts, rows, result, lines):
+    lanes, count, quarter = parts.shape
     pieces, wide = lines.shape[1:]
-    total = parts[0].astype(jnp.float32)
-    for part in range(1, lanes):
+    own = pl.ds(pl.multiple_of(lane[0] * quarter, quarter), quarter)
+    total = rows[:, :, own].astype(jnp.float32).reshape(count, quarter)
+    for part in range(lanes):
         total = total + parts[part].astype(jnp.float32)
     for piece in range(pieces):
         lines[:, piece, :] = total[:, piece * wide : (piece + 1) * wide]
     result[...] = lines[...].astype(jnp.bfloat16)
 
 
-def settle(parts):
+def settle(parts, rows, lane):
     _, count, quarter = parts.shape
     shape = (count, quarter // 128, 128)
+    vmem = pl.BlockSpec(memory_space=pltpu.VMEM)
     return pl.pallas_call(
         settle_kernel,
+        in_specs=[pl.BlockSpec(memory_space=pltpu.SMEM), vmem, vmem],
+        out_specs=vmem,
         out_shape=jax.ShapeDtypeStruct(shape, jnp.bfloat16),
         scratch_shapes=[pltpu.VMEM(shape, jnp.float32)],
         compiler_params=pltpu.CompilerParams(vmem_limit_bytes=20 << 20),
         name="settle",
-    )(parts)
-
-
-def combine_kernel(chosen, shares, returned, residual, result, lines):
+    )(lane.reshape(1), parts, rows)
+
+
+def combine_kernel(chosen, shares, returned, result, lines):
     count, pieces, wide = lines.shape
     top = chosen.shape[0] // count
     for row in range(count):
@@ -319,22 +392,22 @@
         lines[row] = total
     for piece in range(pieces):
         here = slice(piece * wide, (piece + 1) * wide)
-        result[:, here] = (residual[:, here] + lines[:, piece, :]).astype(jnp.bfloat16)
-
-
-def combine(chosen, shares, returned, residual):
-    count, quarter = residual.shape
+        result[:, here] = lines[:, piece, :].astype(jnp.bfloat16)
+
+
+def combine(chosen, shares, returned, count):
+    _, pieces, wide = returned.shape
     vmem = pl.BlockSpec(memory_space=pltpu.VMEM)
     smem = pl.BlockSpec(memory_space=pltpu.SMEM)
     return pl.pallas_call(
         combine_kernel,
-        in_specs=[smem, smem, vmem, vmem],
+        in_specs=[smem, smem, vmem],
         out_specs=vmem,
-        out_shape=jax.ShapeDtypeStruct((count, quarter), jnp.bfloat16),
-        scratch_shapes=[pltpu.VMEM((count, *returned.shape[1:]), jnp.float32)],
+        out_shape=jax.ShapeDtypeStruct((count, pieces * wide), jnp.bfloat16),
+        scratch_shapes=[pltpu.VMEM((count, pieces, wide), jnp.float32)],
         compiler_params=pltpu.CompilerParams(vmem_limit_bytes=20 << 20),
         name="combine",
-    )(chosen, shares, returned, residual)
+    )(chosen, shares, returned)
 
 
 def body(
@@ -364,39 +437,31 @@
     lanes = lax.axis_size("tp")
     experts = lax.axis_size(EP)
     lane = lax.axis_index("tp")
-    block = width // layers
-
-    spread_rows, normed = norm(tokens, mixer_gain, layers)
+
+    spread_rows, normed = norm(tokens, mixer_gain, expert_ids, layers, experts)
     spread_rows = swap(spread_rows, "z")
     weights = lax.all_gather(
         jnp.concatenate([w_query, w_key, w_value, w_out.T], axis=1), PLANE, axis=0, tiled=True
     )
-    partial_rows = jnp.dot(
-        spread_rows.reshape(layers * rows, block),
-        weights[:, : 3 * cols],
-        preferred_element_type=jnp.float32,
-    ).astype(jnp.bfloat16)
-    summed = swap(partial_rows.reshape(layers, rows, 3 * cols), "z")
+    summed = swap(project(spread_rows, weights, rows, 3 * cols), "z")
     factors = low_rank(
         normed, decay_down, decay_up, decay_base, rate_down, rate_up, head_gain, lane
     )
-    match = expert_ids[:, :, None] == jnp.arange(experts, dtype=jnp.int32)[None, None, :]
-    order = jnp.arange(rows, dtype=jnp.int32)[:, None, None]
-    slots = jnp.min(jnp.where(match, order, rows), axis=(0, 1))
+    own = layers // lanes
+    slots = lax.dynamic_slice_in_dim(spread_rows[:, 2 * rows, :experts], lane * own, own, 0)
+    slots = slots.astype(jnp.int32).reshape(-1)
     shares = (route_weight / jnp.sum(route_weight, axis=1, keepdims=True)).reshape(-1)
     chosen = expert_ids.reshape(-1)
     summed, factors, slots, shares, chosen = lax.optimization_barrier(
         (summed, factors, slots, shares, chosen)
     )
     next_state, spread_out = recurrence(summed, factors, head_state)
-    partial_out = output(swap(spread_out, "z"), weights, lanes)
-    home_out = swap(partial_out.reshape(layers * lanes, rows, block), ("z", "tp"))
-    home_out = home_out.reshape(layers, lanes, rows, block)
-    outbound, residual = dispatch(home_out, tokens, expert_gain, slots, lane)
-    arrived = swap(outbound, EP)
-    expert_parts = expert_rows(arrived, w_gate[0], w_up[0], w_down[0], lanes)
-    returned = swap(settle(swap(expert_parts, "tp")), EP)
-    layer_out = combine(chosen, shares, returned, residual)
+    mixed_parts = swap(output(swap(spread_out, "z"), weights, lanes), "tp")
+    arrived = swap(dispatch(mixed_parts, spread_rows, slots, lane, experts), EP)
+    whole = swap(assemble(arrived, layers, lanes, width), "tp")
+    expert_parts = expert_rows(whole, expert_gain, w_gate[0], w_up[0], w_down[0])
+    returned = swap(settle(swap(expert_parts, "tp"), whole, lane), EP)
+    layer_out = combine(chosen, shares, returned, rows)
     return (layer_out, next_state)
 
 

time: 144 us -> 142 us (0.986)
  blocking collectives: 106 us -> 102 us
  local copies, waits for them, and re-layouts: 1.97 us -> 3.95 us
    all_to_all x5 -> x6, blocking collectives: 85.7 us -> 82.2 us  [swap(): return lax.all_to_all(array, axis, split_axis=0, concat_axis=0, tiled=True)]
    unnamed x41 -> x39, local copies, waits for them, and re-layouts: 1.71 us -> 3.68 us
    pallas_call x5 -> x7, Pallas kernels: 4.26 us -> 5.43 us  [the longest x1 1.22 us: combine(): pl.pallas_call(combine_kernel, in_specs=[smem, smem, vmem], out_specs=vme...]
where the time goes in v6:
time: 142 us; the launch traced here: 141 us
  blocking collectives  102 us (72%)
  starting transfers between devices  18 us (13%)
  Pallas kernels  8.85 us (6%)
  waiting for transfers between devices  7.35 us (5%)
  local copies, waits for them, and re-layouts  3.95 us (3%)
    all_to_all x6, blocking collectives, swap(): return lax.all_to_all(array, axis, split_axis=0, concat_axis=0, tiled=True)  82.2 us
    all_gather x1, blocking collectives, body(): lax.all_gather(jnp.concatenate([w_query, w_key, w_value, w_out.T], axis=1...  19.9 us
    all_to_all x2, starting transfers between devices, swap(): return lax.all_to_all(array, axis, split_axis=0, concat_axis=0, tiled=True)  18 us
    all_to_all x2, waiting for transfers between devices, swap(): return lax.all_to_all(array, axis, split_axis=0, concat_axis=0, tiled=True)  7.35 us
    unnamed x39, local copies, waits for them, and re-layouts  3.68 us
  transfers between devices with their start and end apart: 2, of which 1 were waited for; matrix products, arithmetic and copies ran while one was open for 0% of the time, Pallas kernels for 0%

profile of v6, /device:TPU:1, one launch (start us, length us, event | category | flops | bytes accessed | tf_op | source)
XLA Modules:
  0.0 141.3 jit_solution(8339276045804624553)
XLA Ops:
  0.6 0.7 copy-done.11
  1.3 0.8 copy-done.8
  2.2 0.7 copy-done.10
  2.8 0.9 norm.1
  3.8 11.0 %all-to-all-start = ((bf16[8,48,256]{2,1,0:T(8,128)(2,1)}), bf16[8,48,256]{2,1,0:T(8,128)(2,1)S(1)}, u32[]{:S(2)}, u32[]{:S(2)}) async-start(bf16[8,48,256]{2,1,0:T(8,128)(2,1)} %get-tuple-element.11), calls=%async_computation | async-start | bytes 393216 | tf_op jit(solution)/shard_map/all_to_all | solution.py:18
  14.9 19.9 %all_gather.3.weights = bf16[256,1024]{1,0:T(8,128)(2,1)S(1)} all-gather(bf16[16,1024]{1,0:T(8,128)(2,1)S(1)} %pad_maximum_fusion), channel_id=1, replica_groups=mesh['z'=8,'y'=8,'c'=2,'tp'=4] {'y','c'}, dimensions={0}, use_global_device_ids=true | all-gather | bytes 557056 | tf_op jit(solution)/shard_map/all_gather | solution.py:443
  34.9 0.9 project.1
  35.8 7.1 %all-to-all-start.1 = ((bf16[8,16,768]{2,1,0:T(8,128)(2,1)}), bf16[8,16,768]{2,1,0:T(8,128)(2,1)S(1)}, u32[]{:S(2)}, u32[]{:S(2)}) async-start(bf16[8,16,768]{2,1,0:T(8,128)(2,1)} %project.1), calls=%async_computation.1 | async-start | bytes 393216 | tf_op jit(solution)/shard_map/all_to_all | solution.py:18
  42.9 0.7 copy-done.18
  43.9 0.4 copy-done.13
  44.6 0.6 low_rank.1.factors
  45.2 7.3 %all-to-all-done.1.parts = bf16[8,16,768]{2,1,0:T(8,128)(2,1)S(1)} async-done(((bf16[8,16,768]{2,1,0:T(8,128)(2,1)}), bf16[8,16,768]{2,1,0:T(8,128)(2,1)S(1)}, u32[]{:S(2)}, u32[]{:S(2)}) %all-to-all-start.1) | async-done | bytes 196640 | tf_op jit(solution)/shard_map/all_to_all | solution.py:18
  52.6 2.6 %recurrence.1 = (f32[16,128,128]{2,1,0:T(8,128)}, bf16[8,16,256]{2,1,0:T(8,128)(2,1)S(1)}) custom-call(bf16[8,16,768]{2,1,0:T(8,128)(2,1)S(1)} %all-to-all-done.1.parts, f32[3,16,256]{2,1,0:T(8,128)S(1)} %low_rank.1.factors, f32[16,128,128]{2,1,0:T(8,128)S(1)} %bitcast.23), custom_call_target="tpu_custom_call" | custom-call | tf_op jit(solution)/shard_map/recurrence/pallas_call | solution.py:218
  55.2 9.7 %all_to_all.40.heads = bf16[8,16,256]{2,1,0:T(8,128)(2,1)S(1)} all-to-all(bf16[8,16,256]{2,1,0:T(8,128)(2,1)S(1)} %get-tuple-element.18), channel_id=1, replica_groups=mesh['z'=8,'y'=8,'c'=2,'tp'=4] {'z'}, dimensions={0} | all-to-all | bytes 131072 | tf_op jit(solution)/shard_map/all_to_all | solution.py:18
  65.1 8.3 %all_to_all.41.parts = bf16[4,32,256]{2,1,0:T(8,128)(2,1)S(1)} all-to-all(bf16[4,32,256]{2,1,0:T(8,128)(2,1)S(1)} %output.1), channel_id=1, replica_groups=mesh['z'=8,'y'=8,'c'=2,'tp'=4] {'tp'}, dimensions={0} | all-to-all | bytes 131072 | tf_op jit(solution)/shard_map/all_to_all | solution.py:18
  73.4 1.0 dispatch.1
  74.3 22.3 %all_to_all.42.arrived = bf16[128,4,128]{2,1,0:T(4,128)(2,1)S(1)} all-to-all(bf16[128,4,128]{2,1,0:T(4,128)(2,1)S(1)} %dispatch.1), channel_id=1, replica_groups=mesh['z'=8,'y'=8,'c'=2,'tp'=4] {'z','y','c'}, dimensions={0} | all-to-all | bytes 262144 | tf_op jit(solution)/shard_map/all_to_all | solution.py:18
  96.7 0.3 assemble.1
  97.0 11.7 %all_to_all.43.rows = bf16[4,32,2048]{2,1,0:T(8,128)(2,1)S(1)} all-to-all(bf16[4,32,2048]{2,1,0:T(8,128)(2,1)S(1)} %assemble.1), channel_id=1, replica_groups=mesh['z'=8,'y'=8,'c'=2,'tp'=4] {'tp'}, dimensions={0} | all-to-all | bytes 1048576 | tf_op jit(solution)/shard_map/all_to_all | solution.py:18
  108.7 0.8 expert.1
  109.6 10.7 %all_to_all.44.parts = bf16[4,128,512]{2,1,0:T(8,128)(2,1)S(1)} all-to-all(bf16[4,128,512]{2,1,0:T(8,128)(2,1)S(1)} %expert.1), channel_id=1, replica_groups=mesh['z'=8,'y'=8,'c'=2,'tp'=4] {'tp'}, dimensions={0} | all-to-all | bytes 1048576 | tf_op jit(solution)/shard_map/all_to_all | solution.py:18
  120.3 0.3 settle.1
  120.6 19.5 %all_to_all.45.returned = bf16[128,4,128]{2,1,0:T(4,128)(2,1)S(1)} all-to-all(bf16[128,4,128]{2,1,0:T(4,128)(2,1)S(1)} %settle.1), channel_id=1, replica_groups=mesh['z'=8,'y'=8,'c'=2,'tp'=4] {'z','y','c'}, dimensions={0} | all-to-all | bytes 262144 | tf_op jit(solution)/shard_map/all_to_all | solution.py:18
  140.0 1.2 combine.1
  (44 shorter events, 0.9 us)
Async XLA Ops:
  0.6 0.7 copy-start.11
  1.3 0.8 copy-start.8
  2.1 0.7 copy-start.10
  3.8 11.0 %copy-start.14 = (bf16[256,16]{0,1:T(8,128)(2,1)S(1)}, bf16[256,16]{0,1:T(8,128)(2,1)}, u32[]{:S(2)}) copy-start(bf16[256,16]{0,1:T(8,128)(2,1)} %param.31) | copy-start | bytes 24580
  3.8 11.0 %copy-start.15 = (bf16[16,256]{1,0:T(8,128)(2,1)S(1)}, bf16[16,256]{1,0:T(8,128)(2,1)}, u32[]{:S(2)}) copy-start(bf16[16,256]{1,0:T(8,128)(2,1)} %param.24) | copy-start | bytes 24580
  3.8 11.0 %copy-start.16 = (bf16[16,256]{1,0:T(8,128)(2,1)S(1)}, bf16[16,256]{1,0:T(8,128)(2,1)}, u32[]{:S(2)}) copy-start(bf16[16,256]{1,0:T(8,128)(2,1)} %param.23) | copy-start | bytes 24580
  3.8 11.0 %copy-start.17 = (bf16[16,256]{1,0:T(8,128)(2,1)S(1)}, bf16[16,256]{1,0:T(8,128)(2,1)}, u32[]{:S(2)}) copy-start(bf16[16,256]{1,0:T(8,128)(2,1)} %param.22) | copy-start | bytes 24580
  3.8 31.0 %all-to-all-start = ((bf16[8,48,256]{2,1,0:T(8,128)(2,1)}), bf16[8,48,256]{2,1,0:T(8,128)(2,1)S(1)}, u32[]{:S(2)}, u32[]{:S(2)}) async-start(bf16[8,48,256]{2,1,0:T(8,128)(2,1)} %get-tuple-element.11), calls=%async_computation | async-start | bytes 393216 | tf_op jit(solution)/shard_map/all_to_all | solution.py:18
  14.9 29.0 %copy-start.5 = (bf16[2048,64]{0,1:T(8,128)(2,1)S(1)}, bf16[2048,64]{0,1:T(8,128)(2,1)}, u32[]{:S(2)}) copy-start(bf16[2048,64]{0,1:T(8,128)(2,1)} %param.28) | copy-start | bytes 786436
  14.9 29.0 %copy-start.6 = (bf16[64,1024]{1,0:T(8,128)(2,1)S(1)}, bf16[64,1024]{1,0:T(8,128)(2,1)}, u32[]{:S(2)}) copy-start(bf16[64,1024]{1,0:T(8,128)(2,1)} %up.1) | copy-start | bytes 393220
  14.9 29.0 %copy-start.7 = (bf16[64,1024]{1,0:T(8,128)(2,1)S(1)}, bf16[64,1024]{1,0:T(8,128)(2,1)}, u32[]{:S(2)}) copy-start(bf16[64,1024]{1,0:T(8,128)(2,1)} %rate_up.1) | copy-start | bytes 393220
  34.9 17.7 %copy-start = (f32[16,4,4096]{2,1,0:T(4,128)S(1)}, f32[16,4,4096]{2,1,0:T(4,128)}, u32[]{:S(2)}) copy-start(f32[16,4,4096]{2,1,0:T(4,128)} %param.20) | copy-start | bytes 3145732
  35.8 8.2 %copy-start.4 = (bf16[2048,64]{0,1:T(8,128)(2,1)S(1)}, bf16[2048,64]{0,1:T(8,128)(2,1)}, u32[]{:S(2)}) copy-start(bf16[2048,64]{0,1:T(8,128)(2,1)} %param.25) | copy-start | bytes 786436
  35.8 16.8 %all-to-all-start.1 = ((bf16[8,16,768]{2,1,0:T(8,128)(2,1)}), bf16[8,16,768]{2,1,0:T(8,128)(2,1)S(1)}, u32[]{:S(2)}, u32[]{:S(2)}) async-start(bf16[8,16,768]{2,1,0:T(8,128)(2,1)} %project.1), calls=%async_computation.1 | async-start | bytes 393216 | tf_op jit(solution)/shard_map/all_to_all | solution.py:18
  42.9 0.7 copy-start.18
  43.7 0.7 copy-start.13
  43.9 0.7 copy-start.12
  96.7 12.0 %copy-start.3 = (bf16[1,128,2048]{2,1,0:T(8,128)(2,1)S(1)}, bf16[1,128,2048]{2,1,0:T(8,128)(2,1)}, u32[]{:S(2)}) copy-start(bf16[1,128,2048]{2,1,0:T(8,128)(2,1)} %param.37) | copy-start | bytes 1572868
  96.7 12.0 %copy-start.9 = (f32[2048]{0:T(1024)S(1)}, f32[2048]{0:T(1024)}, u32[]{:S(2)}) copy-start(f32[2048]{0:T(1024)} %param.32) | copy-start | bytes 24580
  97.0 11.7 %copy-start.1 = (bf16[1,2048,128]{2,1,0:T(8,128)(2,1)S(1)}, bf16[1,2048,128]{2,1,0:T(8,128)(2,1)}, u32[]{:S(2)}) copy-start(bf16[1,2048,128]{2,1,0:T(8,128)(2,1)} %param.35) | copy-start | bytes 1572868
  97.0 11.7 %copy-start.2 = (bf16[1,2048,128]{2,1,0:T(8,128)(2,1)S(1)}, bf16[1,2048,128]{2,1,0:T(8,128)(2,1)}, u32[]{:S(2)}) copy-start(bf16[1,2048,128]{2,1,0:T(8,128)(2,1)} %param.36) | copy-start | bytes 1572868

commit v7 on v6

--- a/solution.py
+++ b/solution.py
@@ -59,6 +59,7 @@
     count, width = tokens.shape
     bf16 = jnp.bfloat16
     top = expert_ids.shape[1]
+    inputs = (tokens, gain.reshape(1, width), expert_ids.T)
     return pl.pallas_call(
         functools.partial(norm_kernel, experts),
         in_specs=[pl.BlockSpec(memory_space=pltpu.HBM)] * 3,
@@ -74,7 +75,7 @@
         ],
         compiler_params=pltpu.CompilerParams(vmem_limit_bytes=20 << 20),
         name="norm",
-    )(tokens, gain.reshape(1, width), expert_ids.T)
+    )(*(pltpu.with_memory_space_constraint(x, pltpu.HBM) for x in inputs))
 
 
 def project_kernel(rows, weights, result):
@@ -250,7 +251,7 @@
     )(heads, weights)
 
 
-def dispatch_kernel(slots, lane, parts, rows, outbound, residual, lines):
+def dispatch_kernel(lane, parts, rows, outbound, lines):
     lanes, some, block = parts.shape
     own = rows.shape[0] // lanes
     count = some // own
@@ -260,44 +261,36 @@
     mixed = parts[0].astype(f32)
     for part in range(1, lanes):
         mixed = mixed + parts[part].astype(f32)
+    order = lax.broadcasted_iota(jnp.int32, (count, experts), 0).astype(f32)
     for k in range(own):
-        here = rows[lane[0] * own + k, count : 2 * count, :].astype(f32)
-        total = (here + mixed[k * count : (k + 1) * count]).astype(bf16).astype(f32)
-        base = k * (count + 1)
+        source = lane[0] * own + k
+        here = rows[source, count : 2 * count, :].astype(f32)
+        residual = (here + mixed[k * count : (k + 1) * count]).astype(bf16)
+        table = rows[source, 2 * count :, :experts].astype(f32)
+        chosen = jnp.where(table == order, 1.0, 0.0).astype(bf16)
+        packed = lax.dot_general(
+            chosen, residual, (((0,), (0,)), ((), ())), preferred_element_type=f32
+        )
         for piece in range(pieces):
-            residual[base : base + count, piece, :] = total[:, piece * wide : (piece + 1) * wide]
-        residual[base + count] = jnp.zeros((pieces, wide), f32)
-
-    def send(expert, carry):
-        for k in range(own):
-            slot = slots[k * experts + expert] + k * (count + 1)
-            lines[expert, k * pieces : (k + 1) * pieces, :] = residual[slot]
-        return carry
-
-    lax.fori_loop(0, experts, send, 0, unroll=8)
+            lines[:, k * pieces + piece, :] = packed[:, piece * wide : (piece + 1) * wide]
     outbound[...] = lines[...].astype(bf16)
 
 
-def dispatch(parts, rows, slots, lane, experts):
+def dispatch(parts, rows, lane, experts):
     lanes, some, block = parts.shape
     own = rows.shape[0] // lanes
     wide = 128
-    pieces = block // wide
+    shape = (experts, own * (block // wide), wide)
     vmem = pl.BlockSpec(memory_space=pltpu.VMEM)
-    smem = pl.BlockSpec(memory_space=pltpu.SMEM)
-    shape = (experts, own * pieces, wide)
     return pl.pallas_call(
         dispatch_kernel,
-        in_specs=[smem, smem, vmem, vmem],
+        in_specs=[pl.BlockSpec(memory_space=pltpu.SMEM), vmem, vmem],
         out_specs=vmem,
         out_shape=jax.ShapeDtypeStruct(shape, jnp.bfloat16),
-        scratch_shapes=[
-            pltpu.VMEM((own + some, pieces, wide), jnp.float32),
-            pltpu.VMEM(shape, jnp.float32),
-        ],
+        scratch_shapes=[pltpu.VMEM(shape, jnp.float32)],
         compiler_params=pltpu.CompilerParams(vmem_limit_bytes=20 << 20),
         name="dispatch",
-    )(slots, lane.reshape(1), parts, rows)
+    )(lane.reshape(1), parts, rows)
 
 
 def assemble_kernel(layers, arrived, result, lines):
@@ -381,33 +374,26 @@
     )(lane.reshape(1), parts, rows)
 
 
-def combine_kernel(chosen, shares, returned, result, lines):
-    count, pieces, wide = lines.shape
-    top = chosen.shape[0] // count
-    for row in range(count):
-        total = 0.0
-        for k in range(top):
-            place = row * top + k
-            total = total + shares[place] * returned[chosen[place]].astype(jnp.float32)
-        lines[row] = total
+def combine_kernel(weights, returned, result, lines):
+    pieces, wide = returned.shape[1:]
+    lines[...] = returned[...].astype(jnp.float32)
+    high, low = split_terms(weights[...])
     for piece in range(pieces):
-        here = slice(piece * wide, (piece + 1) * wide)
-        result[:, here] = lines[:, piece, :].astype(jnp.bfloat16)
-
-
-def combine(chosen, shares, returned, count):
+        here = lines[:, piece, :].astype(jnp.bfloat16)
+        total = jnp.dot(high, here, preferred_element_type=jnp.float32)
+        total = total + jnp.dot(low, here, preferred_element_type=jnp.float32)
+        result[:, piece * wide : (piece + 1) * wide] = total.astype(jnp.bfloat16)
+
+
+def combine(weights, returned):
     _, pieces, wide = returned.shape
-    vmem = pl.BlockSpec(memory_space=pltpu.VMEM)
-    smem = pl.BlockSpec(memory_space=pltpu.SMEM)
     return pl.pallas_call(
         combine_kernel,
-        in_specs=[smem, smem, vmem],
-        out_specs=vmem,
-        out_shape=jax.ShapeDtypeStruct((count, pieces * wide), jnp.bfloat16),
-        scratch_shapes=[pltpu.VMEM((count, pieces, wide), jnp.float32)],
+        out_shape=jax.ShapeDtypeStruct((weights.shape[0], pieces * wide), jnp.bfloat16),
+        scratch_shapes=[pltpu.VMEM(returned.shape, jnp.float32)],
         compiler_params=pltpu.CompilerParams(vmem_limit_bytes=20 << 20),
         name="combine",
-    )(chosen, shares, returned)
+    )(weights, returned)
 
 
 def body(
@@ -441,27 +427,24 @@
     spread_rows, normed = norm(tokens, mixer_gain, expert_ids, layers, experts)
     spread_rows = swap(spread_rows, "z")
     weights = lax.all_gather(
-        jnp.concatenate([w_query, w_key, w_value, w_out.T], axis=1), PLANE, axis=0, tiled=True
-    )
+        jnp.concatenate([w_query, w_key, w_value, w_out.T], axis=1), PLANE, axis=0
+    )
+    weights = weights.reshape(-1, weights.shape[2])
     summed = swap(project(spread_rows, weights, rows, 3 * cols), "z")
     factors = low_rank(
         normed, decay_down, decay_up, decay_base, rate_down, rate_up, head_gain, lane
     )
-    own = layers // lanes
-    slots = lax.dynamic_slice_in_dim(spread_rows[:, 2 * rows, :experts], lane * own, own, 0)
-    slots = slots.astype(jnp.int32).reshape(-1)
-    shares = (route_weight / jnp.sum(route_weight, axis=1, keepdims=True)).reshape(-1)
-    chosen = expert_ids.reshape(-1)
-    summed, factors, slots, shares, chosen = lax.optimization_barrier(
-        (summed, factors, slots, shares, chosen)
-    )
+    shares = route_weight / jnp.sum(route_weight, axis=1, keepdims=True)
+    match = expert_ids[:, :, None] == jnp.arange(experts, dtype=jnp.int32)[None, None, :]
+    shares = jnp.sum(jnp.where(match, shares[:, :, None], 0.0), axis=1)
+    summed, factors, shares = lax.optimization_barrier((summed, factors, shares))
     next_state, spread_out = recurrence(summed, factors, head_state)
     mixed_parts = swap(output(swap(spread_out, "z"), weights, lanes), "tp")
-    arrived = swap(dispatch(mixed_parts, spread_rows, slots, lane, experts), EP)
+    arrived = swap(dispatch(mixed_parts, spread_rows, lane, experts), EP)
     whole = swap(assemble(arrived, layers, lanes, width), "tp")
     expert_parts = expert_rows(whole, expert_gain, w_gate[0], w_up[0], w_down[0])
     returned = swap(settle(swap(expert_parts, "tp"), whole, lane), EP)
-    layer_out = combine(chosen, shares, returned, rows)
+    layer_out = combine(shares, returned)
     return (layer_out, next_state)
 
 

time: 142 us -> 140 us (0.986)
  local copies, waits for them, and re-layouts: 3.95 us -> 2.04 us
    unnamed x39 -> x34, local copies, waits for them, and re-layouts: 3.68 us -> 2.04 us
where the time goes in v7:
time: 140 us; the launch traced here: 139 us
  blocking collectives  102 us (73%)
  starting transfers between devices  18 us (13%)
  Pallas kernels  8.88 us (6%)
  waiting for transfers between devices  7 us (5%)
  local copies, waits for them, and re-layouts  2.04 us (1%)
    all_to_all x6, blocking collectives, swap(): return lax.all_to_all(array, axis, split_axis=0, concat_axis=0, tiled=True)  82.2 us
    all_gather x1, blocking collectives, body(): lax.all_gather(jnp.concatenate([w_query, w_key, w_value, w_out.T], axis=1...  19.9 us
    all_to_all x2, starting transfers between devices, swap(): return lax.all_to_all(array, axis, split_axis=0, concat_axis=0, tiled=True)  18 us
    all_to_all x2, waiting for transfers between devices, swap(): return lax.all_to_all(array, axis, split_axis=0, concat_axis=0, tiled=True)  7 us
  transfers between devices with their start and end apart: 2, of which 1 were waited for; matrix products, arithmetic and copies ran while one was open for 0% of the time, Pallas kernels for 0%

profile of v7, /device:TPU:1, one launch (start us, length us, event | category | flops | bytes accessed | tf_op | source)
XLA Modules:
  0.0 139.1 jit_solution(2354468010425655201)
XLA Ops:
  0.6 1.7 %norm.1 = (bf16[8,48,256]{2,1,0:T(8,128)(2,1)}, bf16[16,2048]{1,0:T(8,128)(2,1)S(1)}) custom-call(bf16[16,2048]{1,0:T(8,128)(2,1)} %tokens_in.1, f32[1,2048]{1,0:T(1,128)} %bitcast.31, s32[2,16]{1,0:T(2,128)} %bitcast.33), custom_call_target="tpu_custom_call" | custom-call | tf_op jit(solution)/shard_map/norm/pallas_call | solution.py:63
  2.4 11.0 %all-to-all-start = ((bf16[8,48,256]{2,1,0:T(8,128)(2,1)}), bf16[8,48,256]{2,1,0:T(8,128)(2,1)S(1)}, u32[]{:S(2)}, u32[]{:S(2)}) async-start(bf16[8,48,256]{2,1,0:T(8,128)(2,1)} %get-tuple-element.9), calls=%async_computation | async-start | bytes 393216 | tf_op jit(solution)/shard_map/all_to_all | solution.py:18
  13.5 19.9 %all-gather.weights = bf16[256,1024]{1,0:T(8,128)(2,1)S(1)} all-gather(bf16[16,1024]{1,0:T(8,128)(2,1)S(1)} %pad_maximum_fusion), channel_id=2, replica_groups=mesh['z'=8,'y'=8,'c'=2,'tp'=4] {'y','c'}, dimensions={0}, use_global_device_ids=true | all-gather | bytes 557056 | tf_op jit(solution)/shard_map/all_gather | solution.py:429
  33.4 0.9 project.1
  34.3 7.1 %all-to-all-start.1 = ((bf16[8,16,768]{2,1,0:T(8,128)(2,1)}), bf16[8,16,768]{2,1,0:T(8,128)(2,1)S(1)}, u32[]{:S(2)}, u32[]{:S(2)}) async-start(bf16[8,16,768]{2,1,0:T(8,128)(2,1)} %project.1), calls=%async_computation.1 | async-start | bytes 393216 | tf_op jit(solution)/shard_map/all_to_all | solution.py:18
  41.4 0.7 copy-done.16
  42.1 0.6 copy-done.9
  42.8 0.6 low_rank.1.factors
  43.4 0.7 copy-done.15
  44.1 0.1 select_reduce_fusion.weights
  44.1 7.0 %all-to-all-done.1.parts = bf16[8,16,768]{2,1,0:T(8,128)(2,1)S(1)} async-done(((bf16[8,16,768]{2,1,0:T(8,128)(2,1)}), bf16[8,16,768]{2,1,0:T(8,128)(2,1)S(1)}, u32[]{:S(2)}, u32[]{:S(2)}) %all-to-all-start.1) | async-done | bytes 196640 | tf_op jit(solution)/shard_map/all_to_all | solution.py:18
  51.1 2.6 %recurrence.1 = (f32[16,128,128]{2,1,0:T(8,128)}, bf16[8,16,256]{2,1,0:T(8,128)(2,1)S(1)}) custom-call(bf16[8,16,768]{2,1,0:T(8,128)(2,1)S(1)} %all-to-all-done.1.parts, f32[3,16,256]{2,1,0:T(8,128)S(1)} %low_rank.1.factors, f32[16,128,128]{2,1,0:T(8,128)S(1)} %bitcast.22), custom_call_target="tpu_custom_call" | custom-call | tf_op jit(solution)/shard_map/recurrence/pallas_call | solution.py:219
  53.8 9.7 %all_to_all.40.heads = bf16[8,16,256]{2,1,0:T(8,128)(2,1)S(1)} all-to-all(bf16[8,16,256]{2,1,0:T(8,128)(2,1)S(1)} %get-tuple-element.14), channel_id=1, replica_groups=mesh['z'=8,'y'=8,'c'=2,'tp'=4] {'z'}, dimensions={0} | all-to-all | bytes 131072 | tf_op jit(solution)/shard_map/all_to_all | solution.py:18
  63.4 0.2 output.1
  63.6 8.3 %all_to_all.41.parts = bf16[4,32,256]{2,1,0:T(8,128)(2,1)S(1)} all-to-all(bf16[4,32,256]{2,1,0:T(8,128)(2,1)S(1)} %output.1), channel_id=1, replica_groups=mesh['z'=8,'y'=8,'c'=2,'tp'=4] {'tp'}, dimensions={0} | all-to-all | bytes 131072 | tf_op jit(solution)/shard_map/all_to_all | solution.py:18
  71.9 0.4 dispatch.1
  72.3 22.3 %all_to_all.42.arrived = bf16[128,4,128]{2,1,0:T(4,128)(2,1)S(1)} all-to-all(bf16[128,4,128]{2,1,0:T(4,128)(2,1)S(1)} %dispatch.1), channel_id=1, replica_groups=mesh['z'=8,'y'=8,'c'=2,'tp'=4] {'z','y','c'}, dimensions={0} | all-to-all | bytes 262144 | tf_op jit(solution)/shard_map/all_to_all | solution.py:18
  94.7 0.3 assemble.1
  95.0 11.7 %all_to_all.43.rows = bf16[4,32,2048]{2,1,0:T(8,128)(2,1)S(1)} all-to-all(bf16[4,32,2048]{2,1,0:T(8,128)(2,1)S(1)} %assemble.1), channel_id=1, replica_groups=mesh['z'=8,'y'=8,'c'=2,'tp'=4] {'tp'}, dimensions={0} | all-to-all | bytes 1048576 | tf_op jit(solution)/shard_map/all_to_all | solution.py:18
  106.7 0.8 expert.1
  107.6 10.7 %all_to_all.44.parts = bf16[4,128,512]{2,1,0:T(8,128)(2,1)S(1)} all-to-all(bf16[4,128,512]{2,1,0:T(8,128)(2,1)S(1)} %expert.1), channel_id=1, replica_groups=mesh['z'=8,'y'=8,'c'=2,'tp'=4] {'tp'}, dimensions={0} | all-to-all | bytes 1048576 | tf_op jit(solution)/shard_map/all_to_all | solution.py:18
  118.3 0.3 settle.1
  118.6 19.5 %all_to_all.45.returned = bf16[128,4,128]{2,1,0:T(4,128)(2,1)S(1)} all-to-all(bf16[128,4,128]{2,1,0:T(4,128)(2,1)S(1)} %settle.1), channel_id=1, replica_groups=mesh['z'=8,'y'=8,'c'=2,'tp'=4] {'z','y','c'}, dimensions={0} | all-to-all | bytes 262144 | tf_op jit(solution)/shard_map/all_to_all | solution.py:18
  138.0 1.0 combine.1
  (35 shorter events, 0.1 us)
Async XLA Ops:
  2.3 11.0 %copy-start.11 = (bf16[256,16]{0,1:T(8,128)(2,1)S(1)}, bf16[256,16]{0,1:T(8,128)(2,1)}, u32[]{:S(2)}) copy-start(bf16[256,16]{0,1:T(8,128)(2,1)} %param.31) | copy-start | bytes 24580
  2.4 11.0 %copy-start.12 = (bf16[16,256]{1,0:T(8,128)(2,1)S(1)}, bf16[16,256]{1,0:T(8,128)(2,1)}, u32[]{:S(2)}) copy-start(bf16[16,256]{1,0:T(8,128)(2,1)} %param.24) | copy-start | bytes 24580
  2.4 11.0 %copy-start.13 = (bf16[16,256]{1,0:T(8,128)(2,1)S(1)}, bf16[16,256]{1,0:T(8,128)(2,1)}, u32[]{:S(2)}) copy-start(bf16[16,256]{1,0:T(8,128)(2,1)} %param.23) | copy-start | bytes 24580
  2.4 11.0 %copy-start.14 = (bf16[16,256]{1,0:T(8,128)(2,1)S(1)}, bf16[16,256]{1,0:T(8,128)(2,1)}, u32[]{:S(2)}) copy-start(bf16[16,256]{1,0:T(8,128)(2,1)} %param.22) | copy-start | bytes 24580
  2.4 31.0 %all-to-all-start = ((bf16[8,48,256]{2,1,0:T(8,128)(2,1)}), bf16[8,48,256]{2,1,0:T(8,128)(2,1)S(1)}, u32[]{:S(2)}, u32[]{:S(2)}) async-start(bf16[8,48,256]{2,1,0:T(8,128)(2,1)} %get-tuple-element.9), calls=%async_computation | async-start | bytes 393216 | tf_op jit(solution)/shard_map/all_to_all | solution.py:18
  13.4 28.6 %copy-start.5 = (bf16[2048,64]{0,1:T(8,128)(2,1)S(1)}, bf16[2048,64]{0,1:T(8,128)(2,1)}, u32[]{:S(2)}) copy-start(bf16[2048,64]{0,1:T(8,128)(2,1)} %param.28) | copy-start | bytes 786436
  13.4 28.6 %copy-start.6 = (bf16[64,1024]{1,0:T(8,128)(2,1)S(1)}, bf16[64,1024]{1,0:T(8,128)(2,1)}, u32[]{:S(2)}) copy-start(bf16[64,1024]{1,0:T(8,128)(2,1)} %up.1) | copy-start | bytes 393220
  13.5 28.6 %copy-start.7 = (bf16[64,1024]{1,0:T(8,128)(2,1)S(1)}, bf16[64,1024]{1,0:T(8,128)(2,1)}, u32[]{:S(2)}) copy-start(bf16[64,1024]{1,0:T(8,128)(2,1)} %rate_up.1) | copy-start | bytes 393220
  33.4 17.7 %copy-start = (f32[16,4,4096]{2,1,0:T(4,128)S(1)}, f32[16,4,4096]{2,1,0:T(4,128)}, u32[]{:S(2)}) copy-start(f32[16,4,4096]{2,1,0:T(4,128)} %param.20) | copy-start | bytes 3145732
  34.3 7.8 %copy-start.4 = (bf16[2048,64]{0,1:T(8,128)(2,1)S(1)}, bf16[2048,64]{0,1:T(8,128)(2,1)}, u32[]{:S(2)}) copy-start(bf16[2048,64]{0,1:T(8,128)(2,1)} %param.25) | copy-start | bytes 786436
  34.3 7.8 %copy-start.10 = (f32[256]{0:T(256)S(1)}, f32[256]{0:T(256)}, u32[]{:S(2)}) copy-start(f32[256]{0:T(256)} %param.30) | copy-start | bytes 3076
  34.3 16.8 %all-to-all-start.1 = ((bf16[8,16,768]{2,1,0:T(8,128)(2,1)}), bf16[8,16,768]{2,1,0:T(8,128)(2,1)S(1)}, u32[]{:S(2)}, u32[]{:S(2)}) async-start(bf16[8,16,768]{2,1,0:T(8,128)(2,1)} %project.1), calls=%async_computation.1 | async-start | bytes 393216 | tf_op jit(solution)/shard_map/all_to_all | solution.py:18
  41.4 0.7 copy-start.16
  42.1 0.7 copy-start.9
  43.4 0.7 copy-start.15
  94.7 12.0 %copy-start.3 = (bf16[1,128,2048]{2,1,0:T(8,128)(2,1)S(1)}, bf16[1,128,2048]{2,1,0:T(8,128)(2,1)}, u32[]{:S(2)}) copy-start(bf16[1,128,2048]{2,1,0:T(8,128)(2,1)} %param.37) | copy-start | bytes 1572868
  94.7 12.0 %copy-start.8 = (f32[2048]{0:T(1024)S(1)}, f32[2048]{0:T(1024)}, u32[]{:S(2)}) copy-start(f32[2048]{0:T(1024)} %param.32) | copy-start | bytes 24580
  95.0 11.7 %copy-start.1 = (bf16[1,2048,128]{2,1,0:T(8,128)(2,1)S(1)}, bf16[1,2048,128]{2,1,0:T(8,128)(2,1)}, u32[]{:S(2)}) copy-start(bf16[1,2048,128]{2,1,0:T(8,128)(2,1)} %param.35) | copy-start | bytes 1572868
  95.0 11.7 %copy-start.2 = (bf16[1,2048,128]{2,1,0:T(8,128)(2,1)S(1)}, bf16[1,2048,128]{2,1,0:T(8,128)(2,1)}, u32[]{:S(2)}) copy-start(bf16[1,2048,128]{2,1,0:T(8,128)(2,1)} %param.36) | copy-start | bytes 1572868

commit v8 on v7

--- a/solution.py
+++ b/solution.py
@@ -18,14 +18,16 @@
     return lax.all_to_all(array, axis, split_axis=0, concat_axis=0, tiled=True)
 
 
-def norm_kernel(experts, tokens_in, gain_in, ids_in, rows, normed, tokens, gain, ids, done):
+def norm_kernel(experts, *refs):
+    sources, refs = refs[:6], refs[6:]
+    rows, normed, ids, base, head_gain, route, tokens, gain, done = refs
     layers, depth, block = rows.shape
     count = tokens.shape[0]
     f32, bf16 = jnp.float32, jnp.bfloat16
-    sources = (tokens_in, gain_in, ids_in)
+    targets = (tokens, gain, ids, base, head_gain, route)
     copies = [
         pltpu.make_async_copy(source, target, done.at[k])
-        for k, (source, target) in enumerate(zip(sources, (tokens, gain, ids)))
+        for k, (source, target) in enumerate(zip(sources, targets))
     ]
     for copy in copies:
         copy.start()
@@ -55,23 +57,24 @@
         rows[z, 2 * count :, :experts] = table
 
 
-def norm(tokens, gain, expert_ids, layers, experts):
+def norm(tokens, gain, expert_ids, decay_base, head_gain, route_weight, layers, experts):
     count, width = tokens.shape
     bf16 = jnp.bfloat16
-    top = expert_ids.shape[1]
-    inputs = (tokens, gain.reshape(1, width), expert_ids.T)
+    line = lambda x: x.reshape(1, -1)
+    small = (expert_ids.T, line(decay_base), line(head_gain), route_weight.T)
+    inputs = (tokens, line(gain), *small)
     return pl.pallas_call(
         functools.partial(norm_kernel, experts),
-        in_specs=[pl.BlockSpec(memory_space=pltpu.HBM)] * 3,
+        in_specs=[pl.BlockSpec(memory_space=pltpu.HBM)] * len(inputs),
         out_shape=(
             jax.ShapeDtypeStruct((layers, 3 * count, width // layers), bf16),
             jax.ShapeDtypeStruct((count, width), bf16),
+            *(jax.ShapeDtypeStruct(x.shape, x.dtype) for x in small),
         ),
         scratch_shapes=[
             pltpu.VMEM((count, width), bf16),
             pltpu.VMEM((1, width), jnp.float32),
-            pltpu.VMEM((top, count), jnp.int32),
-            pltpu.SemaphoreType.DMA((3,)),
+            pltpu.SemaphoreType.DMA((len(inputs),)),
         ],
         compiler_params=pltpu.CompilerParams(vmem_limit_bytes=20 << 20),
         name="norm",
@@ -97,7 +100,9 @@
     )(rows, weights)
 
 
-def low_rank_kernel(lane, normed, down, up, base, rate_down, rate_up, gain, result):
+def low_rank_kernel(
+    lane, normed, down, up, base, rate_down, rate_up, gain, ids, route, result, shares
+):
     f32, bf16 = jnp.float32, jnp.bfloat16
     _, count, cols = result.shape
     own = pl.ds(pl.multiple_of(lane[0] * cols, cols), cols)
@@ -113,16 +118,27 @@
     rate_pre = jnp.dot(rate_low, rate_up[:, own], preferred_element_type=f32)
     result[1] = 1.0 / (1.0 + jnp.exp(-rate_pre))
     result[2] = jnp.broadcast_to(gain[...], (count, cols))
-
-
-def low_rank(normed, decay_down, decay_up, decay_base, rate_down, rate_up, head_gain, lane):
-    cols = decay_base.shape[0]
+    route_sum = jnp.sum(route[...], axis=0, keepdims=True)
+    row = lax.broadcasted_iota(jnp.int32, shares.shape, 0)
+    weights = jnp.zeros(shares.shape, f32)
+    for k in range(ids.shape[0]):
+        share = route[k : k + 1, :] / route_sum
+        weights = weights + jnp.where(row == ids[k : k + 1, :], share, 0.0)
+    shares[...] = weights
+
+
+def low_rank(normed, decay_down, decay_up, rate_down, rate_up, small, experts, lane):
+    ids, base, head_gain, route = small
+    count, cols = normed.shape[0], base.shape[1]
     vmem = pl.BlockSpec(memory_space=pltpu.VMEM)
     return pl.pallas_call(
         low_rank_kernel,
-        in_specs=[pl.BlockSpec(memory_space=pltpu.SMEM)] + [vmem] * 7,
-        out_specs=vmem,
-        out_shape=jax.ShapeDtypeStruct((3, normed.shape[0], cols), jnp.float32),
+        in_specs=[pl.BlockSpec(memory_space=pltpu.SMEM)] + [vmem] * 9,
+        out_specs=(vmem, vmem),
+        out_shape=(
+            jax.ShapeDtypeStruct((3, count, cols), jnp.float32),
+            jax.ShapeDtypeStruct((experts, count), jnp.float32),
+        ),
         compiler_params=pltpu.CompilerParams(vmem_limit_bytes=20 << 20),
         name="low_rank",
     )(
@@ -130,10 +146,12 @@
         normed,
         decay_down.T,
         decay_up,
-        decay_base.reshape(1, cols),
+        base,
         rate_down.T,
         rate_up,
-        head_gain.reshape(1, cols),
+        head_gain,
+        ids,
+        route,
     )
 
 
@@ -149,7 +167,7 @@
     )
 
 
-def recurrence_kernel(size, parts, factors, state, new_state, spread_out):
+def recurrence_kernel(size, parts, factors, state, new_state, spread_out, fresh, done):
     decays, rates, gain = factors[0], factors[1], factors[2]
     count, cols = decays.shape
     heads = cols // size
@@ -163,10 +181,9 @@
     values = projected[:, 2 * cols :]
     square = (cols, cols)
     same_head = iota(square, 0) // size == iota(square, 1) // size
-    head_sum = jnp.where(same_head, 1.0, 0.0).astype(f32)
-    head_mean = head_sum * (1.0 / size)
-    total = lambda x, m: jnp.dot(x, m, precision=lax.Precision.HIGHEST, preferred_element_type=f32)
-    units = keys * lax.rsqrt(total(keys * keys, head_sum) + 1.0)
+    head_sum = jnp.where(same_head, 1.0, 0.0).astype(bf16)
+    head_mean = jnp.where(same_head, 1.0 / size, 0.0).astype(bf16)
+    units = keys * lax.rsqrt(exact_dot(keys * keys, head_sum) + 1.0)
     removal = units * rates
 
     def by_line(x):
@@ -196,15 +213,18 @@
         value_rows.reshape(count * lines, cols).astype(bf16), to_half, preferred_element_type=f32
     ).reshape(grid_shape)
     updated = old * by_line(decays) - removed * by_line(removal) + value_grid * by_line(keys)
-    new_state[...] = updated.reshape(new_state.shape)
+    fresh[...] = updated.reshape(fresh.shape)
+    store = pltpu.make_async_copy(fresh, new_state, done)
+    store.start()
     broad = (wide, cols)
     from_half = jnp.where(iota(broad, 0) // size == iota(broad, 1) % 2, 1.0, 0.0).astype(bf16)
     reads = exact_dot((updated * by_line(queries)).reshape(flat), from_half)
     readout = jnp.sum(jnp.where(owner[None], reads.reshape(count, *pick), 0.0), axis=1)
-    centred = readout - total(readout, head_mean)
-    spread = total(centred * centred, head_mean)
+    centred = readout - exact_dot(readout, head_mean)
+    spread = exact_dot(centred * centred, head_mean)
     scaled = (centred * lax.rsqrt(spread + group_eps) * gain).astype(bf16)
     spread_out[...] = jnp.broadcast_to(scaled[None], spread_out.shape)
+    store.wait()
 
 
 def recurrence(parts, factors, old_state):
@@ -222,6 +242,11 @@
             jax.ShapeDtypeStruct(state.shape, jnp.float32),
             jax.ShapeDtypeStruct((layers, count, cols), jnp.bfloat16),
         ),
+        out_specs=(
+            pl.BlockSpec(memory_space=pltpu.HBM),
+            pl.BlockSpec(memory_space=pltpu.VMEM),
+        ),
+        scratch_shapes=[pltpu.VMEM(state.shape, jnp.float32), pltpu.SemaphoreType.DMA],
         compiler_params=pltpu.CompilerParams(vmem_limit_bytes=40 << 20),
         name="recurrence",
     )(parts, factors, state)
@@ -374,26 +399,30 @@
     )(lane.reshape(1), parts, rows)
 
 
-def combine_kernel(weights, returned, result, lines):
-    pieces, wide = returned.shape[1:]
-    lines[...] = returned[...].astype(jnp.float32)
-    high, low = split_terms(weights[...])
+def combine_kernel(shares, returned, result, lines):
+    _, pieces, wide = returned.shape
+    f32 = jnp.float32
+    lines[...] = returned[...].astype(f32)
+    terms = split_terms(shares[...])
     for piece in range(pieces):
         here = lines[:, piece, :].astype(jnp.bfloat16)
-        total = jnp.dot(high, here, preferred_element_type=jnp.float32)
-        total = total + jnp.dot(low, here, preferred_element_type=jnp.float32)
+        total = 0.0
+        for term in terms:
+            total = total + lax.dot_general(
+                term, here, (((0,), (0,)), ((), ())), preferred_element_type=f32
+            )
         result[:, piece * wide : (piece + 1) * wide] = total.astype(jnp.bfloat16)
 
 
-def combine(weights, returned):
+def combine(shares, returned):
     _, pieces, wide = returned.shape
     return pl.pallas_call(
         combine_kernel,
-        out_shape=jax.ShapeDtypeStruct((weights.shape[0], pieces * wide), jnp.bfloat16),
+        out_shape=jax.ShapeDtypeStruct((shares.shape[1], pieces * wide), jnp.bfloat16),
         scratch_shapes=[pltpu.VMEM(returned.shape, jnp.float32)],
         compiler_params=pltpu.CompilerParams(vmem_limit_bytes=20 << 20),
         name="combine",
-    )(weights, returned)
+    )(shares, returned)
 
 
 def body(
@@ -424,20 +453,20 @@
     experts = lax.axis_size(EP)
     lane = lax.axis_index("tp")
 
-    spread_rows, normed = norm(tokens, mixer_gain, expert_ids, layers, experts)
+    spread_rows, normed, *small = norm(
+        tokens, mixer_gain, expert_ids, decay_base, head_gain, route_weight, layers, experts
+    )
     spread_rows = swap(spread_rows, "z")
     weights = lax.all_gather(
         jnp.concatenate([w_query, w_key, w_value, w_out.T], axis=1), PLANE, axis=0
     )
     weights = weights.reshape(-1, weights.shape[2])
+    weights, normed = lax.optimization_barrier((weights, normed))
+    factors, shares = low_rank(
+        normed, decay_down, decay_up, rate_down, rate_up, small, experts, lane
+    )
+    spread_rows, factors, shares = lax.optimization_barrier((spread_rows, factors, shares))
     summed = swap(project(spread_rows, weights, rows, 3 * cols), "z")
-    factors = low_rank(
-        normed, decay_down, decay_up, decay_base, rate_down, rate_up, head_gain, lane
-    )
-    shares = route_weight / jnp.sum(route_weight, axis=1, keepdims=True)
-    match = expert_ids[:, :, None] == jnp.arange(experts, dtype=jnp.int32)[None, None, :]
-    shares = jnp.sum(jnp.where(match, shares[:, :, None], 0.0), axis=1)
-    summed, factors, shares = lax.optimization_barrier((summed, factors, shares))
     next_state, spread_out = recurrence(summed, factors, head_state)
     mixed_parts = swap(output(swap(spread_out, "z"), weights, lanes), "tp")
     arrived = swap(dispatch(mixed_parts, spread_rows, lane, experts), EP)

time: 140 us -> 139 us (level)
  blocking collectives: 102 us -> 119 us
  starting transfers between devices: 18 us -> 11 us
  waiting for transfers between devices: 7 us -> 0.01 us
  local copies, waits for them, and re-layouts: 2.04 us -> 0.08 us
    all_to_all x6 -> x7, blocking collectives: 82.2 us -> 98.7 us  [swap(): return lax.all_to_all(array, axis, split_axis=0, concat_axis=0, tiled=True)]
    all_to_all x2 -> x1, starting transfers between devices: 18 us -> 11 us  [swap(): return lax.all_to_all(array, axis, split_axis=0, concat_axis=0, tiled=True)]
    all_to_all x2 -> x1, waiting for transfers between devices: 7 us -> 0.01 us  [swap(): return lax.all_to_all(array, axis, split_axis=0, concat_axis=0, tiled=True)]
    unnamed x34 -> x26, local copies, waits for them, and re-layouts: 2.04 us -> 0.08 us
  transfers between devices with their start and end apart: 2 -> 1, of which waited for: 1 -> 0; matrix products, arithmetic and copies ran while one was open for 0% -> 0% of each run, Pallas kernels for 0% -> 0%
where the time goes in v8:
time: 139 us; the launch traced here: 138 us
  blocking collectives  119 us (86%)
  starting transfers between devices  11 us (8%)
  Pallas kernels  7.73 us (6%)
    all_to_all x7, blocking collectives, swap(): return lax.all_to_all(array, axis, split_axis=0, concat_axis=0, tiled=True)  98.7 us
    all_gather x1, blocking collectives, body(): lax.all_gather(jnp.concatenate([w_query, w_key, w_value, w_out.T], axis=1...  19.9 us
    all_to_all x1, starting transfers between devices, swap(): return lax.all_to_all(array, axis, split_axis=0, concat_axis=0, tiled=True)  11 us
  transfers between devices with their start and end apart: 1, of which 0 were waited for; matrix products, arithmetic and copies ran while one was open for 0% of the time, Pallas kernels for 0%

profile of v8, /device:TPU:1, one launch (start us, length us, event | category | flops | bytes accessed | tf_op | source)
XLA Modules:
  0.0 138.3 jit_solution(5897705329544887723)
XLA Ops:
  0.6 1.7 %norm.1 = (bf16[8,48,256]{2,1,0:T(8,128)(2,1)}, bf16[16,2048]{1,0:T(8,128)(2,1)S(1)}, s32[2,16]{1,0:T(2,128)S(1)}, f32[1,256]{1,0:T(1,128)S(1)}, f32[1,256]{1,0:T(1,128)S(1)}, /*index=5*/f32[2,16]{1,0:T(2,128)S(1)}) custom-call(bf16[16,2048]{1,0:T(8,128)(2,1)} %refs_0_.1, f32[1,2048]{1,0:T(1,128)} %bitcast.30, s32[2,16]{1,0:T(2,128)} %bitcast.32, ...), custom_call_target="tpu_custom_call" | custom-call | tf_op jit(solution)/shard_map/norm/pallas_call | solution.py:66
  2.4 0.0 copy-start.9
  2.4 0.0 copy-start.11
  2.4 0.0 copy-start.12
  2.4 11.0 %all-to-all-start = ((bf16[8,48,256]{2,1,0:T(8,128)(2,1)}), bf16[8,48,256]{2,1,0:T(8,128)(2,1)S(1)}, u32[]{:S(2)}, u32[]{:S(2)}) async-start(bf16[8,48,256]{2,1,0:T(8,128)(2,1)} %get-tuple-element.17), calls=%async_computation | async-start | bytes 393216 | tf_op jit(solution)/shard_map/all_to_all | solution.py:18
  13.5 0.0 copy-start.5
  13.5 19.9 %all-gather.weights = bf16[256,1024]{1,0:T(8,128)(2,1)S(1)} all-gather(bf16[16,1024]{1,0:T(8,128)(2,1)S(1)} %pad_maximum_fusion), channel_id=2, replica_groups=mesh['z'=8,'y'=8,'c'=2,'tp'=4] {'y','c'}, dimensions={0}, use_global_device_ids=true | all-gather | bytes 557056 | tf_op jit(solution)/shard_map/all_gather | solution.py:460
  33.5 0.6 low_rank.1
  34.2 0.2 project.1
  34.4 16.5 %all_to_all.40.parts = bf16[8,16,768]{2,1,0:T(8,128)(2,1)S(1)} all-to-all(bf16[8,16,768]{2,1,0:T(8,128)(2,1)S(1)} %project.1), channel_id=1, replica_groups=mesh['z'=8,'y'=8,'c'=2,'tp'=4] {'z'}, dimensions={0} | all-to-all | bytes 393216 | tf_op jit(solution)/shard_map/all_to_all | solution.py:18
  50.9 2.1 %recurrence.1 = (f32[16,128,128]{2,1,0:T(8,128)}, bf16[8,16,256]{2,1,0:T(8,128)(2,1)S(1)}) custom-call(bf16[8,16,768]{2,1,0:T(8,128)(2,1)S(1)} %all_to_all.40.parts, f32[3,16,256]{2,1,0:T(8,128)S(1)} %get-tuple-element.29.factors, f32[16,128,128]{2,1,0:T(8,128)S(1)} %bitcast.23), custom_call_target="tpu_custom_call" | custom-call | tf_op jit(solution)/shard_map/recurrence/pallas_call | solution.py:239
  53.0 9.6 %all_to_all.41.heads = bf16[8,16,256]{2,1,0:T(8,128)(2,1)S(1)} all-to-all(bf16[8,16,256]{2,1,0:T(8,128)(2,1)S(1)} %get-tuple-element.30), channel_id=1, replica_groups=mesh['z'=8,'y'=8,'c'=2,'tp'=4] {'z'}, dimensions={0} | all-to-all | bytes 131072 | tf_op jit(solution)/shard_map/all_to_all | solution.py:18
  62.6 0.2 output.1
  62.8 8.3 %all_to_all.42.parts = bf16[4,32,256]{2,1,0:T(8,128)(2,1)S(1)} all-to-all(bf16[4,32,256]{2,1,0:T(8,128)(2,1)S(1)} %output.1), channel_id=1, replica_groups=mesh['z'=8,'y'=8,'c'=2,'tp'=4] {'tp'}, dimensions={0} | all-to-all | bytes 131072 | tf_op jit(solution)/shard_map/all_to_all | solution.py:18
  71.1 0.4 dispatch.1
  71.5 22.3 %all_to_all.43.arrived = bf16[128,4,128]{2,1,0:T(4,128)(2,1)S(1)} all-to-all(bf16[128,4,128]{2,1,0:T(4,128)(2,1)S(1)} %dispatch.1), channel_id=1, replica_groups=mesh['z'=8,'y'=8,'c'=2,'tp'=4] {'z','y','c'}, dimensions={0} | all-to-all | bytes 262144 | tf_op jit(solution)/shard_map/all_to_all | solution.py:18
  93.9 0.3 assemble.1
  94.2 0.0 copy-start.2
  94.2 11.7 %all_to_all.44.rows = bf16[4,32,2048]{2,1,0:T(8,128)(2,1)S(1)} all-to-all(bf16[4,32,2048]{2,1,0:T(8,128)(2,1)S(1)} %assemble.1), channel_id=1, replica_groups=mesh['z'=8,'y'=8,'c'=2,'tp'=4] {'tp'}, dimensions={0} | all-to-all | bytes 1048576 | tf_op jit(solution)/shard_map/all_to_all | solution.py:18
  105.9 0.8 expert.1
  106.8 10.7 %all_to_all.45.parts = bf16[4,128,512]{2,1,0:T(8,128)(2,1)S(1)} all-to-all(bf16[4,128,512]{2,1,0:T(8,128)(2,1)S(1)} %expert.1), channel_id=1, replica_groups=mesh['z'=8,'y'=8,'c'=2,'tp'=4] {'tp'}, dimensions={0} | all-to-all | bytes 1048576 | tf_op jit(solution)/shard_map/all_to_all | solution.py:18
  117.5 0.3 settle.1
  117.8 19.5 %all_to_all.46.returned = bf16[128,4,128]{2,1,0:T(4,128)(2,1)S(1)} all-to-all(bf16[128,4,128]{2,1,0:T(4,128)(2,1)S(1)} %settle.1), channel_id=1, replica_groups=mesh['z'=8,'y'=8,'c'=2,'tp'=4] {'z','y','c'}, dimensions={0} | all-to-all | bytes 262144 | tf_op jit(solution)/shard_map/all_to_all | solution.py:18
  137.2 1.0 combine.1
  (23 shorter events, 0.1 us)
Async XLA Ops:
  2.4 11.1 %copy-start.9 = (bf16[256,16]{0,1:T(8,128)(2,1)S(1)}, bf16[256,16]{0,1:T(8,128)(2,1)}, u32[]{:S(2)}) copy-start(bf16[256,16]{0,1:T(8,128)(2,1)} %param.31) | copy-start | bytes 24580
  2.4 11.1 %copy-start.10 = (bf16[16,256]{1,0:T(8,128)(2,1)S(1)}, bf16[16,256]{1,0:T(8,128)(2,1)}, u32[]{:S(2)}) copy-start(bf16[16,256]{1,0:T(8,128)(2,1)} %param.24) | copy-start | bytes 24580
  2.4 11.1 %copy-start.11 = (bf16[16,256]{1,0:T(8,128)(2,1)S(1)}, bf16[16,256]{1,0:T(8,128)(2,1)}, u32[]{:S(2)}) copy-start(bf16[16,256]{1,0:T(8,128)(2,1)} %param.23) | copy-start | bytes 24580
  2.4 11.1 %copy-start.12 = (bf16[16,256]{1,0:T(8,128)(2,1)S(1)}, bf16[16,256]{1,0:T(8,128)(2,1)}, u32[]{:S(2)}) copy-start(bf16[16,256]{1,0:T(8,128)(2,1)} %param.22) | copy-start | bytes 24580
  2.4 31.0 %copy-start.6 = (bf16[64,1024]{1,0:T(8,128)(2,1)S(1)}, bf16[64,1024]{1,0:T(8,128)(2,1)}, u32[]{:S(2)}) copy-start(bf16[64,1024]{1,0:T(8,128)(2,1)} %up.1) | copy-start | bytes 393220
  2.4 31.0 %copy-start.7 = (bf16[64,1024]{1,0:T(8,128)(2,1)S(1)}, bf16[64,1024]{1,0:T(8,128)(2,1)}, u32[]{:S(2)}) copy-start(bf16[64,1024]{1,0:T(8,128)(2,1)} %rate_up.1) | copy-start | bytes 393220
  2.4 31.7 %all-to-all-start = ((bf16[8,48,256]{2,1,0:T(8,128)(2,1)}), bf16[8,48,256]{2,1,0:T(8,128)(2,1)S(1)}, u32[]{:S(2)}, u32[]{:S(2)}) async-start(bf16[8,48,256]{2,1,0:T(8,128)(2,1)} %get-tuple-element.17), calls=%async_computation | async-start | bytes 393216 | tf_op jit(solution)/shard_map/all_to_all | solution.py:18
  13.5 20.0 %copy-start.4 = (bf16[2048,64]{0,1:T(8,128)(2,1)S(1)}, bf16[2048,64]{0,1:T(8,128)(2,1)}, u32[]{:S(2)}) copy-start(bf16[2048,64]{0,1:T(8,128)(2,1)} %param.25) | copy-start | bytes 786436
  13.5 20.0 %copy-start.5 = (bf16[2048,64]{0,1:T(8,128)(2,1)S(1)}, bf16[2048,64]{0,1:T(8,128)(2,1)}, u32[]{:S(2)}) copy-start(bf16[2048,64]{0,1:T(8,128)(2,1)} %param.28) | copy-start | bytes 786436
  33.5 17.4 %copy-start = (f32[16,4,4096]{2,1,0:T(4,128)S(1)}, f32[16,4,4096]{2,1,0:T(4,128)}, u32[]{:S(2)}) copy-start(f32[16,4,4096]{2,1,0:T(4,128)} %param.20) | copy-start | bytes 3145732
  93.9 12.0 %copy-start.3 = (bf16[1,128,2048]{2,1,0:T(8,128)(2,1)S(1)}, bf16[1,128,2048]{2,1,0:T(8,128)(2,1)}, u32[]{:S(2)}) copy-start(bf16[1,128,2048]{2,1,0:T(8,128)(2,1)} %param.37) | copy-start | bytes 1572868
  93.9 12.0 %copy-start.8 = (f32[2048]{0:T(1024)S(1)}, f32[2048]{0:T(1024)}, u32[]{:S(2)}) copy-start(f32[2048]{0:T(1024)} %param.32) | copy-start | bytes 24580
  94.2 11.7 %copy-start.1 = (bf16[1,2048,128]{2,1,0:T(8,128)(2,1)S(1)}, bf16[1,2048,128]{2,1,0:T(8,128)(2,1)}, u32[]{:S(2)}) copy-start(bf16[1,2048,128]{2,1,0:T(8,128)(2,1)} %param.35) | copy-start | bytes 1572868
  94.2 11.7 %copy-start.2 = (bf16[1,2048,128]{2,1,0:T(8,128)(2,1)S(1)}, bf16[1,2048,128]{2,1,0:T(8,128)(2,1)}, u32[]{:S(2)}) copy-start(bf16[1,2048,128]{2,1,0:T(8,128)(2,1)} %param.36) | copy-start | bytes 1572868

commit v9 on v8

--- a/solution.py
+++ b/solution.py
@@ -262,12 +262,12 @@
         (((1,), (1,)), ((), ())),
         preferred_element_type=jnp.float32,
     )
-    result[...] = product.astype(jnp.bfloat16).reshape(result.shape)
+    result[...] = jnp.broadcast_to(product.astype(jnp.bfloat16)[None], result.shape)
 
 
 def output(heads, weights, lanes):
     layers, count, _ = heads.shape
-    shape = (lanes, layers * count // lanes, weights.shape[0])
+    shape = (lanes, layers * count, weights.shape[0])
     return pl.pallas_call(
         output_kernel,
         out_shape=jax.ShapeDtypeStruct(shape, jnp.bfloat16),
@@ -276,10 +276,10 @@
     )(heads, weights)
 
 
-def dispatch_kernel(lane, parts, rows, outbound, lines):
+def dispatch_kernel(parts, rows, outbound, lines):
     lanes, some, block = parts.shape
-    own = rows.shape[0] // lanes
-    count = some // own
+    layers = rows.shape[0]
+    count = some // layers
     experts, _, wide = lines.shape
     pieces = block // wide
     f32, bf16 = jnp.float32, jnp.bfloat16
@@ -287,11 +287,10 @@
     for part in range(1, lanes):
         mixed = mixed + parts[part].astype(f32)
     order = lax.broadcasted_iota(jnp.int32, (count, experts), 0).astype(f32)
-    for k in range(own):
-        source = lane[0] * own + k
-        here = rows[source, count : 2 * count, :].astype(f32)
+    for k in range(layers):
+        here = rows[k, count : 2 * count, :].astype(f32)
         residual = (here + mixed[k * count : (k + 1) * count]).astype(bf16)
-        table = rows[source, 2 * count :, :experts].astype(f32)
+        table = rows[k, 2 * count :, :experts].astype(f32)
         chosen = jnp.where(table == order, 1.0, 0.0).astype(bf16)
         packed = lax.dot_general(
             chosen, residual, (((0,), (0,)), ((), ())), preferred_element_type=f32
@@ -301,56 +300,35 @@
     outbound[...] = lines[...].astype(bf16)
 
 
-def dispatch(parts, rows, lane, experts):
-    lanes, some, block = parts.shape
-    own = rows.shape[0] // lanes
+def dispatch(parts, rows, experts):
+    _, _, block = parts.shape
     wide = 128
-    shape = (experts, own * (block // wide), wide)
-    vmem = pl.BlockSpec(memory_space=pltpu.VMEM)
+    shape = (experts, rows.shape[0] * (block // wide), wide)
     return pl.pallas_call(
         dispatch_kernel,
-        in_specs=[pl.BlockSpec(memory_space=pltpu.SMEM), vmem, vmem],
-        out_specs=vmem,
         out_shape=jax.ShapeDtypeStruct(shape, jnp.bfloat16),
         scratch_shapes=[pltpu.VMEM(shape, jnp.float32)],
         compiler_params=pltpu.CompilerParams(vmem_limit_bytes=20 << 20),
         name="dispatch",
-    )(lane.reshape(1), parts, rows)
-
-
-def assemble_kernel(layers, arrived, result, lines):
-    lanes, some, width = result.shape
-    peers = arrived.shape[0] // layers
+    )(parts, rows)
+
+
+def expert_kernel(layers, arrived, gain, gate, up, down, result, rows, lines):
+    lanes, count, quarter = result.shape
+    peers = count // layers
     wide = arrived.shape[2]
-    own = some // peers
-    pieces = arrived.shape[1] // own
-    lines[...] = arrived[...].astype(jnp.float32)
-    for k in range(own):
+    pieces = arrived.shape[1] // layers
+    f32 = jnp.float32
+    lines[...] = arrived[...].astype(f32)
+    for k in range(layers):
         for z in range(layers):
             for piece in range(pieces):
                 start = (z * pieces + piece) * wide
                 block = lines[z * peers : (z + 1) * peers, k * pieces + piece, :]
-                block = block.astype(jnp.bfloat16)
-                for part in range(lanes):
-                    result[part, k * peers : (k + 1) * peers, start : start + wide] = block
-
-
-def assemble(arrived, layers, lanes, width):
-    some = arrived.shape[0] // lanes
-    return pl.pallas_call(
-        functools.partial(assemble_kernel, layers),
-        out_shape=jax.ShapeDtypeStruct((lanes, some, width), jnp.bfloat16),
-        scratch_shapes=[pltpu.VMEM(arrived.shape, jnp.float32)],
-        compiler_params=pltpu.CompilerParams(vmem_limit_bytes=20 << 20),
-        name="assemble",
-    )(arrived)
-
-
-def expert_kernel(rows, gain, gate, up, down, result):
-    lanes, count, quarter = result.shape
-    width = rows.shape[2]
-    f32 = jnp.float32
-    widened = rows[...].astype(f32).reshape(count, width)
+                rows[k * peers : (k + 1) * peers, start : start + wide] = block.astype(
+                    jnp.bfloat16
+                )
+    widened = rows[...].astype(f32)
     scale = lax.rsqrt(jnp.mean(widened * widened, axis=1, keepdims=True) + norm_eps)
     normed = (widened * scale * gain[...]).astype(jnp.bfloat16)
     gate_act = jnp.dot(normed, gate[...], preferred_element_type=f32)
@@ -362,21 +340,26 @@
         result[part] = product.astype(jnp.bfloat16)
 
 
-def expert_rows(rows, gain, gate, up, down):
-    lanes, some, width = rows.shape
-    return pl.pallas_call(
-        expert_kernel,
-        out_shape=jax.ShapeDtypeStruct((lanes, lanes * some, width // lanes), jnp.bfloat16),
+def expert_rows(arrived, gain, gate, up, down, layers, lanes):
+    count = arrived.shape[0]
+    width = gate.shape[0]
+    return pl.pallas_call(
+        functools.partial(expert_kernel, layers),
+        out_shape=(
+            jax.ShapeDtypeStruct((lanes, count, width // lanes), jnp.bfloat16),
+            jax.ShapeDtypeStruct((count, width), jnp.bfloat16),
+        ),
+        scratch_shapes=[pltpu.VMEM(arrived.shape, jnp.float32)],
         compiler_params=pltpu.CompilerParams(vmem_limit_bytes=20 << 20),
         name="expert",
-    )(rows, gain.reshape(1, width), gate, up, down)
+    )(arrived, gain.reshape(1, width), gate, up, down)
 
 
 def settle_kernel(lane, parts, rows, result, lines):
     lanes, count, quarter = parts.shape
     pieces, wide = lines.shape[1:]
     own = pl.ds(pl.multiple_of(lane[0] * quarter, quarter), quarter)
-    total = rows[:, :, own].astype(jnp.float32).reshape(count, quarter)
+    total = rows[:, own].astype(jnp.float32)
     for part in range(lanes):
         total = total + parts[part].astype(jnp.float32)
     for piece in range(pieces):
@@ -469,9 +452,10 @@
     summed = swap(project(spread_rows, weights, rows, 3 * cols), "z")
     next_state, spread_out = recurrence(summed, factors, head_state)
     mixed_parts = swap(output(swap(spread_out, "z"), weights, lanes), "tp")
-    arrived = swap(dispatch(mixed_parts, spread_rows, lane, experts), EP)
-    whole = swap(assemble(arrived, layers, lanes, width), "tp")
-    expert_parts = expert_rows(whole, expert_gain, w_gate[0], w_up[0], w_down[0])
+    arrived = swap(dispatch(mixed_parts, spread_rows, experts), EP)
+    expert_parts, whole = expert_rows(
+        arrived, expert_gain, w_gate[0], w_up[0], w_down[0], layers, lanes
+    )
     returned = swap(settle(swap(expert_parts, "tp"), whole, lane), EP)
     layer_out = combine(shares, returned)
     return (layer_out, next_state)

time: 139 us -> 137 us (0.986)
  blocking collectives: 119 us -> 116 us
    all_to_all x7 -> x6, blocking collectives: 98.7 us -> 96 us  [swap(): return lax.all_to_all(array, axis, split_axis=0, concat_axis=0, tiled=True)]
    pallas_call x3 -> x2, Pallas kernels: 1.52 us -> 2.81 us  [the longest x1 1.99 us: expert_rows(): pl.pallas_call(functools.partial(expert_kernel, layers), out_shape=(jax.S...]
where the time goes in v9:
time: 137 us
  blocking collectives  116 us (85%)
  starting transfers between devices  11 us (8%)
  Pallas kernels  9.03 us (7%)
    all_to_all x6, blocking collectives, swap(): return lax.all_to_all(array, axis, split_axis=0, concat_axis=0, tiled=True)  96 us
    all_gather x1, blocking collectives, body(): lax.all_gather(jnp.concatenate([w_query, w_key, w_value, w_out.T], axis=1...  19.9 us
    all_to_all x1, starting transfers between devices, swap(): return lax.all_to_all(array, axis, split_axis=0, concat_axis=0, tiled=True)  11 us
  transfers between devices with their start and end apart: 1, of which 0 were waited for; matrix products, arithmetic and copies ran while one was open for 0% of the time, Pallas kernels for 0%

profile of v9, /device:TPU:1, one launch (start us, length us, event | category | flops | bytes accessed | tf_op | source)
XLA Modules:
  0.0 136.9 jit_solution(11352512487397218134)
XLA Ops:
  0.6 1.7 %norm.1 = (bf16[8,48,256]{2,1,0:T(8,128)(2,1)}, bf16[16,2048]{1,0:T(8,128)(2,1)S(1)}, s32[2,16]{1,0:T(2,128)S(1)}, f32[1,256]{1,0:T(1,128)S(1)}, f32[1,256]{1,0:T(1,128)S(1)}, /*index=5*/f32[2,16]{1,0:T(2,128)S(1)}) custom-call(bf16[16,2048]{1,0:T(8,128)(2,1)} %refs_0_.1, f32[1,2048]{1,0:T(1,128)} %bitcast.30, s32[2,16]{1,0:T(2,128)} %bitcast.32, ...), custom_call_target="tpu_custom_call" | custom-call | tf_op jit(solution)/shard_map/norm/pallas_call | solution.py:66
  2.4 0.0 copy-start.9
  2.4 0.0 copy-start.10
  2.4 0.0 copy-start.11
  2.4 0.0 copy-start.12
  2.4 0.0 copy-start.6
  2.4 0.0 copy-start.7
  2.4 11.0 %all-to-all-start = ((bf16[8,48,256]{2,1,0:T(8,128)(2,1)}), bf16[8,48,256]{2,1,0:T(8,128)(2,1)S(1)}, u32[]{:S(2)}, u32[]{:S(2)}) async-start(bf16[8,48,256]{2,1,0:T(8,128)(2,1)} %get-tuple-element.19), calls=%async_computation | async-start | bytes 393216 | tf_op jit(solution)/shard_map/all_to_all | solution.py:18
  13.5 0.0 copy-start.5
  13.5 19.9 %all-gather.weights = bf16[256,1024]{1,0:T(8,128)(2,1)S(1)} all-gather(bf16[16,1024]{1,0:T(8,128)(2,1)S(1)} %pad_maximum_fusion), channel_id=2, replica_groups=mesh['z'=8,'y'=8,'c'=2,'tp'=4] {'y','c'}, dimensions={0}, use_global_device_ids=true | all-gather | bytes 557056 | tf_op jit(solution)/shard_map/all_gather | solution.py:443
  33.5 0.6 low_rank.1
  34.2 0.2 project.1
  34.4 16.5 %all_to_all.35.parts = bf16[8,16,768]{2,1,0:T(8,128)(2,1)S(1)} all-to-all(bf16[8,16,768]{2,1,0:T(8,128)(2,1)S(1)} %project.1), channel_id=1, replica_groups=mesh['z'=8,'y'=8,'c'=2,'tp'=4] {'z'}, dimensions={0} | all-to-all | bytes 393216 | tf_op jit(solution)/shard_map/all_to_all | solution.py:18
  50.9 2.1 %recurrence.1 = (f32[16,128,128]{2,1,0:T(8,128)}, bf16[8,16,256]{2,1,0:T(8,128)(2,1)S(1)}) custom-call(bf16[8,16,768]{2,1,0:T(8,128)(2,1)S(1)} %all_to_all.35.parts, f32[3,16,256]{2,1,0:T(8,128)S(1)} %get-tuple-element.31.factors, f32[16,128,128]{2,1,0:T(8,128)S(1)} %bitcast.23), custom_call_target="tpu_custom_call" | custom-call | tf_op jit(solution)/shard_map/recurrence/pallas_call | solution.py:239
  53.0 9.6 %all_to_all.36.heads = bf16[8,16,256]{2,1,0:T(8,128)(2,1)S(1)} all-to-all(bf16[8,16,256]{2,1,0:T(8,128)(2,1)S(1)} %get-tuple-element.32), channel_id=1, replica_groups=mesh['z'=8,'y'=8,'c'=2,'tp'=4] {'z'}, dimensions={0} | all-to-all | bytes 131072 | tf_op jit(solution)/shard_map/all_to_all | solution.py:18
  62.6 0.2 output.1
  62.8 9.3 %all_to_all.37.parts = bf16[4,128,256]{2,1,0:T(8,128)(2,1)S(1)} all-to-all(bf16[4,128,256]{2,1,0:T(8,128)(2,1)S(1)} %output.1), channel_id=1, replica_groups=mesh['z'=8,'y'=8,'c'=2,'tp'=4] {'tp'}, dimensions={0} | all-to-all | bytes 524288 | tf_op jit(solution)/shard_map/all_to_all | solution.py:18
  72.2 0.8 dispatch.1
  73.0 30.3 %all_to_all.38.arrived = bf16[128,16,128]{2,1,0:T(8,128)(2,1)S(1)} all-to-all(bf16[128,16,128]{2,1,0:T(8,128)(2,1)S(1)} %dispatch.1), channel_id=1, replica_groups=mesh['z'=8,'y'=8,'c'=2,'tp'=4] {'z','y','c'}, dimensions={0} | all-to-all | bytes 1048576 | tf_op jit(solution)/shard_map/all_to_all | solution.py:18
  103.4 2.0 %expert.1 = (bf16[4,128,512]{2,1,0:T(8,128)(2,1)S(1)}, bf16[128,2048]{1,0:T(8,128)(2,1)S(1)}) custom-call(bf16[128,16,128]{2,1,0:T(8,128)(2,1)S(1)} %all_to_all.38.arrived, f32[1,2048]{1,0:T(1,128)S(1)} %bitcast.29, bf16[2048,128]{1,0:T(8,128)(2,1)S(1)} %bitcast.24, bf16[2048,128]{1,0:T(8,128)(2,1)S(1)} %bitcast.25, bf16[128,2048]{1,0:T(8,128)(2,1)S(1)} %bitcast.26), custom_call_target="tpu_custom_call" | custom-call | tf_op jit(solution)/shard_map/expert/pallas_call | solution.py:346
  105.4 12.2 %all_to_all.39.parts = bf16[4,128,512]{2,1,0:T(8,128)(2,1)S(1)} all-to-all(bf16[4,128,512]{2,1,0:T(8,128)(2,1)S(1)} %get-tuple-element.33), channel_id=1, replica_groups=mesh['z'=8,'y'=8,'c'=2,'tp'=4] {'tp'}, dimensions={0} | all-to-all | bytes 1048576 | tf_op jit(solution)/shard_map/all_to_all | solution.py:18
  117.6 0.3 settle.1
  117.9 18.0 %all_to_all.40.returned = bf16[128,4,128]{2,1,0:T(4,128)(2,1)S(1)} all-to-all(bf16[128,4,128]{2,1,0:T(4,128)(2,1)S(1)} %settle.1), channel_id=1, replica_groups=mesh['z'=8,'y'=8,'c'=2,'tp'=4] {'z','y','c'}, dimensions={0} | all-to-all | bytes 262144 | tf_op jit(solution)/shard_map/all_to_all | solution.py:18
  135.8 1.0 combine.1
  (21 shorter events, 0.1 us)
Async XLA Ops:
  2.4 11.1 %copy-start.9 = (bf16[256,16]{0,1:T(8,128)(2,1)S(1)}, bf16[256,16]{0,1:T(8,128)(2,1)}, u32[]{:S(2)}) copy-start(bf16[256,16]{0,1:T(8,128)(2,1)} %param.31) | copy-start | bytes 24580
  2.4 11.1 %copy-start.10 = (bf16[16,256]{1,0:T(8,128)(2,1)S(1)}, bf16[16,256]{1,0:T(8,128)(2,1)}, u32[]{:S(2)}) copy-start(bf16[16,256]{1,0:T(8,128)(2,1)} %param.24) | copy-start | bytes 24580
  2.4 11.1 %copy-start.11 = (bf16[16,256]{1,0:T(8,128)(2,1)S(1)}, bf16[16,256]{1,0:T(8,128)(2,1)}, u32[]{:S(2)}) copy-start(bf16[16,256]{1,0:T(8,128)(2,1)} %param.23) | copy-start | bytes 24580
  2.4 11.1 %copy-start.12 = (bf16[16,256]{1,0:T(8,128)(2,1)S(1)}, bf16[16,256]{1,0:T(8,128)(2,1)}, u32[]{:S(2)}) copy-start(bf16[16,256]{1,0:T(8,128)(2,1)} %param.22) | copy-start | bytes 24580
  2.4 31.0 %copy-start.6 = (bf16[64,1024]{1,0:T(8,128)(2,1)S(1)}, bf16[64,1024]{1,0:T(8,128)(2,1)}, u32[]{:S(2)}) copy-start(bf16[64,1024]{1,0:T(8,128)(2,1)} %up.1) | copy-start | bytes 393220
  2.4 31.0 %copy-start.7 = (bf16[64,1024]{1,0:T(8,128)(2,1)S(1)}, bf16[64,1024]{1,0:T(8,128)(2,1)}, u32[]{:S(2)}) copy-start(bf16[64,1024]{1,0:T(8,128)(2,1)} %rate_up.1) | copy-start | bytes 393220
  2.4 31.7 %all-to-all-start = ((bf16[8,48,256]{2,1,0:T(8,128)(2,1)}), bf16[8,48,256]{2,1,0:T(8,128)(2,1)S(1)}, u32[]{:S(2)}, u32[]{:S(2)}) async-start(bf16[8,48,256]{2,1,0:T(8,128)(2,1)} %get-tuple-element.19), calls=%async_computation | async-start | bytes 393216 | tf_op jit(solution)/shard_map/all_to_all | solution.py:18
  13.5 20.0 %copy-start.4 = (bf16[2048,64]{0,1:T(8,128)(2,1)S(1)}, bf16[2048,64]{0,1:T(8,128)(2,1)}, u32[]{:S(2)}) copy-start(bf16[2048,64]{0,1:T(8,128)(2,1)} %param.25) | copy-start | bytes 786436
  13.5 20.0 %copy-start.5 = (bf16[2048,64]{0,1:T(8,128)(2,1)S(1)}, bf16[2048,64]{0,1:T(8,128)(2,1)}, u32[]{:S(2)}) copy-start(bf16[2048,64]{0,1:T(8,128)(2,1)} %param.28) | copy-start | bytes 786436
  33.5 17.4 %copy-start = (f32[16,4,4096]{2,1,0:T(4,128)S(1)}, f32[16,4,4096]{2,1,0:T(4,128)}, u32[]{:S(2)}) copy-start(f32[16,4,4096]{2,1,0:T(4,128)} %param.20) | copy-start | bytes 3145732
  72.2 31.2 %copy-start.3 = (bf16[1,128,2048]{2,1,0:T(8,128)(2,1)S(1)}, bf16[1,128,2048]{2,1,0:T(8,128)(2,1)}, u32[]{:S(2)}) copy-start(bf16[1,128,2048]{2,1,0:T(8,128)(2,1)} %param.37) | copy-start | bytes 1572868
  72.2 31.2 %copy-start.8 = (f32[2048]{0:T(1024)S(1)}, f32[2048]{0:T(1024)}, u32[]{:S(2)}) copy-start(f32[2048]{0:T(1024)} %param.32) | copy-start | bytes 24580
  73.0 30.3 %copy-start.1 = (bf16[1,2048,128]{2,1,0:T(8,128)(2,1)S(1)}, bf16[1,2048,128]{2,1,0:T(8,128)(2,1)}, u32[]{:S(2)}) copy-start(bf16[1,2048,128]{2,1,0:T(8,128)(2,1)} %param.35) | copy-start | bytes 1572868
  73.0 30.3 %copy-start.2 = (bf16[1,2048,128]{2,1,0:T(8,128)(2,1)S(1)}, bf16[1,2048,128]{2,1,0:T(8,128)(2,1)}, u32[]{:S(2)}) copy-start(bf16[1,2048,128]{2,1,0:T(8,128)(2,1)} %param.36) | copy-start | bytes 1572868

commit v10 on v9

--- a/solution.py
+++ b/solution.py
@@ -11,6 +11,7 @@
 norm_eps = 1e-06
 group_eps = 0.00064
 EP = ("z", "y", "c")
+BY_PLANE = ("y", "c", "z")
 PLANE = ("y", "c")
 
 
@@ -101,7 +102,7 @@
 
 
 def low_rank_kernel(
-    lane, normed, down, up, base, rate_down, rate_up, gain, ids, route, result, shares
+    layers, lane, normed, down, up, base, rate_down, rate_up, gain, ids, route, result, shares
 ):
     f32, bf16 = jnp.float32, jnp.bfloat16
     _, count, cols = result.shape
@@ -120,6 +121,7 @@
     result[2] = jnp.broadcast_to(gain[...], (count, cols))
     route_sum = jnp.sum(route[...], axis=0, keepdims=True)
     row = lax.broadcasted_iota(jnp.int32, shares.shape, 0)
+    row = lax.rem(row, layers) * (shares.shape[0] // layers) + lax.div(row, layers)
     weights = jnp.zeros(shares.shape, f32)
     for k in range(ids.shape[0]):
         share = route[k : k + 1, :] / route_sum
@@ -127,12 +129,12 @@
     shares[...] = weights
 
 
-def low_rank(normed, decay_down, decay_up, rate_down, rate_up, small, experts, lane):
+def low_rank(normed, decay_down, decay_up, rate_down, rate_up, small, layers, experts, lane):
     ids, base, head_gain, route = small
     count, cols = normed.shape[0], base.shape[1]
     vmem = pl.BlockSpec(memory_space=pltpu.VMEM)
     return pl.pallas_call(
-        low_rank_kernel,
+        functools.partial(low_rank_kernel, layers),
         in_specs=[pl.BlockSpec(memory_space=pltpu.SMEM)] + [vmem] * 9,
         out_specs=(vmem, vmem),
         out_shape=(
@@ -296,8 +298,8 @@
             chosen, residual, (((0,), (0,)), ((), ())), preferred_element_type=f32
         )
         for piece in range(pieces):
-            lines[:, k * pieces + piece, :] = packed[:, piece * wide : (piece + 1) * wide]
-    outbound[...] = lines[...].astype(bf16)
+            lines[:, piece * layers + k, :] = packed[:, piece * wide : (piece + 1) * wide]
+    outbound[...] = lines[:, : pieces * layers, :].astype(bf16)
 
 
 def dispatch(parts, rows, experts):
@@ -307,27 +309,24 @@
     return pl.pallas_call(
         dispatch_kernel,
         out_shape=jax.ShapeDtypeStruct(shape, jnp.bfloat16),
-        scratch_shapes=[pltpu.VMEM(shape, jnp.float32)],
+        scratch_shapes=[pltpu.VMEM((experts, shape[1] + 8, wide), jnp.float32)],
         compiler_params=pltpu.CompilerParams(vmem_limit_bytes=20 << 20),
         name="dispatch",
     )(parts, rows)
 
 
-def expert_kernel(layers, arrived, gain, gate, up, down, result, rows, lines):
+def expert_kernel(layers, arrived, gain, gate, up, down, result, rows):
     lanes, count, quarter = result.shape
     peers = count // layers
     wide = arrived.shape[2]
     pieces = arrived.shape[1] // layers
     f32 = jnp.float32
-    lines[...] = arrived[...].astype(f32)
-    for k in range(layers):
-        for z in range(layers):
-            for piece in range(pieces):
-                start = (z * pieces + piece) * wide
-                block = lines[z * peers : (z + 1) * peers, k * pieces + piece, :]
-                rows[k * peers : (k + 1) * peers, start : start + wide] = block.astype(
-                    jnp.bfloat16
-                )
+    for z in range(layers):
+        blocks = arrived[z * peers : (z + 1) * peers].astype(f32)
+        for piece in range(pieces):
+            start = (z * pieces + piece) * wide
+            block = blocks[:, piece * layers : (piece + 1) * layers, :].reshape(count, wide)
+            rows[:, start : start + wide] = block.astype(jnp.bfloat16)
     widened = rows[...].astype(f32)
     scale = lax.rsqrt(jnp.mean(widened * widened, axis=1, keepdims=True) + norm_eps)
     normed = (widened * scale * gain[...]).astype(jnp.bfloat16)
@@ -349,7 +348,6 @@
             jax.ShapeDtypeStruct((lanes, count, width // lanes), jnp.bfloat16),
             jax.ShapeDtypeStruct((count, width), jnp.bfloat16),
         ),
-        scratch_shapes=[pltpu.VMEM(arrived.shape, jnp.float32)],
         compiler_params=pltpu.CompilerParams(vmem_limit_bytes=20 << 20),
         name="expert",
     )(arrived, gain.reshape(1, width), gate, up, down)
@@ -446,7 +444,7 @@
     weights = weights.reshape(-1, weights.shape[2])
     weights, normed = lax.optimization_barrier((weights, normed))
     factors, shares = low_rank(
-        normed, decay_down, decay_up, rate_down, rate_up, small, experts, lane
+        normed, decay_down, decay_up, rate_down, rate_up, small, layers, experts, lane
     )
     spread_rows, factors, shares = lax.optimization_barrier((spread_rows, factors, shares))
     summed = swap(project(spread_rows, weights, rows, 3 * cols), "z")
@@ -456,7 +454,7 @@
     expert_parts, whole = expert_rows(
         arrived, expert_gain, w_gate[0], w_up[0], w_down[0], layers, lanes
     )
-    returned = swap(settle(swap(expert_parts, "tp"), whole, lane), EP)
+    returned = swap(settle(swap(expert_parts, "tp"), whole, lane), BY_PLANE)
     layer_out = combine(shares, returned)
     return (layer_out, next_state)
 

time: 137 us -> 136 us (level)
  no operation moved by 1% of the time
where the time goes in v10:
time: 136 us
  blocking collectives  116 us (85%)
  starting transfers between devices  11 us (8%)
  Pallas kernels  7.95 us (6%)
    all_to_all x6, blocking collectives, swap(): return lax.all_to_all(array, axis, split_axis=0, concat_axis=0, tiled=True)  95.8 us
    all_gather x1, blocking collectives, body(): lax.all_gather(jnp.concatenate([w_query, w_key, w_value, w_out.T], axis=1...  19.9 us
    all_to_all x1, starting transfers between devices, swap(): return lax.all_to_all(array, axis, split_axis=0, concat_axis=0, tiled=True)  11 us
  transfers between devices with their start and end apart: 1, of which 0 were waited for; matrix products, arithmetic and copies ran while one was open for 0% of the time, Pallas kernels for 0%

profile of v10, /device:TPU:1, one launch (start us, length us, event | category | flops | bytes accessed | tf_op | source)
XLA Modules:
  0.0 135.6 jit_solution(10228868672192149359)
XLA Ops:
  0.6 1.7 %norm.1 = (bf16[8,48,256]{2,1,0:T(8,128)(2,1)}, bf16[16,2048]{1,0:T(8,128)(2,1)S(1)}, s32[2,16]{1,0:T(2,128)S(1)}, f32[1,256]{1,0:T(1,128)S(1)}, f32[1,256]{1,0:T(1,128)S(1)}, /*index=5*/f32[2,16]{1,0:T(2,128)S(1)}) custom-call(bf16[16,2048]{1,0:T(8,128)(2,1)} %refs_0_.1, f32[1,2048]{1,0:T(1,128)} %bitcast.30, s32[2,16]{1,0:T(2,128)} %bitcast.32, ...), custom_call_target="tpu_custom_call" | custom-call | tf_op jit(solution)/shard_map/norm/pallas_call | solution.py:67
  2.4 0.0 copy-start.10
  2.4 0.0 copy-start.11
  2.4 0.0 copy-start.7
  2.4 11.0 %all-to-all-start = ((bf16[8,48,256]{2,1,0:T(8,128)(2,1)}), bf16[8,48,256]{2,1,0:T(8,128)(2,1)S(1)}, u32[]{:S(2)}, u32[]{:S(2)}) async-start(bf16[8,48,256]{2,1,0:T(8,128)(2,1)} %get-tuple-element.19), calls=%async_computation | async-start | bytes 393216 | tf_op jit(solution)/shard_map/all_to_all | solution.py:19
  13.5 0.0 copy-start.4
  13.5 0.0 copy-start.5
  13.5 19.9 %all-gather.weights = bf16[256,1024]{1,0:T(8,128)(2,1)S(1)} all-gather(bf16[16,1024]{1,0:T(8,128)(2,1)S(1)} %pad_maximum_fusion), channel_id=2, replica_groups=mesh['z'=8,'y'=8,'c'=2,'tp'=4] {'y','c'}, dimensions={0}, use_global_device_ids=true | all-gather | bytes 557056 | tf_op jit(solution)/shard_map/all_gather | solution.py:441
  33.5 0.0 copy-start
  33.5 0.6 low_rank.1
  34.2 0.2 project.1
  34.4 16.5 %all_to_all.35.parts = bf16[8,16,768]{2,1,0:T(8,128)(2,1)S(1)} all-to-all(bf16[8,16,768]{2,1,0:T(8,128)(2,1)S(1)} %project.1), channel_id=1, replica_groups=mesh['z'=8,'y'=8,'c'=2,'tp'=4] {'z'}, dimensions={0} | all-to-all | bytes 393216 | tf_op jit(solution)/shard_map/all_to_all | solution.py:19
  50.9 2.1 %recurrence.1 = (f32[16,128,128]{2,1,0:T(8,128)}, bf16[8,16,256]{2,1,0:T(8,128)(2,1)S(1)}) custom-call(bf16[8,16,768]{2,1,0:T(8,128)(2,1)S(1)} %all_to_all.35.parts, f32[3,16,256]{2,1,0:T(8,128)S(1)} %get-tuple-element.31.factors, f32[16,128,128]{2,1,0:T(8,128)S(1)} %bitcast.23), custom_call_target="tpu_custom_call" | custom-call | tf_op jit(solution)/shard_map/recurrence/pallas_call | solution.py:241
  53.0 9.6 %all_to_all.36.heads = bf16[8,16,256]{2,1,0:T(8,128)(2,1)S(1)} all-to-all(bf16[8,16,256]{2,1,0:T(8,128)(2,1)S(1)} %get-tuple-element.32), channel_id=1, replica_groups=mesh['z'=8,'y'=8,'c'=2,'tp'=4] {'z'}, dimensions={0} | all-to-all | bytes 131072 | tf_op jit(solution)/shard_map/all_to_all | solution.py:19
  62.6 0.2 output.1
  62.8 9.3 %all_to_all.37.parts = bf16[4,128,256]{2,1,0:T(8,128)(2,1)S(1)} all-to-all(bf16[4,128,256]{2,1,0:T(8,128)(2,1)S(1)} %output.1), channel_id=1, replica_groups=mesh['z'=8,'y'=8,'c'=2,'tp'=4] {'tp'}, dimensions={0} | all-to-all | bytes 524288 | tf_op jit(solution)/shard_map/all_to_all | solution.py:19
  72.2 0.8 dispatch.1
  73.0 0.0 copy-start.1
  73.0 30.3 %all_to_all.38.arrived = bf16[128,16,128]{2,1,0:T(8,128)(2,1)S(1)} all-to-all(bf16[128,16,128]{2,1,0:T(8,128)(2,1)S(1)} %dispatch.1), channel_id=1, replica_groups=mesh['z'=8,'y'=8,'c'=2,'tp'=4] {'z','y','c'}, dimensions={0} | all-to-all | bytes 1048576 | tf_op jit(solution)/shard_map/all_to_all | solution.py:19
  103.4 0.9 expert.1
  104.3 12.2 %all_to_all.39.parts = bf16[4,128,512]{2,1,0:T(8,128)(2,1)S(1)} all-to-all(bf16[4,128,512]{2,1,0:T(8,128)(2,1)S(1)} %get-tuple-element.33), channel_id=1, replica_groups=mesh['z'=8,'y'=8,'c'=2,'tp'=4] {'tp'}, dimensions={0} | all-to-all | bytes 1048576 | tf_op jit(solution)/shard_map/all_to_all | solution.py:19
  116.5 0.3 settle.1
  116.8 17.8 %all_to_all.40.returned = bf16[128,4,128]{2,1,0:T(4,128)(2,1)S(1)} all-to-all(bf16[128,4,128]{2,1,0:T(4,128)(2,1)S(1)} %settle.1), channel_id=1, replica_groups=mesh['z'=8,'y'=8,'c'=2,'tp'=4] {'y','c','z'}, dimensions={0} | all-to-all | bytes 262144 | tf_op jit(solution)/shard_map/all_to_all | solution.py:19
  134.6 1.0 combine.1
  (21 shorter events, 0.1 us)
Async XLA Ops:
  2.4 11.1 %copy-start.9 = (bf16[256,16]{0,1:T(8,128)(2,1)S(1)}, bf16[256,16]{0,1:T(8,128)(2,1)}, u32[]{:S(2)}) copy-start(bf16[256,16]{0,1:T(8,128)(2,1)} %param.31) | copy-start | bytes 24580
  2.4 11.1 %copy-start.10 = (bf16[16,256]{1,0:T(8,128)(2,1)S(1)}, bf16[16,256]{1,0:T(8,128)(2,1)}, u32[]{:S(2)}) copy-start(bf16[16,256]{1,0:T(8,128)(2,1)} %param.24) | copy-start | bytes 24580
  2.4 11.1 %copy-start.11 = (bf16[16,256]{1,0:T(8,128)(2,1)S(1)}, bf16[16,256]{1,0:T(8,128)(2,1)}, u32[]{:S(2)}) copy-start(bf16[16,256]{1,0:T(8,128)(2,1)} %param.23) | copy-start | bytes 24580
  2.4 11.1 %copy-start.12 = (bf16[16,256]{1,0:T(8,128)(2,1)S(1)}, bf16[16,256]{1,0:T(8,128)(2,1)}, u32[]{:S(2)}) copy-start(bf16[16,256]{1,0:T(8,128)(2,1)} %param.22) | copy-start | bytes 24580
  2.4 31.0 %copy-start.6 = (bf16[64,1024]{1,0:T(8,128)(2,1)S(1)}, bf16[64,1024]{1,0:T(8,128)(2,1)}, u32[]{:S(2)}) copy-start(bf16[64,1024]{1,0:T(8,128)(2,1)} %up.1) | copy-start | bytes 393220
  2.4 31.0 %copy-start.7 = (bf16[64,1024]{1,0:T(8,128)(2,1)S(1)}, bf16[64,1024]{1,0:T(8,128)(2,1)}, u32[]{:S(2)}) copy-start(bf16[64,1024]{1,0:T(8,128)(2,1)} %rate_up.1) | copy-start | bytes 393220
  2.4 31.7 %all-to-all-start = ((bf16[8,48,256]{2,1,0:T(8,128)(2,1)}), bf16[8,48,256]{2,1,0:T(8,128)(2,1)S(1)}, u32[]{:S(2)}, u32[]{:S(2)}) async-start(bf16[8,48,256]{2,1,0:T(8,128)(2,1)} %get-tuple-element.19), calls=%async_computation | async-start | bytes 393216 | tf_op jit(solution)/shard_map/all_to_all | solution.py:19
  13.5 20.0 %copy-start.4 = (bf16[2048,64]{0,1:T(8,128)(2,1)S(1)}, bf16[2048,64]{0,1:T(8,128)(2,1)}, u32[]{:S(2)}) copy-start(bf16[2048,64]{0,1:T(8,128)(2,1)} %param.25) | copy-start | bytes 786436
  13.5 20.0 %copy-start.5 = (bf16[2048,64]{0,1:T(8,128)(2,1)S(1)}, bf16[2048,64]{0,1:T(8,128)(2,1)}, u32[]{:S(2)}) copy-start(bf16[2048,64]{0,1:T(8,128)(2,1)} %param.28) | copy-start | bytes 786436
  33.5 17.4 %copy-start = (f32[16,4,4096]{2,1,0:T(4,128)S(1)}, f32[16,4,4096]{2,1,0:T(4,128)}, u32[]{:S(2)}) copy-start(f32[16,4,4096]{2,1,0:T(4,128)} %param.20) | copy-start | bytes 3145732
  72.2 31.2 %copy-start.3 = (bf16[1,128,2048]{2,1,0:T(8,128)(2,1)S(1)}, bf16[1,128,2048]{2,1,0:T(8,128)(2,1)}, u32[]{:S(2)}) copy-start(bf16[1,128,2048]{2,1,0:T(8,128)(2,1)} %param.37) | copy-start | bytes 1572868
  72.2 31.2 %copy-start.8 = (f32[2048]{0:T(1024)S(1)}, f32[2048]{0:T(1024)}, u32[]{:S(2)}) copy-start(f32[2048]{0:T(1024)} %param.32) | copy-start | bytes 24580
  73.0 30.3 %copy-start.1 = (bf16[1,2048,128]{2,1,0:T(8,128)(2,1)S(1)}, bf16[1,2048,128]{2,1,0:T(8,128)(2,1)}, u32[]{:S(2)}) copy-start(bf16[1,2048,128]{2,1,0:T(8,128)(2,1)} %param.35) | copy-start | bytes 1572868
  73.0 30.3 %copy-start.2 = (bf16[1,2048,128]{2,1,0:T(8,128)(2,1)S(1)}, bf16[1,2048,128]{2,1,0:T(8,128)(2,1)}, u32[]{:S(2)}) copy-start(bf16[1,2048,128]{2,1,0:T(8,128)(2,1)} %param.36) | copy-start | bytes 1572868

commit v11 on v10

--- a/solution.py
+++ b/solution.py
@@ -40,6 +40,7 @@
     normed[...] = scaled
     table_shape = (experts, count)
     row = lax.broadcasted_iota(jnp.int32, table_shape, 0)
+    row = lax.rem(row, layers) * (experts // layers) + lax.div(row, layers)
     named = row == ids[0:1, :]
     for k in range(1, ids.shape[0]):
         named = named | (row == ids[k : k + 1, :])
@@ -321,8 +322,9 @@
     wide = arrived.shape[2]
     pieces = arrived.shape[1] // layers
     f32 = jnp.float32
+    planes = arrived[...].reshape(peers, layers, *arrived.shape[1:])
     for z in range(layers):
-        blocks = arrived[z * peers : (z + 1) * peers].astype(f32)
+        blocks = planes[:, z].astype(f32)
         for piece in range(pieces):
             start = (z * pieces + piece) * wide
             block = blocks[:, piece * layers : (piece + 1) * layers, :].reshape(count, wide)
@@ -450,7 +452,7 @@
     summed = swap(project(spread_rows, weights, rows, 3 * cols), "z")
     next_state, spread_out = recurrence(summed, factors, head_state)
     mixed_parts = swap(output(swap(spread_out, "z"), weights, lanes), "tp")
-    arrived = swap(dispatch(mixed_parts, spread_rows, experts), EP)
+    arrived = swap(dispatch(mixed_parts, spread_rows, experts), BY_PLANE)
     expert_parts, whole = expert_rows(
         arrived, expert_gain, w_gate[0], w_up[0], w_down[0], layers, lanes
     )

time: 136 us -> 136 us (level)
  no operation moved by 1% of the time
where the time goes in v11:
time: 136 us
  blocking collectives  116 us (85%)
  starting transfers between devices  11 us (8%)
  Pallas kernels  7.94 us (6%)
    all_to_all x6, blocking collectives, swap(): return lax.all_to_all(array, axis, split_axis=0, concat_axis=0, tiled=True)  95.8 us
    all_gather x1, blocking collectives, body(): lax.all_gather(jnp.concatenate([w_query, w_key, w_value, w_out.T], axis=1...  19.9 us
    all_to_all x1, starting transfers between devices, swap(): return lax.all_to_all(array, axis, split_axis=0, concat_axis=0, tiled=True)  11 us
  transfers between devices with their start and end apart: 1, of which 0 were waited for; matrix products, arithmetic and copies ran while one was open for 0% of the time, Pallas kernels for 0%

profile of v11, /device:TPU:1, one launch (start us, length us, event | category | flops | bytes accessed | tf_op | source)
XLA Modules:
  0.0 135.6 jit_solution(66095371746011513)
XLA Ops:
  0.6 1.7 %norm.1 = (bf16[8,48,256]{2,1,0:T(8,128)(2,1)}, bf16[16,2048]{1,0:T(8,128)(2,1)S(1)}, s32[2,16]{1,0:T(2,128)S(1)}, f32[1,256]{1,0:T(1,128)S(1)}, f32[1,256]{1,0:T(1,128)S(1)}, /*index=5*/f32[2,16]{1,0:T(2,128)S(1)}) custom-call(bf16[16,2048]{1,0:T(8,128)(2,1)} %refs_0_.1, f32[1,2048]{1,0:T(1,128)} %bitcast.30, s32[2,16]{1,0:T(2,128)} %bitcast.32, ...), custom_call_target="tpu_custom_call" | custom-call | tf_op jit(solution)/shard_map/norm/pallas_call | solution.py:68
  2.4 0.0 copy-start.9
  2.4 0.0 copy-start.10
  2.4 0.0 copy-start.11
  2.4 0.0 copy-start.12
  2.4 0.0 copy-start.6
  2.4 0.0 copy-start.7
  2.5 11.0 %all-to-all-start = ((bf16[8,48,256]{2,1,0:T(8,128)(2,1)}), bf16[8,48,256]{2,1,0:T(8,128)(2,1)S(1)}, u32[]{:S(2)}, u32[]{:S(2)}) async-start(bf16[8,48,256]{2,1,0:T(8,128)(2,1)} %get-tuple-element.19), calls=%async_computation | async-start | bytes 393216 | tf_op jit(solution)/shard_map/all_to_all | solution.py:19
  13.5 19.9 %all-gather.weights = bf16[256,1024]{1,0:T(8,128)(2,1)S(1)} all-gather(bf16[16,1024]{1,0:T(8,128)(2,1)S(1)} %pad_maximum_fusion), channel_id=2, replica_groups=mesh['z'=8,'y'=8,'c'=2,'tp'=4] {'y','c'}, dimensions={0}, use_global_device_ids=true | all-gather | bytes 557056 | tf_op jit(solution)/shard_map/all_gather | solution.py:443
  33.5 0.6 low_rank.1
  34.2 0.2 project.1
  34.4 16.5 %all_to_all.35.parts = bf16[8,16,768]{2,1,0:T(8,128)(2,1)S(1)} all-to-all(bf16[8,16,768]{2,1,0:T(8,128)(2,1)S(1)} %project.1), channel_id=1, replica_groups=mesh['z'=8,'y'=8,'c'=2,'tp'=4] {'z'}, dimensions={0} | all-to-all | bytes 393216 | tf_op jit(solution)/shard_map/all_to_all | solution.py:19
  50.9 2.1 %recurrence.1 = (f32[16,128,128]{2,1,0:T(8,128)}, bf16[8,16,256]{2,1,0:T(8,128)(2,1)S(1)}) custom-call(bf16[8,16,768]{2,1,0:T(8,128)(2,1)S(1)} %all_to_all.35.parts, f32[3,16,256]{2,1,0:T(8,128)S(1)} %get-tuple-element.31.factors, f32[16,128,128]{2,1,0:T(8,128)S(1)} %bitcast.23), custom_call_target="tpu_custom_call" | custom-call | tf_op jit(solution)/shard_map/recurrence/pallas_call | solution.py:242
  53.0 9.6 %all_to_all.36.heads = bf16[8,16,256]{2,1,0:T(8,128)(2,1)S(1)} all-to-all(bf16[8,16,256]{2,1,0:T(8,128)(2,1)S(1)} %get-tuple-element.32), channel_id=1, replica_groups=mesh['z'=8,'y'=8,'c'=2,'tp'=4] {'z'}, dimensions={0} | all-to-all | bytes 131072 | tf_op jit(solution)/shard_map/all_to_all | solution.py:19
  62.6 0.2 output.1
  62.8 9.3 %all_to_all.37.parts = bf16[4,128,256]{2,1,0:T(8,128)(2,1)S(1)} all-to-all(bf16[4,128,256]{2,1,0:T(8,128)(2,1)S(1)} %output.1), channel_id=1, replica_groups=mesh['z'=8,'y'=8,'c'=2,'tp'=4] {'tp'}, dimensions={0} | all-to-all | bytes 524288 | tf_op jit(solution)/shard_map/all_to_all | solution.py:19
  72.2 0.8 dispatch.1
  73.0 0.0 copy-start.1
  73.0 30.7 %all_to_all.38.arrived = bf16[128,16,128]{2,1,0:T(8,128)(2,1)S(1)} all-to-all(bf16[128,16,128]{2,1,0:T(8,128)(2,1)S(1)} %dispatch.1), channel_id=1, replica_groups=mesh['z'=8,'y'=8,'c'=2,'tp'=4] {'y','c','z'}, dimensions={0} | all-to-all | bytes 1048576 | tf_op jit(solution)/shard_map/all_to_all | solution.py:19
  103.8 0.9 expert.1
  104.7 11.8 %all_to_all.39.parts = bf16[4,128,512]{2,1,0:T(8,128)(2,1)S(1)} all-to-all(bf16[4,128,512]{2,1,0:T(8,128)(2,1)S(1)} %get-tuple-element.33), channel_id=1, replica_groups=mesh['z'=8,'y'=8,'c'=2,'tp'=4] {'tp'}, dimensions={0} | all-to-all | bytes 1048576 | tf_op jit(solution)/shard_map/all_to_all | solution.py:19
  116.5 0.3 settle.1
  116.8 17.8 %all_to_all.40.returned = bf16[128,4,128]{2,1,0:T(4,128)(2,1)S(1)} all-to-all(bf16[128,4,128]{2,1,0:T(4,128)(2,1)S(1)} %settle.1), channel_id=1, replica_groups=mesh['z'=8,'y'=8,'c'=2,'tp'=4] {'y','c','z'}, dimensions={0} | all-to-all | bytes 262144 | tf_op jit(solution)/shard_map/all_to_all | solution.py:19
  134.6 1.0 combine.1
  (21 shorter events, 0.1 us)
Async XLA Ops:
  2.4 11.1 %copy-start.9 = (bf16[256,16]{0,1:T(8,128)(2,1)S(1)}, bf16[256,16]{0,1:T(8,128)(2,1)}, u32[]{:S(2)}) copy-start(bf16[256,16]{0,1:T(8,128)(2,1)} %param.31) | copy-start | bytes 24580
  2.4 11.1 %copy-start.10 = (bf16[16,256]{1,0:T(8,128)(2,1)S(1)}, bf16[16,256]{1,0:T(8,128)(2,1)}, u32[]{:S(2)}) copy-start(bf16[16,256]{1,0:T(8,128)(2,1)} %param.24) | copy-start | bytes 24580
  2.4 11.1 %copy-start.11 = (bf16[16,256]{1,0:T(8,128)(2,1)S(1)}, bf16[16,256]{1,0:T(8,128)(2,1)}, u32[]{:S(2)}) copy-start(bf16[16,256]{1,0:T(8,128)(2,1)} %param.23) | copy-start | bytes 24580
  2.4 11.1 %copy-start.12 = (bf16[16,256]{1,0:T(8,128)(2,1)S(1)}, bf16[16,256]{1,0:T(8,128)(2,1)}, u32[]{:S(2)}) copy-start(bf16[16,256]{1,0:T(8,128)(2,1)} %param.22) | copy-start | bytes 24580
  2.4 31.0 %copy-start.6 = (bf16[64,1024]{1,0:T(8,128)(2,1)S(1)}, bf16[64,1024]{1,0:T(8,128)(2,1)}, u32[]{:S(2)}) copy-start(bf16[64,1024]{1,0:T(8,128)(2,1)} %up.1) | copy-start | bytes 393220
  2.4 31.0 %copy-start.7 = (bf16[64,1024]{1,0:T(8,128)(2,1)S(1)}, bf16[64,1024]{1,0:T(8,128)(2,1)}, u32[]{:S(2)}) copy-start(bf16[64,1024]{1,0:T(8,128)(2,1)} %rate_up.1) | copy-start | bytes 393220
  2.5 31.7 %all-to-all-start = ((bf16[8,48,256]{2,1,0:T(8,128)(2,1)}), bf16[8,48,256]{2,1,0:T(8,128)(2,1)S(1)}, u32[]{:S(2)}, u32[]{:S(2)}) async-start(bf16[8,48,256]{2,1,0:T(8,128)(2,1)} %get-tuple-element.19), calls=%async_computation | async-start | bytes 393216 | tf_op jit(solution)/shard_map/all_to_all | solution.py:19
  13.5 20.0 %copy-start.4 = (bf16[2048,64]{0,1:T(8,128)(2,1)S(1)}, bf16[2048,64]{0,1:T(8,128)(2,1)}, u32[]{:S(2)}) copy-start(bf16[2048,64]{0,1:T(8,128)(2,1)} %param.25) | copy-start | bytes 786436
  13.5 20.0 %copy-start.5 = (bf16[2048,64]{0,1:T(8,128)(2,1)S(1)}, bf16[2048,64]{0,1:T(8,128)(2,1)}, u32[]{:S(2)}) copy-start(bf16[2048,64]{0,1:T(8,128)(2,1)} %param.28) | copy-start | bytes 786436
  33.5 17.4 %copy-start = (f32[16,4,4096]{2,1,0:T(4,128)S(1)}, f32[16,4,4096]{2,1,0:T(4,128)}, u32[]{:S(2)}) copy-start(f32[16,4,4096]{2,1,0:T(4,128)} %param.20) | copy-start | bytes 3145732
  72.2 31.6 %copy-start.3 = (bf16[1,128,2048]{2,1,0:T(8,128)(2,1)S(1)}, bf16[1,128,2048]{2,1,0:T(8,128)(2,1)}, u32[]{:S(2)}) copy-start(bf16[1,128,2048]{2,1,0:T(8,128)(2,1)} %param.37) | copy-start | bytes 1572868
  72.2 31.6 %copy-start.8 = (f32[2048]{0:T(1024)S(1)}, f32[2048]{0:T(1024)}, u32[]{:S(2)}) copy-start(f32[2048]{0:T(1024)} %param.32) | copy-start | bytes 24580
  73.0 30.7 %copy-start.1 = (bf16[1,2048,128]{2,1,0:T(8,128)(2,1)S(1)}, bf16[1,2048,128]{2,1,0:T(8,128)(2,1)}, u32[]{:S(2)}) copy-start(bf16[1,2048,128]{2,1,0:T(8,128)(2,1)} %param.35) | copy-start | bytes 1572868
  73.0 30.7 %copy-start.2 = (bf16[1,2048,128]{2,1,0:T(8,128)(2,1)S(1)}, bf16[1,2048,128]{2,1,0:T(8,128)(2,1)}, u32[]{:S(2)}) copy-start(bf16[1,2048,128]{2,1,0:T(8,128)(2,1)} %param.36) | copy-start | bytes 1572868
